TPU v7x, 256 devices: a whole 4x4x8 slice. The times are simulated.
256 devices in a mesh: ra: 16 (over y, x), cb: 16 (over z, core).
Axes of the slice: x: 4, y: 4, z: 8, core: 2. Of those that a mesh axis runs over, the one named last changes fastest.
Arguments:
- tokens: bfloat16 [768, 4096], P(None, 'ra'), may hold values from -27 to 27, as said below
- gain_first: float32 [4096], P('ra'), may hold values from 0.1 to 1.9
- up_first: bfloat16 [4096, 16384], P('ra', 'cb'), may hold values from -0.09375 to 0.09375
- down_first: bfloat16 [16384, 4096], P('cb', 'ra'), may hold values from -0.046875 to 0.046875
- gain_second: float32 [4096], P('ra'), may hold values from 0.1 to 1.9
- up_second: bfloat16 [4096, 16384], P('ra', 'cb'), may hold values from -0.09375 to 0.09375
- down_second: bfloat16 [16384, 4096], P('cb', 'ra'), may hold values from -0.046875 to 0.046875
Outputs:
- mixed: bfloat16 [768, 4096], P(None, 'ra')
Inputs may be any that keep to these rules, and one draw needn't show every extreme that they name: `tokens`: channels come in 32 groups of equal width with different scales.
All inputs are finite; a program needn't handle non-finite values.
Results may differ from a plain program's by a relative error of at most 0.0079.
Values may be sent and summed in bfloat16 or wider, within the bound.
No kernel may reach another device: no remote copies, remote signals or barrier semaphores. Data moves between devices by JAX's collectives and lax.ppermute only.
A program may use at most 64 MiB of HBM per device.

v0:
```python
import functools

import jax
import jax.numpy as jnp
from jax import lax
from jax.experimental import pallas as pl
from jax.experimental.pallas import tpu as pltpu
from jax.sharding import Mesh, PartitionSpec as P


RA = ("y", "x")
BF = jnp.bfloat16
F32 = jnp.float32
LANES = 128
EPS = 1e-06


def exchange(parts, axis):
    return lax.all_to_all(parts, axis, 0, 0, tiled=True)


def from_other_core(w):
    return lax.ppermute(w, "c", [(0, 1), (1, 0)])


def along_y(a, shift):
    n = lax.axis_size("y")
    return lax.ppermute(a, "y", [(i, (i + shift) % n) for i in range(n)])


def by_plane(a, sign):
    ny, nz = lax.axis_size("y"), lax.axis_size("z")
    perm = [(y * nz + z, (y + sign * (z // 2)) % ny * nz + z) for y in range(ny) for z in range(nz)]
    return lax.ppermute(a, ("y", "z"), perm)


def call(kernel, out, scratch=(), limit=16, whole=None):
    vmem = pl.BlockSpec(memory_space=pltpu.VMEM)
    lies = pl.BlockSpec(memory_space=pltpu.HBM)

    def run(*args):
        first = len(args) if whole is None else whole
        return pl.pallas_call(
            kernel,
            out_shape=out,
            in_specs=[vmem] * first + [lies] * (len(args) - first),
            out_specs=jax.tree.map(lambda _: vmem, out),
            scratch_shapes=list(scratch),
            compiler_params=pltpu.CompilerParams(vmem_limit_bytes=limit << 20),
        )(*args)

    return run


def sds(shape, dtype=BF):
    return jax.ShapeDtypeStruct(shape, dtype)


def stat_columns(sq):
    high = sq.astype(BF)
    low = (sq - high.astype(F32)).astype(BF)
    lane = lax.broadcasted_iota(jnp.int32, (sq.shape[0], LANES), 1)
    block = jnp.where(lane == 0, high.astype(F32), jnp.where(lane == 1, low.astype(F32), 0.0))
    return block.astype(BF)


def fetch(sources, held, sems):
    copies = [pltpu.make_async_copy(w, held.at[i], sems.at[i]) for i, w in enumerate(sources)]
    for copy in copies:
        copy.start()
    return copies


def up_first_kernel(tokens, gain, own, other, out, x, g, held, sems, few_sems):
    half, hid = x.shape[0], own.shape[1]
    start = pl.multiple_of(lax.axis_index("c") * half, half)
    first = [
        pltpu.make_async_copy(tokens.at[pl.ds(start, half), :], x, few_sems.at[0]),
        pltpu.make_async_copy(gain, g, few_sems.at[1]),
    ]
    for copy in first:
        copy.start()
    copies = fetch((own, other), held, sems)
    for copy in first:
        copy.wait()
    xf = x[...].astype(F32)
    out[:, 2 * hid :] = stat_columns(jnp.sum(xf * xf, axis=1, keepdims=True))
    scaled = (xf * g[...]).astype(BF)
    for i, copy in enumerate(copies):
        copy.wait()
        out[:, i * hid : (i + 1) * hid] = jnp.dot(scaled, held[i], preferred_element_type=F32).astype(BF)


def summed(parts):
    total = parts[0].astype(F32)
    for i in range(1, parts.shape[0]):
        total += parts[i].astype(F32)
    return total


def activate_kernel(parts, out, *, width):
    hid = parts.shape[2] - LANES
    total = summed(parts)
    meansq = (total[:, hid : hid + 1] + total[:, hid + 1 : hid + 2]) / width
    act = jnp.maximum(total[:, :hid] * lax.rsqrt(meansq + EPS), 0.0)
    act = (act * act).astype(BF)
    for i in range(out.shape[0]):
        out[i] = act


def down_kernel(hidden, *refs):
    *blocks, out, held, sems = refs
    copies = fetch(blocks, held, sems)
    n = len(blocks) // 2
    k = blocks[0].shape[0]
    for d in range(n):
        copies[d].wait()
        acc = jnp.dot(hidden[:, :k], held[d], preferred_element_type=F32)
        copies[n + d].wait()
        acc += jnp.dot(hidden[:, k:], held[n + d], preferred_element_type=F32)
        acc = acc.astype(BF)
        out[2 * d] = acc[:, :LANES]
        out[2 * d + 1] = acc[:, LANES:]


def finish_first_kernel(parts, kept, mid, payload):
    rows = mid.shape[0]
    x = (0.5 * kept[:rows, :] + summed(parts)).astype(BF)
    gain = kept[rows:, :]
    high = gain.astype(BF).astype(F32)
    rest = gain - high
    middle = rest.astype(BF).astype(F32)
    low = rest - middle
    row = lax.broadcasted_iota(jnp.int32, gain.shape, 0)
    coded = jnp.where(row == 0, high, jnp.where(row == 1, middle, low)).astype(BF)
    mid[...] = x
    for i in range(payload.shape[0]):
        payload[i, :rows, :] = x
        payload[i, rows:, :] = coded


def up_second_kernel(x, *refs):
    *blocks, out, held, sems = refs
    copies = fetch(blocks, held, sems)
    n = len(blocks) // 2
    depth, hid = blocks[0].shape
    rows = out.shape[0]
    scaled, sq = [], jnp.zeros((rows, 1), F32)
    for i in range(x.shape[0]):
        xf = x[i, :rows, :].astype(F32)
        coded = x[i, rows:, :].astype(F32)
        gain = coded[0:1] + coded[1:2] + coded[2:3]
        sq += jnp.sum(xf * xf, axis=1, keepdims=True)
        scaled.append((xf * gain).astype(BF))
    scaled = jnp.concatenate(scaled, axis=1)
    for side in range(2):
        acc = jnp.zeros((rows, hid), F32)
        for d in range(n):
            copies[side * n + d].wait()
            acc += jnp.dot(
                scaled[:, d * depth : (d + 1) * depth], held[side * n + d], preferred_element_type=F32
            )
        out[:, side * hid : (side + 1) * hid] = acc.astype(BF)
    out[:, 2 * hid :] = stat_columns(sq)


def finish_second_kernel(parts, kept, out):
    out[...] = (0.5 * kept[...].astype(F32) + summed(parts)).astype(BF)


def assemble_kernel(own, other, out):
    chunks, rows, _ = own.shape
    n = chunks // 2
    y, c = lax.axis_index("y"), lax.axis_index("c")
    for side, ref in ((c, own), (1 - c, other)):
        for d in range(n):
            start = pl.multiple_of((side * n + lax.rem(y + d, n)) * rows, rows)
            out[pl.ds(start, rows), :LANES] = ref[2 * d]
            out[pl.ds(start, rows), LANES:] = ref[2 * d + 1]


def spread(x, peers):
    return jnp.broadcast_to(x[None], (peers, *x.shape))


def after(w, done):
    return lax.optimization_barrier((w, done))


def around(w):
    own = [w] + [along_y(w, d) for d in range(1, lax.axis_size("y"))]
    return own + [from_other_core(v) for v in own]


def body(tokens, gain_first, up_first, down_first, gain_second, up_second, down_second):
    ny, nx, nz = lax.axis_size("y"), lax.axis_size("x"), lax.axis_size("z")
    y, z, c = lax.axis_index("y"), lax.axis_index("z"), lax.axis_index("c")
    count, channels = tokens.shape
    width = channels * ny * nx
    half = count // 2
    per_y = half // ny
    few = per_y // nx
    hid = 2 * up_first.shape[1]
    wide = hid + LANES
    blocks = 2 * ny

    def held(n, w):
        return [pltpu.VMEM((n, *w.shape), BF), pltpu.SemaphoreType.DMA((n,))]

    activate = call(functools.partial(activate_kernel, width=width), sds((nx, few, hid)))
    down = call(down_kernel, sds((nz, per_y, LANES)), held(blocks, down_first), whole=1)

    arrays = [pltpu.VMEM((half, channels), BF), pltpu.VMEM((1, channels), F32)]
    scratch = arrays + held(2, up_first) + [pltpu.SemaphoreType.DMA((2,))]
    payload = call(up_first_kernel, sds((half, wide)), scratch, whole=0)(
        tokens, gain_first[None, :], up_first, from_other_core(up_first)
    )
    start = c * half + lax.rem(y + z // 2, ny) * per_y
    column = lax.rem(z, 2) * LANES
    kept = lax.dynamic_slice(tokens, (start, column), (per_y, LANES)).astype(F32)
    gain = lax.dynamic_slice(gain_second, (column,), (LANES,))
    kept = jnp.concatenate([kept, spread(gain, 8)], axis=0)
    kept, payload = after(kept, payload)
    parts = exchange(payload.reshape(ny * nx, few, wide), RA)
    kept = by_plane(kept, 1)
    down_first, kept = after(down_first, kept)
    downs = around(down_first)
    hidden = activate(parts)

    hidden = exchange(hidden, "x").reshape(per_y, hid)
    ups = around(up_second)
    branch = down(hidden, *downs)
    branch = exchange(branch, "z")
    downs = around(down_second)
    middle, payload = call(finish_first_kernel, (sds((per_y, LANES)), sds((nz, per_y + 8, LANES))))(
        branch, kept
    )
    payload = exchange(payload, "z")
    payload = call(up_second_kernel, sds((per_y, wide)), held(blocks, up_second), whole=1)(payload, *ups)
    parts = exchange(payload.reshape(nx, few, wide), "x")
    hidden = activate(parts)
    hidden = exchange(hidden, "x").reshape(per_y, hid)
    branch = down(hidden, *downs)
    finished = call(finish_second_kernel, sds((per_y, LANES)))(exchange(branch, "z"), middle)
    rows = exchange(spread(by_plane(finished, -1), nz), "z")
    return call(assemble_kernel, sds((count, channels)))(rows, from_other_core(rows))


def solution(mesh):
    fine = Mesh(mesh.devices.reshape(4, 4, 8, 2), ("y", "x", "z", "c"))
    cb = ("z", "c")
    placed = (
        P(None, RA),
        P(RA),
        P(RA, cb),
        P(cb, RA),
        P(RA),
        P(RA, cb),
        P(cb, RA),
    )

    return jax.shard_map(body, mesh=fine, in_specs=placed, out_specs=P(None, RA), check_vma=False)
```

profile of v0, /device:TPU:1, one launch (start us, length us, event | category | flops | bytes accessed | tf_op | source)
XLA Modules:
  0.0 189.7 jit_solution(9314494409437453465)
XLA Ops:
  0.0 3.2 %collective-permute-start = (bf16[256,1024]{1,0:T(8,128)(2,1)}, bf16[256,1024]{1,0:T(8,128)(2,1)S(1)}, u32[]{:S(2)}, u32[]{:S(2)}) collective-permute-start(bf16[256,1024]{1,0:T(8,128)(2,1)} %own.1), channel_id=1, source_target_pairs={{0,1},{1,0},{2,3},{3,2},{4,5},{5,4},{6,7},{7,6},{8,9},{9,8},{10,11... | collective-permute-start | bytes 1572872 | tf_op jit(solution)/shard_map/ppermute | solution.py:23
  7.7 2.4 %shard_map.73 = bf16[384,2176]{1,0:T(8,128)(2,1)} custom-call(bf16[768,256]{1,0:T(8,128)(2,1)S(1)} %copy-done.6, f32[1,256]{1,0:T(1,128)S(1)} %bitcast.7, bf16[256,1024]{1,0:T(8,128)(2,1)S(1)} %copy-done.5, bf16[256,1024]{1,0:T(8,128)(2,1)S(1)} %collective-permute-done.other), custom_call_target="tpu_custom_call" | custom-call | tf_op jit(solution)/shard_map/pallas_call | solution.py:43
  10.1 5.2 %all-to-all-start = ((bf16[16,24,2176]{2,1,0:T(8,128)(2,1)}), bf16[16,24,2176]{2,1,0:T(8,128)(2,1)S(1)}, u32[]{:S(2)}, u32[]{:S(2)}) async-start(bf16[16,24,2176]{2,1,0:T(8,128)(2,1)} %bitcast.1), calls=%async_computation | async-start | bytes 3342336 | tf_op jit(solution)/shard_map/all_to_all | solution.py:19
  17.4 2.4 %collective-permute-start.3 = (bf16[1024,256]{1,0:T(8,128)(2,1)S(1)}, bf16[1024,256]{1,0:T(8,128)(2,1)}, u32[]{:S(2)}, u32[]{:S(2)}) collective-permute-start(bf16[1024,256]{1,0:T(8,128)(2,1)S(1)} %copy-done), channel_id=1, source_target_pairs={{0,128},{64,192},{128,0},{192,64},{1,129},{65,193},{129,1},{193,65... | collective-permute-start | bytes 1572872 | tf_op jit(solution)/shard_map/ppermute | solution.py:28
  23.4 24.1 %collective-permute-done.2.refs_1_ = bf16[1024,256]{1,0:T(8,128)(2,1)} collective-permute-done((bf16[1024,256]{1,0:T(8,128)(2,1)S(1)}, bf16[1024,256]{1,0:T(8,128)(2,1)}, u32[]{:S(2)}, u32[]{:S(2)}) %collective-permute-start.2) | collective-permute-done | bytes 524320 | tf_op jit(solution)/shard_map/ppermute | solution.py:28
  47.5 13.5 %collective-permute-start.6 = (bf16[1024,256]{1,0:T(8,128)(2,1)}, bf16[1024,256]{1,0:T(8,128)(2,1)}, u32[]{:S(2)}, u32[]{:S(2)}) collective-permute-start(bf16[1024,256]{1,0:T(8,128)(2,1)} %collective-permute-done.2.refs_1_), channel_id=1, source_target_pairs={{0,1},{1,0},{2,3},{3,2},{4,5},{5,4},{6,7},{7,6},{8,9},{9,8},{10,11... | collective-permute-start | bytes 1572872 | tf_op jit(solution)/shard_map/ppermute | solution.py:23
  61.7 8.2 %collective-permute-done.9.refs_1_ = bf16[256,1024]{1,0:T(8,128)(2,1)S(1)} collective-permute-done((bf16[256,1024]{1,0:T(8,128)(2,1)S(1)}, bf16[256,1024]{1,0:T(8,128)(2,1)S(1)}, u32[]{:S(2)}, u32[]{:S(2)}) %collective-permute-start.9) | collective-permute-done | bytes 524320 | tf_op jit(solution)/shard_map/ppermute | solution.py:28
  73.3 4.7 %all-to-all-start.1 = ((bf16[4,24,2048]{2,1,0:T(8,128)(2,1)}), bf16[4,24,2048]{2,1,0:T(8,128)(2,1)S(1)}, u32[]{:S(2)}, u32[]{:S(2)}) async-start(bf16[4,24,2048]{2,1,0:T(8,128)(2,1)} %shard_map.74), calls=%async_computation.1 | async-start | bytes 786432 | tf_op jit(solution)/shard_map/all_to_all | solution.py:19
  79.7 5.0 %all-to-all-done.1 = bf16[4,24,2048]{2,1,0:T(8,128)(2,1)S(1)} async-done(((bf16[4,24,2048]{2,1,0:T(8,128)(2,1)}), bf16[4,24,2048]{2,1,0:T(8,128)(2,1)S(1)}, u32[]{:S(2)}, u32[]{:S(2)}) %all-to-all-start.1) | async-done | bytes 393248 | tf_op jit(solution)/shard_map/all_to_all | solution.py:19
  85.7 3.7 %shard_map.75 = bf16[8,96,128]{2,1,0:T(8,128)(2,1)} custom-call(bf16[96,2048]{1,0:T(8,128)(2,1)S(1)} %bitcast.5, bf16[1024,256]{1,0:T(8,128)(2,1)S(1)} %copy-done, bf16[1024,256]{1,0:T(8,128)(2,1)} %collective-permute-done.2.refs_1_, bf16[1024,256]{1,0:T(8,128)(2,1)} %collective-permute-done.3.refs_2_, bf16[1024,256]{1,0:T(8,128)(2,1)} %collective-permute-done.4.refs_3_, ...), custom_call_target="tpu_custom_call" | custom-call | tf_op jit(solution)/shard_map/pallas_call | solution.py:43
  89.4 12.4 %all-to-all-start.2 = ((bf16[8,96,128]{2,1,0:T(8,128)(2,1)}), bf16[8,96,128]{2,1,0:T(8,128)(2,1)S(1)}, u32[]{:S(2)}, u32[]{:S(2)}) async-start(bf16[8,96,128]{2,1,0:T(8,128)(2,1)} %shard_map.75), calls=%async_computation.2 | async-start | bytes 393216 | tf_op jit(solution)/shard_map/all_to_all | solution.py:19
  101.8 3.4 %collective-permute-start.14 = (bf16[256,1024]{1,0:T(8,128)(2,1)}, bf16[256,1024]{1,0:T(8,128)(2,1)}, u32[]{:S(2)}, u32[]{:S(2)}) collective-permute-start(bf16[256,1024]{1,0:T(8,128)(2,1)} %collective-permute-done.10.refs_2_), channel_id=1, source_target_pairs={{0,1},{1,0},{2,3},{3,2},{4,5},{5,4},{6,7},{7,6},{8,9},{9,8},{10,11... | collective-permute-start | bytes 1572872 | tf_op jit(solution)/shard_map/ppermute | solution.py:23
  105.8 2.9 %collective-permute-start.17 = (bf16[1024,256]{1,0:T(8,128)(2,1)S(1)}, bf16[1024,256]{1,0:T(8,128)(2,1)S(1)}, u32[]{:S(2)}, u32[]{:S(2)}) collective-permute-start(bf16[1024,256]{1,0:T(8,128)(2,1)S(1)} %copy-done.2), channel_id=1, source_target_pairs={{0,128},{64,192},{128,0},{192,64},{1,129},{65,193},{129,1},{193,65... | collective-permute-start | bytes 1572872 | tf_op jit(solution)/shard_map/ppermute | solution.py:28
  111.2 5.4 %all-to-all-start.3 = ((bf16[8,104,128]{2,1,0:T(8,128)(2,1)}), bf16[8,104,128]{2,1,0:T(8,128)(2,1)S(1)}, u32[]{:S(2)}, u32[]{:S(2)}) async-start(bf16[8,104,128]{2,1,0:T(8,128)(2,1)} %get-tuple-element.15), calls=%async_computation.3 | async-start | bytes 425984 | tf_op jit(solution)/shard_map/all_to_all | solution.py:19
  116.6 8.8 %all-to-all-done.3.x = bf16[8,104,128]{2,1,0:T(8,128)(2,1)S(1)} async-done(((bf16[8,104,128]{2,1,0:T(8,128)(2,1)}), bf16[8,104,128]{2,1,0:T(8,128)(2,1)S(1)}, u32[]{:S(2)}, u32[]{:S(2)}) %all-to-all-start.3) | async-done | bytes 213024 | tf_op jit(solution)/shard_map/all_to_all | solution.py:19
  125.5 3.0 %shard_map.77 = bf16[96,2176]{1,0:T(8,128)(2,1)} custom-call(bf16[8,104,128]{2,1,0:T(8,128)(2,1)S(1)} %all-to-all-done.3.x, bf16[256,1024]{1,0:T(8,128)(2,1)S(1)} %copy-done.1, bf16[256,1024]{1,0:T(8,128)(2,1)S(1)} %collective-permute-done.9.refs_1_, bf16[256,1024]{1,0:T(8,128)(2,1)} %collective-permute-done.10.refs_2_, ...), custom_call_target="tpu_custom_call" | custom-call | tf_op jit(solution)/shard_map/pallas_call | solution.py:43
  128.5 3.5 %all-to-all-start.4 = ((bf16[4,24,2176]{2,1,0:T(8,128)(2,1)}), bf16[4,24,2176]{2,1,0:T(8,128)(2,1)S(1)}, u32[]{:S(2)}, u32[]{:S(2)}) async-start(bf16[4,24,2176]{2,1,0:T(8,128)(2,1)} %bitcast.3), calls=%async_computation.4 | async-start | bytes 835584 | tf_op jit(solution)/shard_map/all_to_all | solution.py:19
  132.0 3.5 %collective-permute-start.19 = (bf16[1024,256]{1,0:T(8,128)(2,1)S(1)}, bf16[1024,256]{1,0:T(8,128)(2,1)S(1)}, u32[]{:S(2)}, u32[]{:S(2)}) collective-permute-start(bf16[1024,256]{1,0:T(8,128)(2,1)S(1)} %copy-done.2), channel_id=1, source_target_pairs={{0,1},{1,0},{2,3},{3,2},{4,5},{5,4},{6,7},{7,6},{8,9},{9,8},{10,11... | collective-permute-start | bytes 1572872 | tf_op jit(solution)/shard_map/ppermute | solution.py:23
  139.2 3.5 %all-to-all-start.5 = ((bf16[4,24,2048]{2,1,0:T(8,128)(2,1)}), bf16[4,24,2048]{2,1,0:T(8,128)(2,1)S(1)}, u32[]{:S(2)}, u32[]{:S(2)}) async-start(bf16[4,24,2048]{2,1,0:T(8,128)(2,1)} %shard_map.78), calls=%async_computation.5 | async-start | bytes 786432 | tf_op jit(solution)/shard_map/all_to_all | solution.py:19
  142.7 6.2 %all-to-all-done.5 = bf16[4,24,2048]{2,1,0:T(8,128)(2,1)S(1)} async-done(((bf16[4,24,2048]{2,1,0:T(8,128)(2,1)}), bf16[4,24,2048]{2,1,0:T(8,128)(2,1)S(1)}, u32[]{:S(2)}, u32[]{:S(2)}) %all-to-all-start.5) | async-done | bytes 393248 | tf_op jit(solution)/shard_map/all_to_all | solution.py:19
  148.9 2.3 %shard_map.79 = bf16[8,96,128]{2,1,0:T(8,128)(2,1)S(1)} custom-call(bf16[96,2048]{1,0:T(8,128)(2,1)S(1)} %bitcast.6, bf16[1024,256]{1,0:T(8,128)(2,1)S(1)} %copy-done.2, bf16[1024,256]{1,0:T(8,128)(2,1)S(1)} %collective-permute-done.16.refs_1_, bf16[1024,256]{1,0:T(8,128)(2,1)S(1)} %collective-permute-done.17.refs_2_, ...), custom_call_target="tpu_custom_call" | custom-call | tf_op jit(solution)/shard_map/pallas_call | solution.py:43
  151.1 11.0 %all_to_all.40.parts = bf16[8,96,128]{2,1,0:T(8,128)(2,1)S(1)} all-to-all(bf16[8,96,128]{2,1,0:T(8,128)(2,1)S(1)} %shard_map.79), channel_id=1, replica_groups=mesh['y'=4,'x'=4,'z'=8,'c'=2] {'z'}, dimensions={0} | all-to-all | bytes 393216 | tf_op jit(solution)/shard_map/all_to_all | solution.py:19
  162.9 15.4 %all_to_all.41.own = bf16[8,96,128]{2,1,0:T(8,128)(2,1)S(1)} all-to-all(bf16[8,96,128]{2,1,0:T(8,128)(2,1)S(1)} %broadcast_in_dim.8), channel_id=1, replica_groups=mesh['y'=4,'x'=4,'z'=8,'c'=2] {'z'}, dimensions={0} | all-to-all | bytes 393216 | tf_op jit(solution)/shard_map/all_to_all | solution.py:19
  178.3 9.5 %collective-permute-start.24 = (bf16[8,96,128]{2,1,0:T(8,128)(2,1)S(1)}, bf16[8,96,128]{2,1,0:T(8,128)(2,1)S(1)}, u32[]{:S(2)}, u32[]{:S(2)}) collective-permute-start(bf16[8,96,128]{2,1,0:T(8,128)(2,1)S(1)} %all_to_all.41.own), channel_id=1, source_target_pairs={{0,1},{1,0},{2,3},{3,2},{4,5},{5,4},{6,7},{7,6},{8,9},{9,8},{10,11... | collective-permute-start | bytes 589832 | tf_op jit(solution)/shard_map/ppermute | solution.py:23
  (70 shorter events, 26.4 us)
Async XLA Ops:
  10.1 62.0 %all-to-all-start = ((bf16[16,24,2176]{2,1,0:T(8,128)(2,1)}), bf16[16,24,2176]{2,1,0:T(8,128)(2,1)S(1)}, u32[]{:S(2)}, u32[]{:S(2)}) async-start(bf16[16,24,2176]{2,1,0:T(8,128)(2,1)} %bitcast.1), calls=%async_computation | async-start | bytes 3342336 | tf_op jit(solution)/shard_map/all_to_all | solution.py:19
  16.0 31.5 %collective-permute-start.2 = (bf16[1024,256]{1,0:T(8,128)(2,1)S(1)}, bf16[1024,256]{1,0:T(8,128)(2,1)}, u32[]{:S(2)}, u32[]{:S(2)}) collective-permute-start(bf16[1024,256]{1,0:T(8,128)(2,1)S(1)} %copy-done), channel_id=1, source_target_pairs={{0,64},{64,128},{128,192},{192,0},{1,65},{65,129},{129,193},{193,1... | collective-permute-start | bytes 1572872 | tf_op jit(solution)/shard_map/ppermute | solution.py:28
  17.4 43.6 %collective-permute-start.3 = (bf16[1024,256]{1,0:T(8,128)(2,1)S(1)}, bf16[1024,256]{1,0:T(8,128)(2,1)}, u32[]{:S(2)}, u32[]{:S(2)}) collective-permute-start(bf16[1024,256]{1,0:T(8,128)(2,1)S(1)} %copy-done), channel_id=1, source_target_pairs={{0,128},{64,192},{128,0},{192,64},{1,129},{65,193},{129,1},{193,65... | collective-permute-start | bytes 1572872 | tf_op jit(solution)/shard_map/ppermute | solution.py:28
  19.8 41.8 %collective-permute-start.4 = (bf16[1024,256]{1,0:T(8,128)(2,1)S(1)}, bf16[1024,256]{1,0:T(8,128)(2,1)}, u32[]{:S(2)}, u32[]{:S(2)}) collective-permute-start(bf16[1024,256]{1,0:T(8,128)(2,1)S(1)} %copy-done), channel_id=1, source_target_pairs={{0,192},{64,0},{128,64},{192,128},{1,193},{65,1},{129,65},{193,129... | collective-permute-start | bytes 1572872 | tf_op jit(solution)/shard_map/ppermute | solution.py:28
  21.0 48.8 %collective-permute-start.9 = (bf16[256,1024]{1,0:T(8,128)(2,1)S(1)}, bf16[256,1024]{1,0:T(8,128)(2,1)S(1)}, u32[]{:S(2)}, u32[]{:S(2)}) collective-permute-start(bf16[256,1024]{1,0:T(8,128)(2,1)S(1)} %copy-done.1), channel_id=1, source_target_pairs={{0,64},{64,128},{128,192},{192,0},{1,65},{65,129},{129,193},{193,1... | collective-permute-start | bytes 1572872 | tf_op jit(solution)/shard_map/ppermute | solution.py:28
  21.3 49.4 %collective-permute-start.5 = (bf16[1024,256]{1,0:T(8,128)(2,1)S(1)}, bf16[1024,256]{1,0:T(8,128)(2,1)S(1)}, u32[]{:S(2)}, u32[]{:S(2)}) collective-permute-start(bf16[1024,256]{1,0:T(8,128)(2,1)S(1)} %copy-done), channel_id=1, source_target_pairs={{0,1},{1,0},{2,3},{3,2},{4,5},{5,4},{6,7},{7,6},{8,9},{9,8},{10,11... | collective-permute-start | bytes 1572872 | tf_op jit(solution)/shard_map/ppermute | solution.py:23
  47.5 30.5 %collective-permute-start.6 = (bf16[1024,256]{1,0:T(8,128)(2,1)}, bf16[1024,256]{1,0:T(8,128)(2,1)}, u32[]{:S(2)}, u32[]{:S(2)}) collective-permute-start(bf16[1024,256]{1,0:T(8,128)(2,1)} %collective-permute-done.2.refs_1_), channel_id=1, source_target_pairs={{0,1},{1,0},{2,3},{3,2},{4,5},{5,4},{6,7},{7,6},{8,9},{9,8},{10,11... | collective-permute-start | bytes 1572872 | tf_op jit(solution)/shard_map/ppermute | solution.py:23
  61.0 18.6 %collective-permute-start.7 = (bf16[1024,256]{1,0:T(8,128)(2,1)}, bf16[1024,256]{1,0:T(8,128)(2,1)}, u32[]{:S(2)}, u32[]{:S(2)}) collective-permute-start(bf16[1024,256]{1,0:T(8,128)(2,1)} %collective-permute-done.3.refs_2_), channel_id=1, source_target_pairs={{0,1},{1,0},{2,3},{3,2},{4,5},{5,4},{6,7},{7,6},{8,9},{9,8},{10,11... | collective-permute-start | bytes 1572872 | tf_op jit(solution)/shard_map/ppermute | solution.py:23
  61.7 18.0 %collective-permute-start.8 = (bf16[1024,256]{1,0:T(8,128)(2,1)}, bf16[1024,256]{1,0:T(8,128)(2,1)}, u32[]{:S(2)}, u32[]{:S(2)}) collective-permute-start(bf16[1024,256]{1,0:T(8,128)(2,1)} %collective-permute-done.4.refs_3_), channel_id=1, source_target_pairs={{0,1},{1,0},{2,3},{3,2},{4,5},{5,4},{6,7},{7,6},{8,9},{9,8},{10,11... | collective-permute-start | bytes 1572872 | tf_op jit(solution)/shard_map/ppermute | solution.py:23
  69.8 32.0 %collective-permute-start.10 = (bf16[256,1024]{1,0:T(8,128)(2,1)S(1)}, bf16[256,1024]{1,0:T(8,128)(2,1)}, u32[]{:S(2)}, u32[]{:S(2)}) collective-permute-start(bf16[256,1024]{1,0:T(8,128)(2,1)S(1)} %copy-done.1), channel_id=1, source_target_pairs={{0,128},{64,192},{128,0},{192,64},{1,129},{65,193},{129,1},{193,65... | collective-permute-start | bytes 1572872 | tf_op jit(solution)/shard_map/ppermute | solution.py:28
  71.5 33.7 %collective-permute-start.11 = (bf16[256,1024]{1,0:T(8,128)(2,1)S(1)}, bf16[256,1024]{1,0:T(8,128)(2,1)}, u32[]{:S(2)}, u32[]{:S(2)}) collective-permute-start(bf16[256,1024]{1,0:T(8,128)(2,1)S(1)} %copy-done.1), channel_id=1, source_target_pairs={{0,192},{64,0},{128,64},{192,128},{1,193},{65,1},{129,65},{193,129... | collective-permute-start | bytes 1572872 | tf_op jit(solution)/shard_map/ppermute | solution.py:28
  73.3 11.4 %all-to-all-start.1 = ((bf16[4,24,2048]{2,1,0:T(8,128)(2,1)}), bf16[4,24,2048]{2,1,0:T(8,128)(2,1)S(1)}, u32[]{:S(2)}, u32[]{:S(2)}) async-start(bf16[4,24,2048]{2,1,0:T(8,128)(2,1)} %shard_map.74), calls=%async_computation.1 | async-start | bytes 786432 | tf_op jit(solution)/shard_map/all_to_all | solution.py:19
  78.0 27.8 %collective-permute-start.12 = (bf16[256,1024]{1,0:T(8,128)(2,1)S(1)}, bf16[256,1024]{1,0:T(8,128)(2,1)}, u32[]{:S(2)}, u32[]{:S(2)}) collective-permute-start(bf16[256,1024]{1,0:T(8,128)(2,1)S(1)} %copy-done.1), channel_id=1, source_target_pairs={{0,1},{1,0},{2,3},{3,2},{4,5},{5,4},{6,7},{7,6},{8,9},{9,8},{10,11... | collective-permute-start | bytes 1572872 | tf_op jit(solution)/shard_map/ppermute | solution.py:23
  79.6 29.1 %collective-permute-start.13 = (bf16[256,1024]{1,0:T(8,128)(2,1)S(1)}, bf16[256,1024]{1,0:T(8,128)(2,1)}, u32[]{:S(2)}, u32[]{:S(2)}) collective-permute-start(bf16[256,1024]{1,0:T(8,128)(2,1)S(1)} %collective-permute-done.9.refs_1_), channel_id=1, source_target_pairs={{0,1},{1,0},{2,3},{3,2},{4,5},{5,4},{6,7},{7,6},{8,9},{9,8},{10,11... | collective-permute-start | bytes 1572872 | tf_op jit(solution)/shard_map/ppermute | solution.py:23
  89.4 21.1 %all-to-all-start.2 = ((bf16[8,96,128]{2,1,0:T(8,128)(2,1)}), bf16[8,96,128]{2,1,0:T(8,128)(2,1)S(1)}, u32[]{:S(2)}, u32[]{:S(2)}) async-start(bf16[8,96,128]{2,1,0:T(8,128)(2,1)} %shard_map.75), calls=%async_computation.2 | async-start | bytes 393216 | tf_op jit(solution)/shard_map/all_to_all | solution.py:19
  101.8 14.8 %collective-permute-start.14 = (bf16[256,1024]{1,0:T(8,128)(2,1)}, bf16[256,1024]{1,0:T(8,128)(2,1)}, u32[]{:S(2)}, u32[]{:S(2)}) collective-permute-start(bf16[256,1024]{1,0:T(8,128)(2,1)} %collective-permute-done.10.refs_2_), channel_id=1, source_target_pairs={{0,1},{1,0},{2,3},{3,2},{4,5},{5,4},{6,7},{7,6},{8,9},{9,8},{10,11... | collective-permute-start | bytes 1572872 | tf_op jit(solution)/shard_map/ppermute | solution.py:23
  105.3 11.4 %collective-permute-start.15 = (bf16[256,1024]{1,0:T(8,128)(2,1)}, bf16[256,1024]{1,0:T(8,128)(2,1)}, u32[]{:S(2)}, u32[]{:S(2)}) collective-permute-start(bf16[256,1024]{1,0:T(8,128)(2,1)} %collective-permute-done.11.refs_3_), channel_id=1, source_target_pairs={{0,1},{1,0},{2,3},{3,2},{4,5},{5,4},{6,7},{7,6},{8,9},{9,8},{10,11... | collective-permute-start | bytes 1572872 | tf_op jit(solution)/shard_map/ppermute | solution.py:23
  105.4 30.1 %collective-permute-start.16 = (bf16[1024,256]{1,0:T(8,128)(2,1)S(1)}, bf16[1024,256]{1,0:T(8,128)(2,1)S(1)}, u32[]{:S(2)}, u32[]{:S(2)}) collective-permute-start(bf16[1024,256]{1,0:T(8,128)(2,1)S(1)} %copy-done.2), channel_id=1, source_target_pairs={{0,64},{64,128},{128,192},{192,0},{1,65},{65,129},{129,193},{193,1... | collective-permute-start | bytes 1572872 | tf_op jit(solution)/shard_map/ppermute | solution.py:28
  105.8 29.8 %collective-permute-start.17 = (bf16[1024,256]{1,0:T(8,128)(2,1)S(1)}, bf16[1024,256]{1,0:T(8,128)(2,1)S(1)}, u32[]{:S(2)}, u32[]{:S(2)}) collective-permute-start(bf16[1024,256]{1,0:T(8,128)(2,1)S(1)} %copy-done.2), channel_id=1, source_target_pairs={{0,128},{64,192},{128,0},{192,64},{1,129},{65,193},{129,1},{193,65... | collective-permute-start | bytes 1572872 | tf_op jit(solution)/shard_map/ppermute | solution.py:28
  108.7 27.3 %collective-permute-start.18 = (bf16[1024,256]{1,0:T(8,128)(2,1)S(1)}, bf16[1024,256]{1,0:T(8,128)(2,1)}, u32[]{:S(2)}, u32[]{:S(2)}) collective-permute-start(bf16[1024,256]{1,0:T(8,128)(2,1)S(1)} %copy-done.2), channel_id=1, source_target_pairs={{0,192},{64,0},{128,64},{192,128},{1,193},{65,1},{129,65},{193,129... | collective-permute-start | bytes 1572872 | tf_op jit(solution)/shard_map/ppermute | solution.py:28
  111.2 14.2 %all-to-all-start.3 = ((bf16[8,104,128]{2,1,0:T(8,128)(2,1)}), bf16[8,104,128]{2,1,0:T(8,128)(2,1)S(1)}, u32[]{:S(2)}, u32[]{:S(2)}) async-start(bf16[8,104,128]{2,1,0:T(8,128)(2,1)} %get-tuple-element.15), calls=%async_computation.3 | async-start | bytes 425984 | tf_op jit(solution)/shard_map/all_to_all | solution.py:19
  128.5 9.8 %all-to-all-start.4 = ((bf16[4,24,2176]{2,1,0:T(8,128)(2,1)}), bf16[4,24,2176]{2,1,0:T(8,128)(2,1)S(1)}, u32[]{:S(2)}, u32[]{:S(2)}) async-start(bf16[4,24,2176]{2,1,0:T(8,128)(2,1)} %bitcast.3), calls=%async_computation.4 | async-start | bytes 835584 | tf_op jit(solution)/shard_map/all_to_all | solution.py:19
  132.0 10.7 %collective-permute-start.19 = (bf16[1024,256]{1,0:T(8,128)(2,1)S(1)}, bf16[1024,256]{1,0:T(8,128)(2,1)S(1)}, u32[]{:S(2)}, u32[]{:S(2)}) collective-permute-start(bf16[1024,256]{1,0:T(8,128)(2,1)S(1)} %copy-done.2), channel_id=1, source_target_pairs={{0,1},{1,0},{2,3},{3,2},{4,5},{5,4},{6,7},{7,6},{8,9},{9,8},{10,11... | collective-permute-start | bytes 1572872 | tf_op jit(solution)/shard_map/ppermute | solution.py:23
  178.3 10.6 %collective-permute-start.24 = (bf16[8,96,128]{2,1,0:T(8,128)(2,1)S(1)}, bf16[8,96,128]{2,1,0:T(8,128)(2,1)S(1)}, u32[]{:S(2)}, u32[]{:S(2)}) collective-permute-start(bf16[8,96,128]{2,1,0:T(8,128)(2,1)S(1)} %all_to_all.41.own), channel_id=1, source_target_pairs={{0,1},{1,0},{2,3},{3,2},{4,5},{5,4},{6,7},{7,6},{8,9},{9,8},{10,11... | collective-permute-start | bytes 589832 | tf_op jit(solution)/shard_map/ppermute | solution.py:23
  (15 other events, 78.0 us)
where the time goes:
time: 191 us; the launch traced here: 190 us
  starting transfers between devices  84.8 us (44%)
  waiting for transfers between devices  57.2 us (30%)
  blocking collectives  26.4 us (14%)
  Pallas kernels  15 us (8%)
  local copies, waits for them, and re-layouts  5.35 us (3%)
    ppermute x14, starting transfers between devices, from_other_core(): return lax.ppermute(w, 'c', [(0, 1), (1, 0)])  38.3 us
    all_to_all x6, starting transfers between devices, exchange(): return lax.all_to_all(parts, axis, 0, 0, tiled=True)  34.7 us
    ppermute x9, waiting for transfers between devices, along_y(): return lax.ppermute(a, 'y', [(i, (i + shift) % n) for i in range(n)])  32.3 us
    all_to_all x2, blocking collectives, exchange(): return lax.all_to_all(parts, axis, 0, 0, tiled=True)  26.4 us
    all_to_all x6, waiting for transfers between devices, exchange(): return lax.all_to_all(parts, axis, 0, 0, tiled=True)  23.5 us
    pallas_call x9, Pallas kernels, run(): pl.pallas_call(kernel, out_shape=out, in_specs=[vmem] * first + [lies] *...  15 us
    ppermute x9, starting transfers between devices, along_y(): return lax.ppermute(a, 'y', [(i, (i + shift) % n) for i in range(n)])  10.5 us
    unnamed x16, local copies, waits for them, and re-layouts  4.57 us
  transfers between devices with their start and end apart: 31, of which 9 were waited for; matrix products, arithmetic and copies ran while one was open for 1% of the time, Pallas kernels for 5%

commit v1 on v0

--- a/solution.py
+++ b/solution.py
@@ -28,24 +28,27 @@
     return lax.ppermute(a, "y", [(i, (i + shift) % n) for i in range(n)])
 
 
-def by_plane(a, sign):
+def by_plane(a, steps):
     ny, nz = lax.axis_size("y"), lax.axis_size("z")
-    perm = [(y * nz + z, (y + sign * (z // 2)) % ny * nz + z) for y in range(ny) for z in range(nz)]
+    perm = [(y * nz + z, (y + steps(z)) % ny * nz + z) for y in range(ny) for z in range(nz)]
     return lax.ppermute(a, ("y", "z"), perm)
 
 
-def call(kernel, out, scratch=(), limit=16, whole=None):
+def call(kernel, out, scratch=(), limit=16, whole=None, update=None):
     vmem = pl.BlockSpec(memory_space=pltpu.VMEM)
-    lies = pl.BlockSpec(memory_space=pltpu.HBM)
+    lies = pl.BlockSpec(memory_space=pltpu.HBM if update is None else pl.ANY)
 
     def run(*args):
         first = len(args) if whole is None else whole
+        if update is None:
+            args = [*args[:first], *(pltpu.with_memory_space_constraint(a, pltpu.HBM) for a in args[first:])]
         return pl.pallas_call(
             kernel,
             out_shape=out,
             in_specs=[vmem] * first + [lies] * (len(args) - first),
-            out_specs=jax.tree.map(lambda _: vmem, out),
+            out_specs=jax.tree.map(lambda _: vmem if update is None else lies, out),
             scratch_shapes=list(scratch),
+            input_output_aliases={} if update is None else {update: 0},
             compiler_params=pltpu.CompilerParams(vmem_limit_bytes=limit << 20),
         )(*args)
 
@@ -64,31 +67,46 @@
     return block.astype(BF)
 
 
-def fetch(sources, held, sems):
-    copies = [pltpu.make_async_copy(w, held.at[i], sems.at[i]) for i, w in enumerate(sources)]
+def fetch(pairs, sems):
+    copies = [pltpu.make_async_copy(source, held, sems.at[i]) for i, (source, held) in enumerate(pairs)]
     for copy in copies:
         copy.start()
     return copies
 
 
-def up_first_kernel(tokens, gain, own, other, out, x, g, held, sems, few_sems):
+def up_own_kernel(gain, next_gain, tokens, own, out, scaled, kept, x, some, w, sems):
     half, hid = x.shape[0], own.shape[1]
-    start = pl.multiple_of(lax.axis_index("c") * half, half)
-    first = [
-        pltpu.make_async_copy(tokens.at[pl.ds(start, half), :], x, few_sems.at[0]),
-        pltpu.make_async_copy(gain, g, few_sems.at[1]),
-    ]
-    for copy in first:
-        copy.start()
-    copies = fetch((own, other), held, sems)
-    for copy in first:
-        copy.wait()
+    rows = some.shape[0]
+    y, z, c = lax.axis_index("y"), lax.axis_index("z"), lax.axis_index("c")
+    first = pl.multiple_of(c * half, half)
+    there = lax.rem(y + z // 2, lax.axis_size("y"))
+    copies = fetch(
+        (
+            (tokens.at[pl.ds(first, half), :], x),
+            (own, w),
+            (tokens.at[pl.ds(pl.multiple_of(first + there * rows, rows), rows), :], some),
+        ),
+        sems,
+    )
+    copies[0].wait()
     xf = x[...].astype(F32)
     out[:, 2 * hid :] = stat_columns(jnp.sum(xf * xf, axis=1, keepdims=True))
-    scaled = (xf * g[...]).astype(BF)
-    for i, copy in enumerate(copies):
-        copy.wait()
-        out[:, i * hid : (i + 1) * hid] = jnp.dot(scaled, held[i], preferred_element_type=F32).astype(BF)
+    scaled[...] = (xf * gain[...]).astype(BF)
+    copies[1].wait()
+    out[:, :hid] = jnp.dot(scaled[...], w[...], preferred_element_type=F32).astype(BF)
+    copies[2].wait()
+    left = lax.rem(z, 2) == 0
+    kept[:rows, :] = jnp.where(left, some[:, :LANES].astype(F32), some[:, LANES:].astype(F32))
+    chosen = jnp.where(left, next_gain[:, :LANES], next_gain[:, LANES:])
+    kept[rows:, :] = jnp.broadcast_to(chosen, (8, LANES))
+
+
+def up_other_kernel(scaled, other, so_far, out, w, part, sems):
+    del so_far
+    hid = other.shape[1]
+    fetch(((other, w),), sems)[0].wait()
+    part[...] = jnp.dot(scaled[...], w[...], preferred_element_type=F32).astype(BF)
+    fetch(((part, out.at[:, hid : 2 * hid]),), sems)[0].wait()
 
 
 def summed(parts):
@@ -108,16 +126,42 @@
         out[i] = act
 
 
+def spots(blocks, held):
+    pairs, i = [], 0
+    for block in blocks:
+        if isinstance(block, tuple):
+            rows = block[0].shape[0]
+            pairs += [(block[0], held.at[i, :rows]), (block[1], held.at[i, rows:])]
+        else:
+            pairs.append((block, held.at[i]))
+        i += 1
+    return pairs
+
+
+def grouped(refs, n):
+    if len(refs) == n:
+        return list(refs)
+    middle = n // 2
+    return [*refs[:middle], (refs[middle], refs[middle + 1]), *refs[middle + 2 :]]
+
+
 def down_kernel(hidden, *refs):
     *blocks, out, held, sems = refs
-    copies = fetch(blocks, held, sems)
-    n = len(blocks) // 2
-    k = blocks[0].shape[0]
+    n, k = held.shape[0] // 2, held.shape[1]
+    per = len(blocks) // 2
+    copies = fetch(spots(grouped(blocks[:per], n) + grouped(blocks[per:], n), held), sems)
+    waited = [0, 0]
+
+    def ready(side, d):
+        upto = per if d == n - 1 else (d + 1 if d < n // 2 else d + 1 + per - n)
+        for i in range(waited[side], upto):
+            copies[side * per + i].wait()
+        waited[side] = upto
+        return held[side * n + d]
+
     for d in range(n):
-        copies[d].wait()
-        acc = jnp.dot(hidden[:, :k], held[d], preferred_element_type=F32)
-        copies[n + d].wait()
-        acc += jnp.dot(hidden[:, k:], held[n + d], preferred_element_type=F32)
+        acc = jnp.dot(hidden[:, :k], ready(0, d), preferred_element_type=F32)
+        acc += jnp.dot(hidden[:, k:], ready(1, d), preferred_element_type=F32)
         acc = acc.astype(BF)
         out[2 * d] = acc[:, :LANES]
         out[2 * d + 1] = acc[:, LANES:]
@@ -141,7 +185,7 @@
 
 def up_second_kernel(x, *refs):
     *blocks, out, held, sems = refs
-    copies = fetch(blocks, held, sems)
+    copies = fetch(spots(blocks, held), sems)
     n = len(blocks) // 2
     depth, hid = blocks[0].shape
     rows = out.shape[0]
@@ -187,14 +231,18 @@
     return lax.optimization_barrier((w, done))
 
 
-def around(w):
-    own = [w] + [along_y(w, d) for d in range(1, lax.axis_size("y"))]
+def around(w, forward=False):
+    n = lax.axis_size("y")
+    own = [w] + [along_y(w, d) for d in range(1, n) if not (forward and d == n // 2)]
+    if forward:
+        half = w.shape[0] // 2
+        far = [along_y(own[1][:half], 1), along_y(own[-1][half:], n - 1)]
+        own[n // 2 : n // 2] = far
     return own + [from_other_core(v) for v in own]
 
 
 def body(tokens, gain_first, up_first, down_first, gain_second, up_second, down_second):
     ny, nx, nz = lax.axis_size("y"), lax.axis_size("x"), lax.axis_size("z")
-    y, z, c = lax.axis_index("y"), lax.axis_index("z"), lax.axis_index("c")
     count, channels = tokens.shape
     width = channels * ny * nx
     half = count // 2
@@ -204,45 +252,48 @@
     wide = hid + LANES
     blocks = 2 * ny
 
-    def held(n, w):
-        return [pltpu.VMEM((n, *w.shape), BF), pltpu.SemaphoreType.DMA((n,))]
+    def held(w, more=0):
+        return [pltpu.VMEM((blocks, *w.shape), BF), pltpu.SemaphoreType.DMA((blocks + more,))]
 
     activate = call(functools.partial(activate_kernel, width=width), sds((nx, few, hid)))
-    down = call(down_kernel, sds((nz, per_y, LANES)), held(blocks, down_first), whole=1)
-
-    arrays = [pltpu.VMEM((half, channels), BF), pltpu.VMEM((1, channels), F32)]
-    scratch = arrays + held(2, up_first) + [pltpu.SemaphoreType.DMA((2,))]
-    payload = call(up_first_kernel, sds((half, wide)), scratch, whole=0)(
-        tokens, gain_first[None, :], up_first, from_other_core(up_first)
-    )
-    start = c * half + lax.rem(y + z // 2, ny) * per_y
-    column = lax.rem(z, 2) * LANES
-    kept = lax.dynamic_slice(tokens, (start, column), (per_y, LANES)).astype(F32)
-    gain = lax.dynamic_slice(gain_second, (column,), (LANES,))
-    kept = jnp.concatenate([kept, spread(gain, 8)], axis=0)
-    kept, payload = after(kept, payload)
+
+    block = pltpu.VMEM(up_first.shape, BF)
+    payload, scaled, kept = call(
+        up_own_kernel,
+        (sds((half, wide)), sds((half, channels)), sds((per_y + 8, LANES), F32)),
+        [pltpu.VMEM((half, channels), BF), pltpu.VMEM((per_y, channels), BF), block, pltpu.SemaphoreType.DMA((3,))],
+        whole=2,
+    )(gain_first[None, :], gain_second[None, :], tokens, up_first)
+    payload = call(
+        up_other_kernel,
+        sds((half, wide)),
+        [block, pltpu.VMEM((half, hid // 2), BF), pltpu.SemaphoreType.DMA((1,))],
+        whole=1,
+        update=2,
+    )(scaled, from_other_core(up_first), payload)
     parts = exchange(payload.reshape(ny * nx, few, wide), RA)
-    kept = by_plane(kept, 1)
+    kept = by_plane(kept, lambda z: max(z // 2, 1))
+    kept = by_plane(kept, lambda z: -1 if z < 2 else 0)
     down_first, kept = after(down_first, kept)
-    downs = around(down_first)
+    downs = around(down_first, forward=True)
     hidden = activate(parts)
 
     hidden = exchange(hidden, "x").reshape(per_y, hid)
     ups = around(up_second)
-    branch = down(hidden, *downs)
+    branch = call(down_kernel, sds((nz, per_y, LANES)), held(down_first, 2), whole=1)(hidden, *downs)
     branch = exchange(branch, "z")
     downs = around(down_second)
     middle, payload = call(finish_first_kernel, (sds((per_y, LANES)), sds((nz, per_y + 8, LANES))))(
         branch, kept
     )
     payload = exchange(payload, "z")
-    payload = call(up_second_kernel, sds((per_y, wide)), held(blocks, up_second), whole=1)(payload, *ups)
+    payload = call(up_second_kernel, sds((per_y, wide)), held(up_second), whole=1)(payload, *ups)
     parts = exchange(payload.reshape(nx, few, wide), "x")
     hidden = activate(parts)
     hidden = exchange(hidden, "x").reshape(per_y, hid)
-    branch = down(hidden, *downs)
+    branch = call(down_kernel, sds((nz, per_y, LANES)), held(down_second), whole=1)(hidden, *downs)
     finished = call(finish_second_kernel, sds((per_y, LANES)))(exchange(branch, "z"), middle)
-    rows = exchange(spread(by_plane(finished, -1), nz), "z")
+    rows = exchange(spread(by_plane(finished, lambda z: -(z // 2)), nz), "z")
     return call(assemble_kernel, sds((count, channels)))(rows, from_other_core(rows))
 
 

time: 191 us -> 186 us (0.974)
  waiting for transfers between devices: 57.2 us -> 46.9 us
  starting transfers between devices: 84.8 us -> 90.7 us
  Pallas kernels: 15 us -> 18.9 us
  local copies, waits for them, and re-layouts: 5.35 us -> 2.57 us
    ppermute x9 -> x10, waiting for transfers between devices: 32.3 us -> 4.07 us  [along_y(): return lax.ppermute(a, 'y', [(i, (i + shift) % n) for i in range(n)])]
    ppermute x2 -> x3, waiting for transfers between devices: 0.01 us -> 17.2 us  [by_plane(): return lax.ppermute(a, ('y', 'z'), perm)]
    all_to_all x6, starting transfers between devices: 34.7 us -> 28 us  [exchange(): return lax.all_to_all(parts, axis, 0, 0, tiled=True)]
    ppermute x14 -> x15, starting transfers between devices: 38.3 us -> 45 us  [from_other_core(): return lax.ppermute(w, 'c', [(0, 1), (1, 0)])]
    ppermute x2 -> x3, starting transfers between devices: 1.33 us -> 5.73 us  [by_plane(): return lax.ppermute(a, ('y', 'z'), perm)]
    pallas_call x9 -> x10, Pallas kernels: 15 us -> 18.9 us  [run(): pl.pallas_call(kernel, out_shape=out, in_specs=[vmem] * first + [lies] *...]
    unnamed x16 -> x28, local copies, waits for them, and re-layouts: 4.57 us -> 2.5 us
    ppermute x9 -> x10, starting transfers between devices: 10.5 us -> 11.9 us  [along_y(): return lax.ppermute(a, 'y', [(i, (i + shift) % n) for i in range(n)])]
  transfers between devices with their start and end apart: 31 -> 34, of which waited for: 9 -> 10; matrix products, arithmetic and copies ran while one was open for 1% -> 0% of each run, Pallas kernels for 5% -> 7%
where the time goes in v1:
time: 186 us
  starting transfers between devices  90.7 us (49%)
  waiting for transfers between devices  46.9 us (25%)
  blocking collectives  26.4 us (14%)
  Pallas kernels  18.9 us (10%)
  local copies, waits for them, and re-layouts  2.57 us (1%)
    ppermute x15, starting transfers between devices, from_other_core(): return lax.ppermute(w, 'c', [(0, 1), (1, 0)])  45 us
    all_to_all x6, starting transfers between devices, exchange(): return lax.all_to_all(parts, axis, 0, 0, tiled=True)  28 us
    all_to_all x2, blocking collectives, exchange(): return lax.all_to_all(parts, axis, 0, 0, tiled=True)  26.4 us
    all_to_all x6, waiting for transfers between devices, exchange(): return lax.all_to_all(parts, axis, 0, 0, tiled=True)  24.5 us
    pallas_call x10, Pallas kernels, run(): pl.pallas_call(kernel, out_shape=out, in_specs=[vmem] * first + [lies] *...  18.9 us
    ppermute x3, waiting for transfers between devices, by_plane(): return lax.ppermute(a, ('y', 'z'), perm)  17.2 us
    ppermute x10, starting transfers between devices, along_y(): return lax.ppermute(a, 'y', [(i, (i + shift) % n) for i in range(n)])  11.9 us
    ppermute x3, starting transfers between devices, by_plane(): return lax.ppermute(a, ('y', 'z'), perm)  5.73 us
  transfers between devices with their start and end apart: 34, of which 10 were waited for; matrix products, arithmetic and copies ran while one was open for 0% of the time, Pallas kernels for 7%

profile of v1, /device:TPU:1, one launch (start us, length us, event | category | flops | bytes accessed | tf_op | source)
XLA Modules:
  0.0 185.7 jit_solution(4167624146541321008)
XLA Ops:
  0.0 3.2 %collective-permute-start = (bf16[256,1024]{1,0:T(8,128)(2,1)}, bf16[256,1024]{1,0:T(8,128)(2,1)S(1)}, u32[]{:S(2)}, u32[]{:S(2)}) collective-permute-start(bf16[256,1024]{1,0:T(8,128)(2,1)} %own.1), channel_id=1, source_target_pairs={{0,1},{1,0},{2,3},{3,2},{4,5},{5,4},{6,7},{7,6},{8,9},{9,8},{10,11... | collective-permute-start | bytes 1572872 | tf_op jit(solution)/shard_map/ppermute | solution.py:23
  8.7 5.2 %all-to-all-start = ((bf16[16,24,2176]{2,1,0:T(8,128)(2,1)}), bf16[16,24,2176]{2,1,0:T(8,128)(2,1)S(1)}, u32[]{:S(2)}, u32[]{:S(2)}) async-start(bf16[16,24,2176]{2,1,0:T(8,128)(2,1)} %bitcast.2), calls=%async_computation | async-start | bytes 3342336 | tf_op jit(solution)/shard_map/all_to_all | solution.py:19
  15.3 9.5 %collective-permute-done.1 = f32[104,128]{1,0:T(8,128)S(1)} collective-permute-done((f32[104,128]{1,0:T(8,128)S(1)}, f32[104,128]{1,0:T(8,128)S(1)}, u32[]{:S(2)}, u32[]{:S(2)}) %collective-permute-start.1) | collective-permute-done | bytes 53280 | tf_op jit(solution)/shard_map/ppermute | solution.py:34
  24.8 3.7 %collective-permute-start.2 = (f32[104,128]{1,0:T(8,128)S(1)}, f32[104,128]{1,0:T(8,128)S(1)}, u32[]{:S(2)}, u32[]{:S(2)}) collective-permute-start(f32[104,128]{1,0:T(8,128)S(1)} %collective-permute-done.1), channel_id=1, source_target_pairs={{0,192},{2,194},{4,4},{6,6},{8,8},{10,10},{12,12},{14,14},{64,0},{... | collective-permute-start | bytes 159752 | tf_op jit(solution)/shard_map/ppermute | solution.py:34
  28.5 7.7 %collective-permute-done.2.kept = f32[104,128]{1,0:T(8,128)S(1)} collective-permute-done((f32[104,128]{1,0:T(8,128)S(1)}, f32[104,128]{1,0:T(8,128)S(1)}, u32[]{:S(2)}, u32[]{:S(2)}) %collective-permute-start.2) | collective-permute-done | bytes 53280 | tf_op jit(solution)/shard_map/ppermute | solution.py:34
  39.1 5.7 %collective-permute-start.7 = (bf16[1024,256]{1,0:T(8,128)(2,1)S(1)}, bf16[1024,256]{1,0:T(8,128)(2,1)S(1)}, u32[]{:S(2)}, u32[]{:S(2)}) collective-permute-start(bf16[1024,256]{1,0:T(8,128)(2,1)S(1)} %copy-done.4), channel_id=1, source_target_pairs={{0,1},{1,0},{2,3},{3,2},{4,5},{5,4},{6,7},{7,6},{8,9},{9,8},{10,11... | collective-permute-start | bytes 1572872 | tf_op jit(solution)/shard_map/ppermute | solution.py:23
  44.8 3.7 %collective-permute-done.3.refs_1_ = bf16[1024,256]{1,0:T(8,128)(2,1)S(1)} collective-permute-done((bf16[1024,256]{1,0:T(8,128)(2,1)S(1)}, bf16[1024,256]{1,0:T(8,128)(2,1)S(1)}, u32[]{:S(2)}, u32[]{:S(2)}) %collective-permute-start.3) | collective-permute-done | bytes 524320 | tf_op jit(solution)/shard_map/ppermute | solution.py:28
  48.5 9.1 %collective-permute-start.8 = (bf16[1024,256]{1,0:T(8,128)(2,1)S(1)}, bf16[1024,256]{1,0:T(8,128)(2,1)S(1)}, u32[]{:S(2)}, u32[]{:S(2)}) collective-permute-start(bf16[1024,256]{1,0:T(8,128)(2,1)S(1)} %collective-permute-done.3.refs_1_), channel_id=1, source_target_pairs={{0,1},{1,0},{2,3},{3,2},{4,5},{5,4},{6,7},{7,6},{8,9},{9,8},{10,11... | collective-permute-start | bytes 1572872 | tf_op jit(solution)/shard_map/ppermute | solution.py:23
  60.5 6.5 %collective-permute-start.11 = (bf16[1024,256]{1,0:T(8,128)(2,1)S(1)}, bf16[1024,256]{1,0:T(8,128)(2,1)}, u32[]{:S(2)}, u32[]{:S(2)}) collective-permute-start(bf16[1024,256]{1,0:T(8,128)(2,1)S(1)} %collective-permute-done.5.refs_4_), channel_id=1, source_target_pairs={{0,1},{1,0},{2,3},{3,2},{4,5},{5,4},{6,7},{7,6},{8,9},{9,8},{10,11... | collective-permute-start | bytes 1572872 | tf_op jit(solution)/shard_map/ppermute | solution.py:23
  74.8 6.8 %all-to-all-start.1 = ((bf16[4,24,2048]{2,1,0:T(8,128)(2,1)}), bf16[4,24,2048]{2,1,0:T(8,128)(2,1)S(1)}, u32[]{:S(2)}, u32[]{:S(2)}) async-start(bf16[4,24,2048]{2,1,0:T(8,128)(2,1)} %shard_map.75), calls=%async_computation.1 | async-start | bytes 786432 | tf_op jit(solution)/shard_map/all_to_all | solution.py:19
  83.1 5.2 %all-to-all-done.1 = bf16[4,24,2048]{2,1,0:T(8,128)(2,1)S(1)} async-done(((bf16[4,24,2048]{2,1,0:T(8,128)(2,1)}), bf16[4,24,2048]{2,1,0:T(8,128)(2,1)S(1)}, u32[]{:S(2)}, u32[]{:S(2)}) %all-to-all-start.1) | async-done | bytes 393248 | tf_op jit(solution)/shard_map/all_to_all | solution.py:19
  88.3 4.3 %shard_map.76 = bf16[8,96,128]{2,1,0:T(8,128)(2,1)} custom-call(bf16[96,2048]{1,0:T(8,128)(2,1)S(1)} %bitcast.6, bf16[1024,256]{1,0:T(8,128)(2,1)} %refs_0_.2, bf16[1024,256]{1,0:T(8,128)(2,1)} %copy-done.2, bf16[512,256]{1,0:T(8,128)(2,1)} %collective-permute-done.4.refs_2_, bf16[512,256]{1,0:T(8,128)(2,1)} %collective-permute-done.6.refs_3_, ...), custom_call_target="tpu_custom_call" | custom-call | tf_op jit(solution)/shard_map/pallas_call | solution.py:45
  92.7 4.2 %all-to-all-start.2 = ((bf16[8,96,128]{2,1,0:T(8,128)(2,1)}), bf16[8,96,128]{2,1,0:T(8,128)(2,1)S(1)}, u32[]{:S(2)}, u32[]{:S(2)}) async-start(bf16[8,96,128]{2,1,0:T(8,128)(2,1)} %shard_map.76), calls=%async_computation.2 | async-start | bytes 393216 | tf_op jit(solution)/shard_map/all_to_all | solution.py:19
  106.3 4.9 %all-to-all-start.3 = ((bf16[8,104,128]{2,1,0:T(8,128)(2,1)}), bf16[8,104,128]{2,1,0:T(8,128)(2,1)S(1)}, u32[]{:S(2)}, u32[]{:S(2)}) async-start(bf16[8,104,128]{2,1,0:T(8,128)(2,1)} %get-tuple-element.17), calls=%async_computation.3 | async-start | bytes 425984 | tf_op jit(solution)/shard_map/all_to_all | solution.py:19
  111.2 8.8 %all-to-all-done.3.x = bf16[8,104,128]{2,1,0:T(8,128)(2,1)S(1)} async-done(((bf16[8,104,128]{2,1,0:T(8,128)(2,1)}), bf16[8,104,128]{2,1,0:T(8,128)(2,1)S(1)}, u32[]{:S(2)}, u32[]{:S(2)}) %all-to-all-start.3) | async-done | bytes 213024 | tf_op jit(solution)/shard_map/all_to_all | solution.py:19
  120.1 3.3 %shard_map.78 = bf16[96,2176]{1,0:T(8,128)(2,1)} custom-call(bf16[8,104,128]{2,1,0:T(8,128)(2,1)S(1)} %all-to-all-done.3.x, bf16[256,1024]{1,0:T(8,128)(2,1)} %refs_0_.3, bf16[256,1024]{1,0:T(8,128)(2,1)} %copy-done.6, bf16[256,1024]{1,0:T(8,128)(2,1)} %collective-permute-done.13.refs_2_, bf16[256,1024]{1,0:T(8,128)(2,1)} %collective-permute-done.14.refs_3_, ...), custom_call_target="tpu_custom_call" | custom-call | tf_op jit(solution)/shard_map/pallas_call | solution.py:45
  123.3 3.5 %all-to-all-start.4 = ((bf16[4,24,2176]{2,1,0:T(8,128)(2,1)}), bf16[4,24,2176]{2,1,0:T(8,128)(2,1)S(1)}, u32[]{:S(2)}, u32[]{:S(2)}) async-start(bf16[4,24,2176]{2,1,0:T(8,128)(2,1)} %bitcast.4), calls=%async_computation.4 | async-start | bytes 835584 | tf_op jit(solution)/shard_map/all_to_all | solution.py:19
  126.8 3.4 %collective-permute-start.22 = (bf16[1024,256]{1,0:T(8,128)(2,1)S(1)}, bf16[1024,256]{1,0:T(8,128)(2,1)}, u32[]{:S(2)}, u32[]{:S(2)}) collective-permute-start(bf16[1024,256]{1,0:T(8,128)(2,1)S(1)} %copy-done.5), channel_id=1, source_target_pairs={{0,1},{1,0},{2,3},{3,2},{4,5},{5,4},{6,7},{7,6},{8,9},{9,8},{10,11... | collective-permute-start | bytes 1572872 | tf_op jit(solution)/shard_map/ppermute | solution.py:23
  134.1 3.5 %all-to-all-start.5 = ((bf16[4,24,2048]{2,1,0:T(8,128)(2,1)}), bf16[4,24,2048]{2,1,0:T(8,128)(2,1)S(1)}, u32[]{:S(2)}, u32[]{:S(2)}) async-start(bf16[4,24,2048]{2,1,0:T(8,128)(2,1)} %shard_map.79), calls=%async_computation.5 | async-start | bytes 786432 | tf_op jit(solution)/shard_map/all_to_all | solution.py:19
  137.6 6.2 %all-to-all-done.5 = bf16[4,24,2048]{2,1,0:T(8,128)(2,1)S(1)} async-done(((bf16[4,24,2048]{2,1,0:T(8,128)(2,1)}), bf16[4,24,2048]{2,1,0:T(8,128)(2,1)S(1)}, u32[]{:S(2)}, u32[]{:S(2)}) %all-to-all-start.5) | async-done | bytes 393248 | tf_op jit(solution)/shard_map/all_to_all | solution.py:19
  143.7 3.6 %shard_map.80 = bf16[8,96,128]{2,1,0:T(8,128)(2,1)S(1)} custom-call(bf16[96,2048]{1,0:T(8,128)(2,1)S(1)} %bitcast.7, bf16[1024,256]{1,0:T(8,128)(2,1)} %refs_0_.4, bf16[1024,256]{1,0:T(8,128)(2,1)} %copy-done.8, bf16[1024,256]{1,0:T(8,128)(2,1)} %copy-done.9, bf16[1024,256]{1,0:T(8,128)(2,1)} %copy-done.10, ...), custom_call_target="tpu_custom_call" | custom-call | tf_op jit(solution)/shard_map/pallas_call | solution.py:45
  147.3 11.0 %all_to_all.40.parts = bf16[8,96,128]{2,1,0:T(8,128)(2,1)S(1)} all-to-all(bf16[8,96,128]{2,1,0:T(8,128)(2,1)S(1)} %shard_map.80), channel_id=1, replica_groups=mesh['y'=4,'x'=4,'z'=8,'c'=2] {'z'}, dimensions={0} | all-to-all | bytes 393216 | tf_op jit(solution)/shard_map/all_to_all | solution.py:19
  159.1 15.4 %all_to_all.41.own = bf16[8,96,128]{2,1,0:T(8,128)(2,1)S(1)} all-to-all(bf16[8,96,128]{2,1,0:T(8,128)(2,1)S(1)} %broadcast_in_dim.14), channel_id=1, replica_groups=mesh['y'=4,'x'=4,'z'=8,'c'=2] {'z'}, dimensions={0} | all-to-all | bytes 393216 | tf_op jit(solution)/shard_map/all_to_all | solution.py:19
  174.5 9.3 %collective-permute-start.27 = (bf16[8,96,128]{2,1,0:T(8,128)(2,1)S(1)}, bf16[8,96,128]{2,1,0:T(8,128)(2,1)S(1)}, u32[]{:S(2)}, u32[]{:S(2)}) collective-permute-start(bf16[8,96,128]{2,1,0:T(8,128)(2,1)S(1)} %all_to_all.41.own), channel_id=1, source_target_pairs={{0,1},{1,0},{2,3},{3,2},{4,5},{5,4},{6,7},{7,6},{8,9},{9,8},{10,11... | collective-permute-start | bytes 589832 | tf_op jit(solution)/shard_map/ppermute | solution.py:23
  (87 shorter events, 37.9 us)
Async XLA Ops:
  8.7 64.9 %all-to-all-start = ((bf16[16,24,2176]{2,1,0:T(8,128)(2,1)}), bf16[16,24,2176]{2,1,0:T(8,128)(2,1)S(1)}, u32[]{:S(2)}, u32[]{:S(2)}) async-start(bf16[16,24,2176]{2,1,0:T(8,128)(2,1)} %bitcast.2), calls=%async_computation | async-start | bytes 3342336 | tf_op jit(solution)/shard_map/all_to_all | solution.py:19
  13.9 10.9 %collective-permute-start.1 = (f32[104,128]{1,0:T(8,128)S(1)}, f32[104,128]{1,0:T(8,128)S(1)}, u32[]{:S(2)}, u32[]{:S(2)}) collective-permute-start(f32[104,128]{1,0:T(8,128)S(1)} %get-tuple-element.14), channel_id=1, source_target_pairs={{0,64},{2,66},{4,68},{6,70},{8,136},{10,138},{12,204},{14,206},{64... | collective-permute-start | bytes 159752 | tf_op jit(solution)/shard_map/ppermute | solution.py:34
  24.8 11.4 %collective-permute-start.2 = (f32[104,128]{1,0:T(8,128)S(1)}, f32[104,128]{1,0:T(8,128)S(1)}, u32[]{:S(2)}, u32[]{:S(2)}) collective-permute-start(f32[104,128]{1,0:T(8,128)S(1)} %collective-permute-done.1), channel_id=1, source_target_pairs={{0,192},{2,194},{4,4},{6,6},{8,8},{10,10},{12,12},{14,14},{64,0},{... | collective-permute-start | bytes 159752 | tf_op jit(solution)/shard_map/ppermute | solution.py:34
  36.2 12.3 %collective-permute-start.3 = (bf16[1024,256]{1,0:T(8,128)(2,1)S(1)}, bf16[1024,256]{1,0:T(8,128)(2,1)S(1)}, u32[]{:S(2)}, u32[]{:S(2)}) collective-permute-start(bf16[1024,256]{1,0:T(8,128)(2,1)S(1)} %copy-done.4), channel_id=1, source_target_pairs={{0,64},{64,128},{128,192},{192,0},{1,65},{65,129},{129,193},{193,1... | collective-permute-start | bytes 1572872 | tf_op jit(solution)/shard_map/ppermute | solution.py:28
  37.7 20.0 %collective-permute-start.5 = (bf16[1024,256]{1,0:T(8,128)(2,1)S(1)}, bf16[1024,256]{1,0:T(8,128)(2,1)S(1)}, u32[]{:S(2)}, u32[]{:S(2)}) collective-permute-start(bf16[1024,256]{1,0:T(8,128)(2,1)S(1)} %copy-done.4), channel_id=1, source_target_pairs={{0,192},{64,0},{128,64},{192,128},{1,193},{65,1},{129,65},{193,129... | collective-permute-start | bytes 1572872 | tf_op jit(solution)/shard_map/ppermute | solution.py:28
  38.8 21.6 %collective-permute-start.12 = (bf16[256,1024]{1,0:T(8,128)(2,1)}, bf16[256,1024]{1,0:T(8,128)(2,1)S(1)}, u32[]{:S(2)}, u32[]{:S(2)}) collective-permute-start(bf16[256,1024]{1,0:T(8,128)(2,1)} %refs_0_.3), channel_id=1, source_target_pairs={{0,64},{64,128},{128,192},{192,0},{1,65},{65,129},{129,193},{193,1... | collective-permute-start | bytes 1572872 | tf_op jit(solution)/shard_map/ppermute | solution.py:28
  39.1 31.1 %collective-permute-start.7 = (bf16[1024,256]{1,0:T(8,128)(2,1)S(1)}, bf16[1024,256]{1,0:T(8,128)(2,1)S(1)}, u32[]{:S(2)}, u32[]{:S(2)}) collective-permute-start(bf16[1024,256]{1,0:T(8,128)(2,1)S(1)} %copy-done.4), channel_id=1, source_target_pairs={{0,1},{1,0},{2,3},{3,2},{4,5},{5,4},{6,7},{7,6},{8,9},{9,8},{10,11... | collective-permute-start | bytes 1572872 | tf_op jit(solution)/shard_map/ppermute | solution.py:23
  48.5 22.2 %collective-permute-start.8 = (bf16[1024,256]{1,0:T(8,128)(2,1)S(1)}, bf16[1024,256]{1,0:T(8,128)(2,1)S(1)}, u32[]{:S(2)}, u32[]{:S(2)}) collective-permute-start(bf16[1024,256]{1,0:T(8,128)(2,1)S(1)} %collective-permute-done.3.refs_1_), channel_id=1, source_target_pairs={{0,1},{1,0},{2,3},{3,2},{4,5},{5,4},{6,7},{7,6},{8,9},{9,8},{10,11... | collective-permute-start | bytes 1572872 | tf_op jit(solution)/shard_map/ppermute | solution.py:23
  57.8 12.5 %collective-permute-start.6 = (bf16[512,256]{1,0:T(8,128)(2,1)S(1)}, bf16[512,256]{1,0:T(8,128)(2,1)}, u32[]{:S(2)}, u32[]{:S(2)}) collective-permute-start(bf16[512,256]{1,0:T(8,128)(2,1)S(1)} %slice.9), channel_id=1, source_target_pairs={{0,192},{64,0},{128,64},{192,128},{1,193},{65,1},{129,65},{193,129... | collective-permute-start | bytes 786440 | tf_op jit(solution)/shard_map/ppermute | solution.py:28
  60.5 22.6 %collective-permute-start.11 = (bf16[1024,256]{1,0:T(8,128)(2,1)S(1)}, bf16[1024,256]{1,0:T(8,128)(2,1)}, u32[]{:S(2)}, u32[]{:S(2)}) collective-permute-start(bf16[1024,256]{1,0:T(8,128)(2,1)S(1)} %collective-permute-done.5.refs_4_), channel_id=1, source_target_pairs={{0,1},{1,0},{2,3},{3,2},{4,5},{5,4},{6,7},{7,6},{8,9},{9,8},{10,11... | collective-permute-start | bytes 1572872 | tf_op jit(solution)/shard_map/ppermute | solution.py:23
  67.3 14.3 %collective-permute-start.9 = (bf16[512,256]{1,0:T(8,128)(2,1)}, bf16[512,256]{1,0:T(8,128)(2,1)}, u32[]{:S(2)}, u32[]{:S(2)}) collective-permute-start(bf16[512,256]{1,0:T(8,128)(2,1)} %collective-permute-done.4.refs_2_), channel_id=1, source_target_pairs={{0,1},{1,0},{2,3},{3,2},{4,5},{5,4},{6,7},{7,6},{8,9},{9,8},{10,11... | collective-permute-start | bytes 786440 | tf_op jit(solution)/shard_map/ppermute | solution.py:23
  70.2 12.6 %collective-permute-start.10 = (bf16[512,256]{1,0:T(8,128)(2,1)}, bf16[512,256]{1,0:T(8,128)(2,1)}, u32[]{:S(2)}, u32[]{:S(2)}) collective-permute-start(bf16[512,256]{1,0:T(8,128)(2,1)} %collective-permute-done.6.refs_3_), channel_id=1, source_target_pairs={{0,1},{1,0},{2,3},{3,2},{4,5},{5,4},{6,7},{7,6},{8,9},{9,8},{10,11... | collective-permute-start | bytes 786440 | tf_op jit(solution)/shard_map/ppermute | solution.py:23
  70.2 26.6 %collective-permute-start.13 = (bf16[256,1024]{1,0:T(8,128)(2,1)}, bf16[256,1024]{1,0:T(8,128)(2,1)}, u32[]{:S(2)}, u32[]{:S(2)}) collective-permute-start(bf16[256,1024]{1,0:T(8,128)(2,1)} %refs_0_.3), channel_id=1, source_target_pairs={{0,128},{64,192},{128,0},{192,64},{1,129},{65,193},{129,1},{193,65... | collective-permute-start | bytes 1572872 | tf_op jit(solution)/shard_map/ppermute | solution.py:28
  71.8 27.8 %collective-permute-start.14 = (bf16[256,1024]{1,0:T(8,128)(2,1)}, bf16[256,1024]{1,0:T(8,128)(2,1)}, u32[]{:S(2)}, u32[]{:S(2)}) collective-permute-start(bf16[256,1024]{1,0:T(8,128)(2,1)} %refs_0_.3), channel_id=1, source_target_pairs={{0,192},{64,0},{128,64},{192,128},{1,193},{65,1},{129,65},{193,129... | collective-permute-start | bytes 1572872 | tf_op jit(solution)/shard_map/ppermute | solution.py:28
  74.8 13.5 %all-to-all-start.1 = ((bf16[4,24,2048]{2,1,0:T(8,128)(2,1)}), bf16[4,24,2048]{2,1,0:T(8,128)(2,1)S(1)}, u32[]{:S(2)}, u32[]{:S(2)}) async-start(bf16[4,24,2048]{2,1,0:T(8,128)(2,1)} %shard_map.75), calls=%async_computation.1 | async-start | bytes 786432 | tf_op jit(solution)/shard_map/all_to_all | solution.py:19
  81.6 19.1 %collective-permute-start.15 = (bf16[256,1024]{1,0:T(8,128)(2,1)}, bf16[256,1024]{1,0:T(8,128)(2,1)}, u32[]{:S(2)}, u32[]{:S(2)}) collective-permute-start(bf16[256,1024]{1,0:T(8,128)(2,1)} %refs_0_.3), channel_id=1, source_target_pairs={{0,1},{1,0},{2,3},{3,2},{4,5},{5,4},{6,7},{7,6},{8,9},{9,8},{10,11... | collective-permute-start | bytes 1572872 | tf_op jit(solution)/shard_map/ppermute | solution.py:23
  82.8 20.2 %collective-permute-start.16 = (bf16[256,1024]{1,0:T(8,128)(2,1)S(1)}, bf16[256,1024]{1,0:T(8,128)(2,1)}, u32[]{:S(2)}, u32[]{:S(2)}) collective-permute-start(bf16[256,1024]{1,0:T(8,128)(2,1)S(1)} %copy-done.7), channel_id=1, source_target_pairs={{0,1},{1,0},{2,3},{3,2},{4,5},{5,4},{6,7},{7,6},{8,9},{9,8},{10,11... | collective-permute-start | bytes 1572872 | tf_op jit(solution)/shard_map/ppermute | solution.py:23
  92.7 12.9 %all-to-all-start.2 = ((bf16[8,96,128]{2,1,0:T(8,128)(2,1)}), bf16[8,96,128]{2,1,0:T(8,128)(2,1)S(1)}, u32[]{:S(2)}, u32[]{:S(2)}) async-start(bf16[8,96,128]{2,1,0:T(8,128)(2,1)} %shard_map.76), calls=%async_computation.2 | async-start | bytes 393216 | tf_op jit(solution)/shard_map/all_to_all | solution.py:19
  96.9 14.3 %collective-permute-start.17 = (bf16[256,1024]{1,0:T(8,128)(2,1)}, bf16[256,1024]{1,0:T(8,128)(2,1)S(1)}, u32[]{:S(2)}, u32[]{:S(2)}) collective-permute-start(bf16[256,1024]{1,0:T(8,128)(2,1)} %collective-permute-done.13.refs_2_), channel_id=1, source_target_pairs={{0,1},{1,0},{2,3},{3,2},{4,5},{5,4},{6,7},{7,6},{8,9},{9,8},{10,11... | collective-permute-start | bytes 1572872 | tf_op jit(solution)/shard_map/ppermute | solution.py:23
  99.6 11.6 %collective-permute-start.18 = (bf16[256,1024]{1,0:T(8,128)(2,1)}, bf16[256,1024]{1,0:T(8,128)(2,1)}, u32[]{:S(2)}, u32[]{:S(2)}) collective-permute-start(bf16[256,1024]{1,0:T(8,128)(2,1)} %collective-permute-done.14.refs_3_), channel_id=1, source_target_pairs={{0,1},{1,0},{2,3},{3,2},{4,5},{5,4},{6,7},{7,6},{8,9},{9,8},{10,11... | collective-permute-start | bytes 1572872 | tf_op jit(solution)/shard_map/ppermute | solution.py:23
  99.8 30.4 %collective-permute-start.19 = (bf16[1024,256]{1,0:T(8,128)(2,1)S(1)}, bf16[1024,256]{1,0:T(8,128)(2,1)S(1)}, u32[]{:S(2)}, u32[]{:S(2)}) collective-permute-start(bf16[1024,256]{1,0:T(8,128)(2,1)S(1)} %copy-done.5), channel_id=1, source_target_pairs={{0,64},{64,128},{128,192},{192,0},{1,65},{65,129},{129,193},{193,1... | collective-permute-start | bytes 1572872 | tf_op jit(solution)/shard_map/ppermute | solution.py:28
  100.7 29.6 %collective-permute-start.20 = (bf16[1024,256]{1,0:T(8,128)(2,1)S(1)}, bf16[1024,256]{1,0:T(8,128)(2,1)S(1)}, u32[]{:S(2)}, u32[]{:S(2)}) collective-permute-start(bf16[1024,256]{1,0:T(8,128)(2,1)S(1)} %copy-done.5), channel_id=1, source_target_pairs={{0,128},{64,192},{128,0},{192,64},{1,129},{65,193},{129,1},{193,65... | collective-permute-start | bytes 1572872 | tf_op jit(solution)/shard_map/ppermute | solution.py:28
  103.0 27.7 %collective-permute-start.21 = (bf16[1024,256]{1,0:T(8,128)(2,1)S(1)}, bf16[1024,256]{1,0:T(8,128)(2,1)S(1)}, u32[]{:S(2)}, u32[]{:S(2)}) collective-permute-start(bf16[1024,256]{1,0:T(8,128)(2,1)S(1)} %copy-done.5), channel_id=1, source_target_pairs={{0,192},{64,0},{128,64},{192,128},{1,193},{65,1},{129,65},{193,129... | collective-permute-start | bytes 1572872 | tf_op jit(solution)/shard_map/ppermute | solution.py:28
  106.3 13.7 %all-to-all-start.3 = ((bf16[8,104,128]{2,1,0:T(8,128)(2,1)}), bf16[8,104,128]{2,1,0:T(8,128)(2,1)S(1)}, u32[]{:S(2)}, u32[]{:S(2)}) async-start(bf16[8,104,128]{2,1,0:T(8,128)(2,1)} %get-tuple-element.17), calls=%async_computation.3 | async-start | bytes 425984 | tf_op jit(solution)/shard_map/all_to_all | solution.py:19
  (24 other events, 233.2 us)

commit v2 on v1

--- a/solution.py
+++ b/solution.py
@@ -231,14 +231,14 @@
     return lax.optimization_barrier((w, done))
 
 
-def around(w, forward=False):
+def around(w, swapped, forward=False):
     n = lax.axis_size("y")
     own = [w] + [along_y(w, d) for d in range(1, n) if not (forward and d == n // 2)]
     if forward:
         half = w.shape[0] // 2
         far = [along_y(own[1][:half], 1), along_y(own[-1][half:], n - 1)]
         own[n // 2 : n // 2] = far
-    return own + [from_other_core(v) for v in own]
+    return own + [swapped] + [from_other_core(v) for v in own[1:]]
 
 
 def body(tokens, gain_first, up_first, down_first, gain_second, up_second, down_second):
@@ -272,17 +272,21 @@
         update=2,
     )(scaled, from_other_core(up_first), payload)
     parts = exchange(payload.reshape(ny * nx, few, wide), RA)
-    kept = by_plane(kept, lambda z: max(z // 2, 1))
-    kept = by_plane(kept, lambda z: -1 if z < 2 else 0)
-    down_first, kept = after(down_first, kept)
-    downs = around(down_first, forward=True)
+    kept = by_plane(kept, lambda z: z // 2)
+    swapped, order = [], payload
+    for w in (down_second, up_second, down_first):
+        w, order = after(w, order)
+        order = from_other_core(w)
+        swapped.append(order)
+    down_first, order = after(down_first, order)
+    downs = around(down_first, order, forward=True)
     hidden = activate(parts)
 
     hidden = exchange(hidden, "x").reshape(per_y, hid)
-    ups = around(up_second)
+    ups = around(up_second, swapped[1])
     branch = call(down_kernel, sds((nz, per_y, LANES)), held(down_first, 2), whole=1)(hidden, *downs)
     branch = exchange(branch, "z")
-    downs = around(down_second)
+    downs = around(down_second, swapped[0])
     middle, payload = call(finish_first_kernel, (sds((per_y, LANES)), sds((nz, per_y + 8, LANES))))(
         branch, kept
     )

time: 186 us -> 191 us (1.027)
  waiting for transfers between devices: 46.9 us -> 72.7 us
  starting transfers between devices: 90.7 us -> 69.5 us
    ppermute x10, waiting for transfers between devices: 4.07 us -> 43.4 us  [along_y(): return lax.ppermute(a, 'y', [(i, (i + shift) % n) for i in range(n)])]
    ppermute x15, starting transfers between devices: 45 us -> 23.1 us  [from_other_core(): return lax.ppermute(w, 'c', [(0, 1), (1, 0)])]
    ppermute x3 -> x2, waiting for transfers between devices: 17.2 us -> 0.01 us  [by_plane(): return lax.ppermute(a, ('y', 'z'), perm)]
    all_to_all x6, starting transfers between devices: 28 us -> 34.4 us  [exchange(): return lax.all_to_all(parts, axis, 0, 0, tiled=True)]
    ppermute x3 -> x2, starting transfers between devices: 5.73 us -> 1.31 us  [by_plane(): return lax.ppermute(a, ('y', 'z'), perm)]
    ppermute x15, waiting for transfers between devices: 1.11 us -> 4.77 us  [from_other_core(): return lax.ppermute(w, 'c', [(0, 1), (1, 0)])]
  transfers between devices with their start and end apart: 34 -> 33, of which waited for: 10 -> 10; matrix products, arithmetic and copies ran while one was open for 0% -> 0% of each run, Pallas kernels for 7% -> 7%
where the time goes in v2:
time: 191 us
  waiting for transfers between devices  72.7 us (38%)
  starting transfers between devices  69.5 us (36%)
  blocking collectives  26.4 us (14%)
  Pallas kernels  18.9 us (10%)
  local copies, waits for them, and re-layouts  2.9 us (2%)
    ppermute x10, waiting for transfers between devices, along_y(): return lax.ppermute(a, 'y', [(i, (i + shift) % n) for i in range(n)])  43.4 us
    all_to_all x6, starting transfers between devices, exchange(): return lax.all_to_all(parts, axis, 0, 0, tiled=True)  34.4 us
    all_to_all x2, blocking collectives, exchange(): return lax.all_to_all(parts, axis, 0, 0, tiled=True)  26.4 us
    all_to_all x6, waiting for transfers between devices, exchange(): return lax.all_to_all(parts, axis, 0, 0, tiled=True)  24.5 us
    ppermute x15, starting transfers between devices, from_other_core(): return lax.ppermute(w, 'c', [(0, 1), (1, 0)])  23.1 us
    pallas_call x10, Pallas kernels, run(): pl.pallas_call(kernel, out_shape=out, in_specs=[vmem] * first + [lies] *...  18.9 us
    ppermute x10, starting transfers between devices, along_y(): return lax.ppermute(a, 'y', [(i, (i + shift) % n) for i in range(n)])  10.7 us
    ppermute x15, waiting for transfers between devices, from_other_core(): return lax.ppermute(w, 'c', [(0, 1), (1, 0)])  4.77 us
  transfers between devices with their start and end apart: 33, of which 10 were waited for; matrix products, arithmetic and copies ran while one was open for 0% of the time, Pallas kernels for 7%

profile of v2, /device:TPU:1, one launch (start us, length us, event | category | flops | bytes accessed | tf_op | source)
XLA Modules:
  0.0 190.7 jit_solution(11822293247212441681)
XLA Ops:
  0.0 3.2 %collective-permute-start = (bf16[256,1024]{1,0:T(8,128)(2,1)}, bf16[256,1024]{1,0:T(8,128)(2,1)S(1)}, u32[]{:S(2)}, u32[]{:S(2)}) collective-permute-start(bf16[256,1024]{1,0:T(8,128)(2,1)} %own.1), channel_id=1, source_target_pairs={{0,1},{1,0},{2,3},{3,2},{4,5},{5,4},{6,7},{7,6},{8,9},{9,8},{10,11... | collective-permute-start | bytes 1572872 | tf_op jit(solution)/shard_map/ppermute | solution.py:23
  4.6 2.8 %shard_map.73 = (bf16[384,2176]{1,0:T(8,128)(2,1)}, bf16[384,256]{1,0:T(8,128)(2,1)S(1)}, f32[104,128]{1,0:T(8,128)S(1)}) custom-call(f32[1,256]{1,0:T(1,128)S(1)} %bitcast.8, f32[1,256]{1,0:T(1,128)S(1)} %bitcast.9, bf16[768,256]{1,0:T(8,128)(2,1)} %tokens.1, bf16[256,1024]{1,0:T(8,128)(2,1)} %own.1), custom_call_target="tpu_custom_call" | custom-call | tf_op jit(solution)/shard_map/pallas_call | solution.py:45
  13.5 5.0 %all-to-all-start = ((bf16[16,24,2176]{2,1,0:T(8,128)(2,1)}), bf16[16,24,2176]{2,1,0:T(8,128)(2,1)S(1)}, u32[]{:S(2)}, u32[]{:S(2)}) async-start(bf16[16,24,2176]{2,1,0:T(8,128)(2,1)} %bitcast.2), calls=%async_computation | async-start | bytes 3342336 | tf_op jit(solution)/shard_map/all_to_all | solution.py:19
  21.5 29.4 %collective-permute-done.4.refs_1_ = bf16[1024,256]{1,0:T(8,128)(2,1)S(1)} collective-permute-done((bf16[1024,256]{1,0:T(8,128)(2,1)S(1)}, bf16[1024,256]{1,0:T(8,128)(2,1)S(1)}, u32[]{:S(2)}, u32[]{:S(2)}) %collective-permute-start.4) | collective-permute-done | bytes 524320 | tf_op jit(solution)/shard_map/ppermute | solution.py:28
  51.0 2.7 %collective-permute-start.7 = (bf16[512,256]{1,0:T(8,128)(2,1)S(1)}, bf16[512,256]{1,0:T(8,128)(2,1)}, u32[]{:S(2)}, u32[]{:S(2)}) collective-permute-start(bf16[512,256]{1,0:T(8,128)(2,1)S(1)} %slice.9), channel_id=1, source_target_pairs={{0,192},{64,0},{128,64},{192,128},{1,193},{65,1},{129,65},{193,129... | collective-permute-start | bytes 786440 | tf_op jit(solution)/shard_map/ppermute | solution.py:28
  53.7 14.0 %collective-permute-done.5.refs_2_ = bf16[512,256]{1,0:T(8,128)(2,1)S(1)} collective-permute-done((bf16[512,256]{1,0:T(8,128)(2,1)S(1)}, bf16[512,256]{1,0:T(8,128)(2,1)S(1)}, u32[]{:S(2)}, u32[]{:S(2)}) %collective-permute-start.5) | collective-permute-done | bytes 262176 | tf_op jit(solution)/shard_map/ppermute | solution.py:28
  72.7 4.1 %all-to-all-start.1 = ((bf16[4,24,2048]{2,1,0:T(8,128)(2,1)}), bf16[4,24,2048]{2,1,0:T(8,128)(2,1)S(1)}, u32[]{:S(2)}, u32[]{:S(2)}) async-start(bf16[4,24,2048]{2,1,0:T(8,128)(2,1)} %shard_map.75), calls=%async_computation.1 | async-start | bytes 786432 | tf_op jit(solution)/shard_map/all_to_all | solution.py:19
  78.3 5.5 %all-to-all-done.1 = bf16[4,24,2048]{2,1,0:T(8,128)(2,1)S(1)} async-done(((bf16[4,24,2048]{2,1,0:T(8,128)(2,1)}), bf16[4,24,2048]{2,1,0:T(8,128)(2,1)S(1)}, u32[]{:S(2)}, u32[]{:S(2)}) %all-to-all-start.1) | async-done | bytes 393248 | tf_op jit(solution)/shard_map/all_to_all | solution.py:19
  83.8 4.3 %shard_map.76 = bf16[8,96,128]{2,1,0:T(8,128)(2,1)} custom-call(bf16[96,2048]{1,0:T(8,128)(2,1)S(1)} %bitcast.6, bf16[1024,256]{1,0:T(8,128)(2,1)} %refs_0_.2, bf16[1024,256]{1,0:T(8,128)(2,1)} %copy-done.2, bf16[512,256]{1,0:T(8,128)(2,1)} %copy-done.18, bf16[512,256]{1,0:T(8,128)(2,1)} %collective-permute-done.7.refs_3_, bf16[1024,256]{1,0:T(8,128)(2,1)} %copy-done.3, ...), custom_call_target="tpu_custom_call" | custom-call | tf_op jit(solution)/shard_map/pallas_call | solution.py:45
  88.2 8.2 %all-to-all-start.2 = ((bf16[8,96,128]{2,1,0:T(8,128)(2,1)}), bf16[8,96,128]{2,1,0:T(8,128)(2,1)S(1)}, u32[]{:S(2)}, u32[]{:S(2)}) async-start(bf16[8,96,128]{2,1,0:T(8,128)(2,1)} %shard_map.76), calls=%async_computation.2 | async-start | bytes 393216 | tf_op jit(solution)/shard_map/all_to_all | solution.py:19
  96.4 2.4 %collective-permute-start.17 = (bf16[256,1024]{1,0:T(8,128)(2,1)}, bf16[256,1024]{1,0:T(8,128)(2,1)}, u32[]{:S(2)}, u32[]{:S(2)}) collective-permute-start(bf16[256,1024]{1,0:T(8,128)(2,1)} %collective-permute-done.14.refs_2_), channel_id=1, source_target_pairs={{0,1},{1,0},{2,3},{3,2},{4,5},{5,4},{6,7},{7,6},{8,9},{9,8},{10,11... | collective-permute-start | bytes 1572872 | tf_op jit(solution)/shard_map/ppermute | solution.py:23
  100.4 2.3 %collective-permute-start.20 = (bf16[1024,256]{1,0:T(8,128)(2,1)S(1)}, bf16[1024,256]{1,0:T(8,128)(2,1)S(1)}, u32[]{:S(2)}, u32[]{:S(2)}) collective-permute-start(bf16[1024,256]{1,0:T(8,128)(2,1)S(1)} %copy-done.7), channel_id=1, source_target_pairs={{0,128},{64,192},{128,0},{192,64},{1,129},{65,193},{129,1},{193,65... | collective-permute-start | bytes 1572872 | tf_op jit(solution)/shard_map/ppermute | solution.py:28
  105.9 10.1 %all-to-all-start.3 = ((bf16[8,104,128]{2,1,0:T(8,128)(2,1)}), bf16[8,104,128]{2,1,0:T(8,128)(2,1)S(1)}, u32[]{:S(2)}, u32[]{:S(2)}) async-start(bf16[8,104,128]{2,1,0:T(8,128)(2,1)} %get-tuple-element.23), calls=%async_computation.3 | async-start | bytes 425984 | tf_op jit(solution)/shard_map/all_to_all | solution.py:19
  116.0 8.8 %all-to-all-done.3.x = bf16[8,104,128]{2,1,0:T(8,128)(2,1)S(1)} async-done(((bf16[8,104,128]{2,1,0:T(8,128)(2,1)}), bf16[8,104,128]{2,1,0:T(8,128)(2,1)S(1)}, u32[]{:S(2)}, u32[]{:S(2)}) %all-to-all-start.3) | async-done | bytes 213024 | tf_op jit(solution)/shard_map/all_to_all | solution.py:19
  124.8 3.3 %shard_map.78 = bf16[96,2176]{1,0:T(8,128)(2,1)} custom-call(bf16[8,104,128]{2,1,0:T(8,128)(2,1)S(1)} %all-to-all-done.3.x, bf16[256,1024]{1,0:T(8,128)(2,1)} %refs_0_.3, bf16[256,1024]{1,0:T(8,128)(2,1)} %copy-done.10, bf16[256,1024]{1,0:T(8,128)(2,1)} %collective-permute-done.14.refs_2_, bf16[256,1024]{1,0:T(8,128)(2,1)} %collective-permute-done.15.refs_3_, ...), custom_call_target="tpu_custom_call" | custom-call | tf_op jit(solution)/shard_map/pallas_call | solution.py:45
  128.1 3.5 %all-to-all-start.4 = ((bf16[4,24,2176]{2,1,0:T(8,128)(2,1)}), bf16[4,24,2176]{2,1,0:T(8,128)(2,1)S(1)}, u32[]{:S(2)}, u32[]{:S(2)}) async-start(bf16[4,24,2176]{2,1,0:T(8,128)(2,1)} %bitcast.4), calls=%async_computation.4 | async-start | bytes 835584 | tf_op jit(solution)/shard_map/all_to_all | solution.py:19
  131.6 3.6 %collective-permute-start.22 = (bf16[1024,256]{1,0:T(8,128)(2,1)S(1)}, bf16[1024,256]{1,0:T(8,128)(2,1)S(1)}, u32[]{:S(2)}, u32[]{:S(2)}) collective-permute-start(bf16[1024,256]{1,0:T(8,128)(2,1)S(1)} %collective-permute-done.19.refs_1_), channel_id=1, source_target_pairs={{0,1},{1,0},{2,3},{3,2},{4,5},{5,4},{6,7},{7,6},{8,9},{9,8},{10,11... | collective-permute-start | bytes 1572872 | tf_op jit(solution)/shard_map/ppermute | solution.py:23
  135.7 2.2 %all-to-all-done.4.parts = bf16[4,24,2176]{2,1,0:T(8,128)(2,1)S(1)} async-done(((bf16[4,24,2176]{2,1,0:T(8,128)(2,1)}), bf16[4,24,2176]{2,1,0:T(8,128)(2,1)S(1)}, u32[]{:S(2)}, u32[]{:S(2)}) %all-to-all-start.4) | async-done | bytes 417824 | tf_op jit(solution)/shard_map/all_to_all | solution.py:19
  138.8 3.5 %all-to-all-start.5 = ((bf16[4,24,2048]{2,1,0:T(8,128)(2,1)}), bf16[4,24,2048]{2,1,0:T(8,128)(2,1)S(1)}, u32[]{:S(2)}, u32[]{:S(2)}) async-start(bf16[4,24,2048]{2,1,0:T(8,128)(2,1)} %shard_map.79), calls=%async_computation.5 | async-start | bytes 786432 | tf_op jit(solution)/shard_map/all_to_all | solution.py:19
  142.3 6.1 %all-to-all-done.5 = bf16[4,24,2048]{2,1,0:T(8,128)(2,1)S(1)} async-done(((bf16[4,24,2048]{2,1,0:T(8,128)(2,1)}), bf16[4,24,2048]{2,1,0:T(8,128)(2,1)S(1)}, u32[]{:S(2)}, u32[]{:S(2)}) %all-to-all-start.5) | async-done | bytes 393248 | tf_op jit(solution)/shard_map/all_to_all | solution.py:19
  148.5 3.6 %shard_map.80 = bf16[8,96,128]{2,1,0:T(8,128)(2,1)S(1)} custom-call(bf16[96,2048]{1,0:T(8,128)(2,1)S(1)} %bitcast.7, bf16[1024,256]{1,0:T(8,128)(2,1)} %refs_0_.4, bf16[1024,256]{1,0:T(8,128)(2,1)} %copy-done.12, bf16[1024,256]{1,0:T(8,128)(2,1)} %copy-done.13, bf16[1024,256]{1,0:T(8,128)(2,1)} %copy-done.15, bf16[1024,256]{1,0:T(8,128)(2,1)} %copy-done.8, ...), custom_call_target="tpu_custom_call" | custom-call | tf_op jit(solution)/shard_map/pallas_call | solution.py:45
  152.1 11.0 %all_to_all.40.parts = bf16[8,96,128]{2,1,0:T(8,128)(2,1)S(1)} all-to-all(bf16[8,96,128]{2,1,0:T(8,128)(2,1)S(1)} %shard_map.80), channel_id=1, replica_groups=mesh['y'=4,'x'=4,'z'=8,'c'=2] {'z'}, dimensions={0} | all-to-all | bytes 393216 | tf_op jit(solution)/shard_map/all_to_all | solution.py:19
  163.9 15.4 %all_to_all.41.own = bf16[8,96,128]{2,1,0:T(8,128)(2,1)S(1)} all-to-all(bf16[8,96,128]{2,1,0:T(8,128)(2,1)S(1)} %broadcast_in_dim.14), channel_id=1, replica_groups=mesh['y'=4,'x'=4,'z'=8,'c'=2] {'z'}, dimensions={0} | all-to-all | bytes 393216 | tf_op jit(solution)/shard_map/all_to_all | solution.py:19
  179.3 9.5 %collective-permute-start.26 = (bf16[8,96,128]{2,1,0:T(8,128)(2,1)S(1)}, bf16[8,96,128]{2,1,0:T(8,128)(2,1)S(1)}, u32[]{:S(2)}, u32[]{:S(2)}) collective-permute-start(bf16[8,96,128]{2,1,0:T(8,128)(2,1)S(1)} %all_to_all.41.own), channel_id=1, source_target_pairs={{0,1},{1,0},{2,3},{3,2},{4,5},{5,4},{6,7},{7,6},{8,9},{9,8},{10,11... | collective-permute-start | bytes 589832 | tf_op jit(solution)/shard_map/ppermute | solution.py:23
  (97 shorter events, 26.0 us)
Async XLA Ops:
  13.5 58.1 %all-to-all-start = ((bf16[16,24,2176]{2,1,0:T(8,128)(2,1)}), bf16[16,24,2176]{2,1,0:T(8,128)(2,1)S(1)}, u32[]{:S(2)}, u32[]{:S(2)}) async-start(bf16[16,24,2176]{2,1,0:T(8,128)(2,1)} %bitcast.2), calls=%async_computation | async-start | bytes 3342336 | tf_op jit(solution)/shard_map/all_to_all | solution.py:19
  18.5 32.3 %collective-permute-start.4 = (bf16[1024,256]{1,0:T(8,128)(2,1)S(1)}, bf16[1024,256]{1,0:T(8,128)(2,1)S(1)}, u32[]{:S(2)}, u32[]{:S(2)}) collective-permute-start(bf16[1024,256]{1,0:T(8,128)(2,1)S(1)} %copy-done.4), channel_id=1, source_target_pairs={{0,64},{64,128},{128,192},{192,0},{1,65},{65,129},{129,193},{193,1... | collective-permute-start | bytes 1572872 | tf_op jit(solution)/shard_map/ppermute | solution.py:28
  20.0 31.0 %collective-permute-start.6 = (bf16[1024,256]{1,0:T(8,128)(2,1)S(1)}, bf16[1024,256]{1,0:T(8,128)(2,1)S(1)}, u32[]{:S(2)}, u32[]{:S(2)}) collective-permute-start(bf16[1024,256]{1,0:T(8,128)(2,1)S(1)} %copy-done.4), channel_id=1, source_target_pairs={{0,192},{64,0},{128,64},{192,128},{1,193},{65,1},{129,65},{193,129... | collective-permute-start | bytes 1572872 | tf_op jit(solution)/shard_map/ppermute | solution.py:28
  21.3 48.2 %collective-permute-start.13 = (bf16[256,1024]{1,0:T(8,128)(2,1)}, bf16[256,1024]{1,0:T(8,128)(2,1)S(1)}, u32[]{:S(2)}, u32[]{:S(2)}) collective-permute-start(bf16[256,1024]{1,0:T(8,128)(2,1)} %refs_0_.3), channel_id=1, source_target_pairs={{0,64},{64,128},{128,192},{192,0},{1,65},{65,129},{129,193},{193,1... | collective-permute-start | bytes 1572872 | tf_op jit(solution)/shard_map/ppermute | solution.py:28
  50.9 16.8 %collective-permute-start.5 = (bf16[512,256]{1,0:T(8,128)(2,1)S(1)}, bf16[512,256]{1,0:T(8,128)(2,1)S(1)}, u32[]{:S(2)}, u32[]{:S(2)}) collective-permute-start(bf16[512,256]{1,0:T(8,128)(2,1)S(1)} %slice.8), channel_id=1, source_target_pairs={{0,64},{64,128},{128,192},{192,0},{1,65},{65,129},{129,193},{193,1... | collective-permute-start | bytes 786440 | tf_op jit(solution)/shard_map/ppermute | solution.py:28
  51.0 18.5 %collective-permute-start.7 = (bf16[512,256]{1,0:T(8,128)(2,1)S(1)}, bf16[512,256]{1,0:T(8,128)(2,1)}, u32[]{:S(2)}, u32[]{:S(2)}) collective-permute-start(bf16[512,256]{1,0:T(8,128)(2,1)S(1)} %slice.9), channel_id=1, source_target_pairs={{0,192},{64,0},{128,64},{192,128},{1,193},{65,1},{129,65},{193,129... | collective-permute-start | bytes 786440 | tf_op jit(solution)/shard_map/ppermute | solution.py:28
  69.0 14.9 %collective-permute-start.8 = (bf16[1024,256]{1,0:T(8,128)(2,1)S(1)}, bf16[1024,256]{1,0:T(8,128)(2,1)}, u32[]{:S(2)}, u32[]{:S(2)}) collective-permute-start(bf16[1024,256]{1,0:T(8,128)(2,1)S(1)} %collective-permute-done.4.refs_1_), channel_id=1, source_target_pairs={{0,1},{1,0},{2,3},{3,2},{4,5},{5,4},{6,7},{7,6},{8,9},{9,8},{10,11... | collective-permute-start | bytes 1572872 | tf_op jit(solution)/shard_map/ppermute | solution.py:23
  69.0 14.9 %collective-permute-start.11 = (bf16[1024,256]{1,0:T(8,128)(2,1)S(1)}, bf16[1024,256]{1,0:T(8,128)(2,1)}, u32[]{:S(2)}, u32[]{:S(2)}) collective-permute-start(bf16[1024,256]{1,0:T(8,128)(2,1)S(1)} %collective-permute-done.6.refs_4_), channel_id=1, source_target_pairs={{0,1},{1,0},{2,3},{3,2},{4,5},{5,4},{6,7},{7,6},{8,9},{9,8},{10,11... | collective-permute-start | bytes 1572872 | tf_op jit(solution)/shard_map/ppermute | solution.py:23
  69.5 7.3 %collective-permute-start.10 = (bf16[512,256]{1,0:T(8,128)(2,1)}, bf16[512,256]{1,0:T(8,128)(2,1)}, u32[]{:S(2)}, u32[]{:S(2)}) collective-permute-start(bf16[512,256]{1,0:T(8,128)(2,1)} %collective-permute-done.7.refs_3_), channel_id=1, source_target_pairs={{0,1},{1,0},{2,3},{3,2},{4,5},{5,4},{6,7},{7,6},{8,9},{9,8},{10,11... | collective-permute-start | bytes 786440 | tf_op jit(solution)/shard_map/ppermute | solution.py:23
  69.5 26.9 %collective-permute-start.14 = (bf16[256,1024]{1,0:T(8,128)(2,1)}, bf16[256,1024]{1,0:T(8,128)(2,1)}, u32[]{:S(2)}, u32[]{:S(2)}) collective-permute-start(bf16[256,1024]{1,0:T(8,128)(2,1)} %refs_0_.3), channel_id=1, source_target_pairs={{0,128},{64,192},{128,0},{192,64},{1,129},{65,193},{129,1},{193,65... | collective-permute-start | bytes 1572872 | tf_op jit(solution)/shard_map/ppermute | solution.py:28
  71.0 27.8 %collective-permute-start.15 = (bf16[256,1024]{1,0:T(8,128)(2,1)}, bf16[256,1024]{1,0:T(8,128)(2,1)}, u32[]{:S(2)}, u32[]{:S(2)}) collective-permute-start(bf16[256,1024]{1,0:T(8,128)(2,1)} %refs_0_.3), channel_id=1, source_target_pairs={{0,192},{64,0},{128,64},{192,128},{1,193},{65,1},{129,65},{193,129... | collective-permute-start | bytes 1572872 | tf_op jit(solution)/shard_map/ppermute | solution.py:28
  72.7 11.1 %all-to-all-start.1 = ((bf16[4,24,2048]{2,1,0:T(8,128)(2,1)}), bf16[4,24,2048]{2,1,0:T(8,128)(2,1)S(1)}, u32[]{:S(2)}, u32[]{:S(2)}) async-start(bf16[4,24,2048]{2,1,0:T(8,128)(2,1)} %shard_map.75), calls=%async_computation.1 | async-start | bytes 786432 | tf_op jit(solution)/shard_map/all_to_all | solution.py:19
  76.8 25.8 %collective-permute-start.16 = (bf16[256,1024]{1,0:T(8,128)(2,1)S(1)}, bf16[256,1024]{1,0:T(8,128)(2,1)S(1)}, u32[]{:S(2)}, u32[]{:S(2)}) collective-permute-start(bf16[256,1024]{1,0:T(8,128)(2,1)S(1)} %copy-done.11), channel_id=1, source_target_pairs={{0,1},{1,0},{2,3},{3,2},{4,5},{5,4},{6,7},{7,6},{8,9},{9,8},{10,11... | collective-permute-start | bytes 1572872 | tf_op jit(solution)/shard_map/ppermute | solution.py:23
  88.2 17.0 %all-to-all-start.2 = ((bf16[8,96,128]{2,1,0:T(8,128)(2,1)}), bf16[8,96,128]{2,1,0:T(8,128)(2,1)S(1)}, u32[]{:S(2)}, u32[]{:S(2)}) async-start(bf16[8,96,128]{2,1,0:T(8,128)(2,1)} %shard_map.76), calls=%async_computation.2 | async-start | bytes 393216 | tf_op jit(solution)/shard_map/all_to_all | solution.py:19
  96.4 19.6 %collective-permute-start.17 = (bf16[256,1024]{1,0:T(8,128)(2,1)}, bf16[256,1024]{1,0:T(8,128)(2,1)}, u32[]{:S(2)}, u32[]{:S(2)}) collective-permute-start(bf16[256,1024]{1,0:T(8,128)(2,1)} %collective-permute-done.14.refs_2_), channel_id=1, source_target_pairs={{0,1},{1,0},{2,3},{3,2},{4,5},{5,4},{6,7},{7,6},{8,9},{9,8},{10,11... | collective-permute-start | bytes 1572872 | tf_op jit(solution)/shard_map/ppermute | solution.py:23
  98.8 17.2 %collective-permute-start.18 = (bf16[256,1024]{1,0:T(8,128)(2,1)}, bf16[256,1024]{1,0:T(8,128)(2,1)}, u32[]{:S(2)}, u32[]{:S(2)}) collective-permute-start(bf16[256,1024]{1,0:T(8,128)(2,1)} %collective-permute-done.15.refs_3_), channel_id=1, source_target_pairs={{0,1},{1,0},{2,3},{3,2},{4,5},{5,4},{6,7},{7,6},{8,9},{9,8},{10,11... | collective-permute-start | bytes 1572872 | tf_op jit(solution)/shard_map/ppermute | solution.py:23
  99.5 32.0 %collective-permute-start.19 = (bf16[1024,256]{1,0:T(8,128)(2,1)S(1)}, bf16[1024,256]{1,0:T(8,128)(2,1)S(1)}, u32[]{:S(2)}, u32[]{:S(2)}) collective-permute-start(bf16[1024,256]{1,0:T(8,128)(2,1)S(1)} %copy-done.7), channel_id=1, source_target_pairs={{0,64},{64,128},{128,192},{192,0},{1,65},{65,129},{129,193},{193,1... | collective-permute-start | bytes 1572872 | tf_op jit(solution)/shard_map/ppermute | solution.py:28
  100.4 34.8 %collective-permute-start.20 = (bf16[1024,256]{1,0:T(8,128)(2,1)S(1)}, bf16[1024,256]{1,0:T(8,128)(2,1)S(1)}, u32[]{:S(2)}, u32[]{:S(2)}) collective-permute-start(bf16[1024,256]{1,0:T(8,128)(2,1)S(1)} %copy-done.7), channel_id=1, source_target_pairs={{0,128},{64,192},{128,0},{192,64},{1,129},{65,193},{129,1},{193,65... | collective-permute-start | bytes 1572872 | tf_op jit(solution)/shard_map/ppermute | solution.py:28
  102.7 32.7 %collective-permute-start.21 = (bf16[1024,256]{1,0:T(8,128)(2,1)S(1)}, bf16[1024,256]{1,0:T(8,128)(2,1)S(1)}, u32[]{:S(2)}, u32[]{:S(2)}) collective-permute-start(bf16[1024,256]{1,0:T(8,128)(2,1)S(1)} %copy-done.7), channel_id=1, source_target_pairs={{0,192},{64,0},{128,64},{192,128},{1,193},{65,1},{129,65},{193,129... | collective-permute-start | bytes 1572872 | tf_op jit(solution)/shard_map/ppermute | solution.py:28
  105.9 19.0 %all-to-all-start.3 = ((bf16[8,104,128]{2,1,0:T(8,128)(2,1)}), bf16[8,104,128]{2,1,0:T(8,128)(2,1)S(1)}, u32[]{:S(2)}, u32[]{:S(2)}) async-start(bf16[8,104,128]{2,1,0:T(8,128)(2,1)} %get-tuple-element.23), calls=%async_computation.3 | async-start | bytes 425984 | tf_op jit(solution)/shard_map/all_to_all | solution.py:19
  128.1 9.8 %all-to-all-start.4 = ((bf16[4,24,2176]{2,1,0:T(8,128)(2,1)}), bf16[4,24,2176]{2,1,0:T(8,128)(2,1)S(1)}, u32[]{:S(2)}, u32[]{:S(2)}) async-start(bf16[4,24,2176]{2,1,0:T(8,128)(2,1)} %bitcast.4), calls=%async_computation.4 | async-start | bytes 835584 | tf_op jit(solution)/shard_map/all_to_all | solution.py:19
  131.6 10.7 %collective-permute-start.22 = (bf16[1024,256]{1,0:T(8,128)(2,1)S(1)}, bf16[1024,256]{1,0:T(8,128)(2,1)S(1)}, u32[]{:S(2)}, u32[]{:S(2)}) collective-permute-start(bf16[1024,256]{1,0:T(8,128)(2,1)S(1)} %collective-permute-done.19.refs_1_), channel_id=1, source_target_pairs={{0,1},{1,0},{2,3},{3,2},{4,5},{5,4},{6,7},{7,6},{8,9},{9,8},{10,11... | collective-permute-start | bytes 1572872 | tf_op jit(solution)/shard_map/ppermute | solution.py:23
  138.8 9.7 %all-to-all-start.5 = ((bf16[4,24,2048]{2,1,0:T(8,128)(2,1)}), bf16[4,24,2048]{2,1,0:T(8,128)(2,1)S(1)}, u32[]{:S(2)}, u32[]{:S(2)}) async-start(bf16[4,24,2048]{2,1,0:T(8,128)(2,1)} %shard_map.79), calls=%async_computation.5 | async-start | bytes 786432 | tf_op jit(solution)/shard_map/all_to_all | solution.py:19
  179.3 10.6 %collective-permute-start.26 = (bf16[8,96,128]{2,1,0:T(8,128)(2,1)S(1)}, bf16[8,96,128]{2,1,0:T(8,128)(2,1)S(1)}, u32[]{:S(2)}, u32[]{:S(2)}) collective-permute-start(bf16[8,96,128]{2,1,0:T(8,128)(2,1)S(1)} %all_to_all.41.own), channel_id=1, source_target_pairs={{0,1},{1,0},{2,3},{3,2},{4,5},{5,4},{6,7},{7,6},{8,9},{9,8},{10,11... | collective-permute-start | bytes 589832 | tf_op jit(solution)/shard_map/ppermute | solution.py:23
  (29 other events, 196.6 us)

commit v3 on v2

--- a/solution.py
+++ b/solution.py
@@ -26,6 +26,11 @@
 def along_y(a, shift):
     n = lax.axis_size("y")
     return lax.ppermute(a, "y", [(i, (i + shift) % n) for i in range(n)])
+
+
+def along_x(a, shift):
+    n = lax.axis_size("x")
+    return lax.ppermute(a, "x", [(i, (i + shift) % n) for i in range(n)])
 
 
 def by_plane(a, steps):
@@ -74,30 +79,39 @@
     return copies
 
 
-def up_own_kernel(gain, next_gain, tokens, own, out, scaled, kept, x, some, w, sems):
+def up_own_kernel(tokens, gain, next_gain, own, out, scaled, kept, x, g, g2, some, some_f, w, sems):
     half, hid = x.shape[0], own.shape[1]
     rows = some.shape[0]
+    nx, few, _ = some_f.shape
     y, z, c = lax.axis_index("y"), lax.axis_index("z"), lax.axis_index("c")
     first = pl.multiple_of(c * half, half)
     there = lax.rem(y + z // 2, lax.axis_size("y"))
     copies = fetch(
         (
+            (gain, g),
             (tokens.at[pl.ds(first, half), :], x),
             (own, w),
             (tokens.at[pl.ds(pl.multiple_of(first + there * rows, rows), rows), :], some),
+            (next_gain, g2),
         ),
         sems,
     )
     copies[0].wait()
+    copies[1].wait()
     xf = x[...].astype(F32)
     out[:, 2 * hid :] = stat_columns(jnp.sum(xf * xf, axis=1, keepdims=True))
-    scaled[...] = (xf * gain[...]).astype(BF)
-    copies[1].wait()
+    scaled[...] = (xf * g[...]).astype(BF)
+    copies[2].wait()
     out[:, :hid] = jnp.dot(scaled[...], w[...], preferred_element_type=F32).astype(BF)
-    copies[2].wait()
+    copies[3].wait()
+    copies[4].wait()
     left = lax.rem(z, 2) == 0
-    kept[:rows, :] = jnp.where(left, some[:, :LANES].astype(F32), some[:, LANES:].astype(F32))
-    chosen = jnp.where(left, next_gain[:, :LANES], next_gain[:, LANES:])
+    chosen = jnp.where(left, some[:, :LANES].astype(F32), some[:, LANES:].astype(F32))
+    for i in range(nx):
+        some_f[i] = chosen[i * few : (i + 1) * few]
+    for j in range(nx):
+        kept[j * few : (j + 1) * few, :] = some_f[lax.rem(lax.axis_index("x") + nx - j, nx)]
+    chosen = jnp.where(left, g2[:, :LANES], g2[:, LANES:])
     kept[rows:, :] = jnp.broadcast_to(chosen, (8, LANES))
 
 
@@ -110,20 +124,19 @@
 
 
 def summed(parts):
-    total = parts[0].astype(F32)
-    for i in range(1, parts.shape[0]):
-        total += parts[i].astype(F32)
+    total = parts[0][...].astype(F32)
+    for i in range(1, len(parts) if isinstance(parts, list) else parts.shape[0]):
+        total += parts[i][...].astype(F32)
     return total
 
 
-def activate_kernel(parts, out, *, width):
-    hid = parts.shape[2] - LANES
-    total = summed(parts)
+def activate_kernel(*refs, width):
+    *parts, out = refs
+    hid = out.shape[1]
+    total = summed(parts[0] if len(parts) == 1 else parts)
     meansq = (total[:, hid : hid + 1] + total[:, hid + 1 : hid + 2]) / width
     act = jnp.maximum(total[:, :hid] * lax.rsqrt(meansq + EPS), 0.0)
-    act = (act * act).astype(BF)
-    for i in range(out.shape[0]):
-        out[i] = act
+    out[...] = (act * act).astype(BF)
 
 
 def spots(blocks, held):
@@ -184,11 +197,13 @@
 
 
 def up_second_kernel(x, *refs):
-    *blocks, out, held, sems = refs
+    *refs, held, sems = refs
+    blocks, outs = refs[: held.shape[0]], refs[held.shape[0] :]
     copies = fetch(spots(blocks, held), sems)
     n = len(blocks) // 2
     depth, hid = blocks[0].shape
-    rows = out.shape[0]
+    few = outs[0].shape[0]
+    rows = few * len(outs)
     scaled, sq = [], jnp.zeros((rows, 1), F32)
     for i in range(x.shape[0]):
         xf = x[i, :rows, :].astype(F32)
@@ -204,23 +219,30 @@
             acc += jnp.dot(
                 scaled[:, d * depth : (d + 1) * depth], held[side * n + d], preferred_element_type=F32
             )
-        out[:, side * hid : (side + 1) * hid] = acc.astype(BF)
-    out[:, 2 * hid :] = stat_columns(sq)
+        for j, out in enumerate(outs):
+            out[:, side * hid : (side + 1) * hid] = acc[j * few : (j + 1) * few].astype(BF)
+    for j, out in enumerate(outs):
+        out[:, 2 * hid :] = stat_columns(sq[j * few : (j + 1) * few])
 
 
 def finish_second_kernel(parts, kept, out):
     out[...] = (0.5 * kept[...].astype(F32) + summed(parts)).astype(BF)
 
 
-def assemble_kernel(own, other, out):
-    chunks, rows, _ = own.shape
-    n = chunks // 2
-    y, c = lax.axis_index("y"), lax.axis_index("c")
+def assemble_kernel(own, other, out, placed):
+    chunks = own.shape[0]
+    ny = chunks // 2
+    few = placed.shape[1]
+    nx = own.shape[1] // few
+    x, y, c = lax.axis_index("x"), lax.axis_index("y"), lax.axis_index("c")
     for side, ref in ((c, own), (1 - c, other)):
-        for d in range(n):
-            start = pl.multiple_of((side * n + lax.rem(y + d, n)) * rows, rows)
-            out[pl.ds(start, rows), :LANES] = ref[2 * d]
-            out[pl.ds(start, rows), LANES:] = ref[2 * d + 1]
+        for i in range(chunks):
+            block = ref[i].astype(F32)
+            row = (side * ny + lax.rem(y + i // 2, ny)) * nx
+            column = (i % 2) * LANES
+            for j in range(nx):
+                placed[row + lax.rem(x + nx - j, nx), :, column : column + LANES] = block[j * few : (j + 1) * few]
+    out[...] = placed[...].reshape(out.shape).astype(BF)
 
 
 def spread(x, peers):
@@ -239,6 +261,10 @@
         far = [along_y(own[1][:half], 1), along_y(own[-1][half:], n - 1)]
         own[n // 2 : n // 2] = far
     return own + [swapped] + [from_other_core(v) for v in own[1:]]
+
+
+def from_x_ring(hidden, nx):
+    return jnp.concatenate([hidden] + [along_x(hidden, j) for j in range(1, nx)], axis=0)
 
 
 def body(tokens, gain_first, up_first, down_first, gain_second, up_second, down_second):
@@ -255,15 +281,25 @@
     def held(w, more=0):
         return [pltpu.VMEM((blocks, *w.shape), BF), pltpu.SemaphoreType.DMA((blocks + more,))]
 
-    activate = call(functools.partial(activate_kernel, width=width), sds((nx, few, hid)))
+    activate = call(functools.partial(activate_kernel, width=width), sds((few, hid)))
+    down_out = sds((nz, per_y, LANES))
 
     block = pltpu.VMEM(up_first.shape, BF)
+    row = pltpu.VMEM((1, channels), F32)
     payload, scaled, kept = call(
         up_own_kernel,
         (sds((half, wide)), sds((half, channels)), sds((per_y + 8, LANES), F32)),
-        [pltpu.VMEM((half, channels), BF), pltpu.VMEM((per_y, channels), BF), block, pltpu.SemaphoreType.DMA((3,))],
-        whole=2,
-    )(gain_first[None, :], gain_second[None, :], tokens, up_first)
+        [
+            pltpu.VMEM((half, channels), BF),
+            row,
+            row,
+            pltpu.VMEM((per_y, channels), BF),
+            pltpu.VMEM((nx, few, LANES), F32),
+            block,
+            pltpu.SemaphoreType.DMA((5,)),
+        ],
+        whole=0,
+    )(tokens, gain_first[None, :], gain_second[None, :], up_first)
     payload = call(
         up_other_kernel,
         sds((half, wide)),
@@ -282,23 +318,24 @@
     downs = around(down_first, order, forward=True)
     hidden = activate(parts)
 
-    hidden = exchange(hidden, "x").reshape(per_y, hid)
+    hidden = from_x_ring(hidden, nx)
+    branch = call(down_kernel, down_out, held(down_first, 2), whole=1)(hidden, *downs)
     ups = around(up_second, swapped[1])
-    branch = call(down_kernel, sds((nz, per_y, LANES)), held(down_first, 2), whole=1)(hidden, *downs)
     branch = exchange(branch, "z")
     downs = around(down_second, swapped[0])
     middle, payload = call(finish_first_kernel, (sds((per_y, LANES)), sds((nz, per_y + 8, LANES))))(
         branch, kept
     )
     payload = exchange(payload, "z")
-    payload = call(up_second_kernel, sds((per_y, wide)), held(up_second), whole=1)(payload, *ups)
-    parts = exchange(payload.reshape(nx, few, wide), "x")
-    hidden = activate(parts)
-    hidden = exchange(hidden, "x").reshape(per_y, hid)
-    branch = call(down_kernel, sds((nz, per_y, LANES)), held(down_second), whole=1)(hidden, *downs)
+    parts = call(up_second_kernel, (sds((few, wide)),) * nx, held(up_second), whole=1)(payload, *ups)
+    parts = [parts[0]] + [along_x(parts[j], nx - j) for j in range(1, nx)]
+    hidden = activate(*parts)
+    hidden = from_x_ring(hidden, nx)
+    branch = call(down_kernel, down_out, held(down_second), whole=1)(hidden, *downs)
     finished = call(finish_second_kernel, sds((per_y, LANES)))(exchange(branch, "z"), middle)
     rows = exchange(spread(by_plane(finished, lambda z: -(z // 2)), nz), "z")
-    return call(assemble_kernel, sds((count, channels)))(rows, from_other_core(rows))
+    placed = pltpu.VMEM((2 * ny * nx, few, channels), F32)
+    return call(assemble_kernel, sds((count, channels)), [placed])(rows, from_other_core(rows))
 
 
 def solution(mesh):

time: 191 us -> 196 us (1.026)
  starting transfers between devices: 69.5 us -> 80.9 us
  waiting for transfers between devices: 72.7 us -> 65.2 us
  local copies, waits for them, and re-layouts: 2.9 us -> 5.89 us
  Pallas kernels: 18.9 us -> 16.7 us
    all_to_all x6 -> x3, waiting for transfers between devices: 24.5 us -> 8.61 us  [exchange(): return lax.all_to_all(parts, axis, 0, 0, tiled=True)]
    ppermute x0 -> x9, starting transfers between devices: none -> 15.5 us  [along_x(): return lax.ppermute(a, 'x', [(i, (i + shift) % n) for i in range(n)])]
    ppermute x0 -> x9, waiting for transfers between devices: none -> 7.27 us  [along_x(): return lax.ppermute(a, 'x', [(i, (i + shift) % n) for i in range(n)])]
    all_to_all x6 -> x3, starting transfers between devices: 34.4 us -> 27.2 us  [exchange(): return lax.all_to_all(parts, axis, 0, 0, tiled=True)]
    ppermute x15, starting transfers between devices: 23.1 us -> 25.5 us  [from_other_core(): return lax.ppermute(w, 'c', [(0, 1), (1, 0)])]
    pallas_call x10, Pallas kernels: 18.9 us -> 16.7 us  [run(): pl.pallas_call(kernel, out_shape=out, in_specs=[vmem] * first + [lies] *...]
    unnamed x40 -> x42, local copies, waits for them, and re-layouts: 2.83 us -> 5.08 us
  transfers between devices with their start and end apart: 33 -> 39, of which waited for: 10 -> 12; matrix products, arithmetic and copies ran while one was open for 0% -> 0% of each run, Pallas kernels for 7% -> 6%
where the time goes in v3:
time: 196 us
  starting transfers between devices  80.9 us (41%)
  waiting for transfers between devices  65.2 us (33%)
  blocking collectives  26.4 us (13%)
  Pallas kernels  16.7 us (9%)
  local copies, waits for them, and re-layouts  5.89 us (3%)
    ppermute x10, waiting for transfers between devices, along_y(): return lax.ppermute(a, 'y', [(i, (i + shift) % n) for i in range(n)])  45.1 us
    all_to_all x3, starting transfers between devices, exchange(): return lax.all_to_all(parts, axis, 0, 0, tiled=True)  27.2 us
    all_to_all x2, blocking collectives, exchange(): return lax.all_to_all(parts, axis, 0, 0, tiled=True)  26.4 us
    ppermute x15, starting transfers between devices, from_other_core(): return lax.ppermute(w, 'c', [(0, 1), (1, 0)])  25.5 us
    pallas_call x10, Pallas kernels, run(): pl.pallas_call(kernel, out_shape=out, in_specs=[vmem] * first + [lies] *...  16.7 us
    ppermute x9, starting transfers between devices, along_x(): return lax.ppermute(a, 'x', [(i, (i + shift) % n) for i in range(n)])  15.5 us
    ppermute x10, starting transfers between devices, along_y(): return lax.ppermute(a, 'y', [(i, (i + shift) % n) for i in range(n)])  11.4 us
    all_to_all x3, waiting for transfers between devices, exchange(): return lax.all_to_all(parts, axis, 0, 0, tiled=True)  8.61 us
  transfers between devices with their start and end apart: 39, of which 12 were waited for; matrix products, arithmetic and copies ran while one was open for 0% of the time, Pallas kernels for 6%

profile of v3, /device:TPU:1, one launch (start us, length us, event | category | flops | bytes accessed | tf_op | source)
XLA Modules:
  0.0 195.6 jit_solution(11892192278621150751)
XLA Ops:
  0.0 3.2 %collective-permute-start = (bf16[256,1024]{1,0:T(8,128)(2,1)}, bf16[256,1024]{1,0:T(8,128)(2,1)S(1)}, u32[]{:S(2)}, u32[]{:S(2)}) collective-permute-start(bf16[256,1024]{1,0:T(8,128)(2,1)} %own.1), channel_id=1, source_target_pairs={{0,1},{1,0},{2,3},{3,2},{4,5},{5,4},{6,7},{7,6},{8,9},{9,8},{10,11... | collective-permute-start | bytes 1572872 | tf_op jit(solution)/shard_map/ppermute | solution.py:23
  3.2 2.8 %shard_map.73 = (bf16[384,2176]{1,0:T(8,128)(2,1)}, bf16[384,256]{1,0:T(8,128)(2,1)S(1)}, f32[104,128]{1,0:T(8,128)S(1)}) custom-call(bf16[768,256]{1,0:T(8,128)(2,1)} %tokens.1, f32[1,256]{1,0:T(1,128)} %bitcast.3, f32[1,256]{1,0:T(1,128)} %bitcast.4, bf16[256,1024]{1,0:T(8,128)(2,1)} %own.1), custom_call_target="tpu_custom_call" | custom-call | tf_op jit(solution)/shard_map/pallas_call | solution.py:50
  10.2 5.2 %all-to-all-start = ((bf16[16,24,2176]{2,1,0:T(8,128)(2,1)}), bf16[16,24,2176]{2,1,0:T(8,128)(2,1)S(1)}, u32[]{:S(2)}, u32[]{:S(2)}) async-start(bf16[16,24,2176]{2,1,0:T(8,128)(2,1)} %bitcast.2), calls=%async_computation | async-start | bytes 3342336 | tf_op jit(solution)/shard_map/all_to_all | solution.py:19
  21.4 27.0 %collective-permute-done.7.refs_1_ = bf16[1024,256]{1,0:T(8,128)(2,1)S(1)} collective-permute-done((bf16[1024,256]{1,0:T(8,128)(2,1)S(1)}, bf16[1024,256]{1,0:T(8,128)(2,1)S(1)}, u32[]{:S(2)}, u32[]{:S(2)}) %collective-permute-start.7) | collective-permute-done | bytes 524320 | tf_op jit(solution)/shard_map/ppermute | solution.py:28
  49.2 2.7 %collective-permute-start.10 = (bf16[512,256]{1,0:T(8,128)(2,1)S(1)}, bf16[512,256]{1,0:T(8,128)(2,1)S(1)}, u32[]{:S(2)}, u32[]{:S(2)}) collective-permute-start(bf16[512,256]{1,0:T(8,128)(2,1)S(1)} %slice.9), channel_id=1, source_target_pairs={{0,192},{64,0},{128,64},{192,128},{1,193},{65,1},{129,65},{193,129... | collective-permute-start | bytes 786440 | tf_op jit(solution)/shard_map/ppermute | solution.py:28
  52.9 12.5 %collective-permute-done.8.refs_2_ = bf16[512,256]{1,0:T(8,128)(2,1)} collective-permute-done((bf16[512,256]{1,0:T(8,128)(2,1)}, bf16[512,256]{1,0:T(8,128)(2,1)}, u32[]{:S(2)}, u32[]{:S(2)}) %collective-permute-start.8) | collective-permute-done | bytes 262176 | tf_op jit(solution)/shard_map/ppermute | solution.py:28
  65.9 2.7 %collective-permute-start.2 = (bf16[24,2048]{1,0:T(8,128)(2,1)S(1)}, bf16[24,2048]{1,0:T(8,128)(2,1)S(1)}, u32[]{:S(2)}, u32[]{:S(2)}) collective-permute-start(bf16[24,2048]{1,0:T(8,128)(2,1)S(1)} %shard_map.75), channel_id=1, source_target_pairs={{0,32},{16,48},{32,0},{48,16},{1,33},{17,49},{33,1},{49,17},{2,34}... | collective-permute-start | bytes 294920 | tf_op jit(solution)/shard_map/ppermute | solution.py:33
  69.5 2.3 %collective-permute-done.2 = bf16[24,2048]{1,0:T(8,128)(2,1)S(1)} collective-permute-done((bf16[24,2048]{1,0:T(8,128)(2,1)S(1)}, bf16[24,2048]{1,0:T(8,128)(2,1)S(1)}, u32[]{:S(2)}, u32[]{:S(2)}) %collective-permute-start.2) | collective-permute-done | bytes 98336 | tf_op jit(solution)/shard_map/ppermute | solution.py:33
  71.8 2.4 %collective-permute-start.3 = (bf16[24,2048]{1,0:T(8,128)(2,1)S(1)}, bf16[24,2048]{1,0:T(8,128)(2,1)S(1)}, u32[]{:S(2)}, u32[]{:S(2)}) collective-permute-start(bf16[24,2048]{1,0:T(8,128)(2,1)S(1)} %shard_map.75), channel_id=1, source_target_pairs={{0,48},{16,0},{32,16},{48,32},{1,49},{17,1},{33,17},{49,33},{2,50}... | collective-permute-start | bytes 294920 | tf_op jit(solution)/shard_map/ppermute | solution.py:33
  77.5 2.3 %collective-permute-start.19 = (bf16[256,1024]{1,0:T(8,128)(2,1)}, bf16[256,1024]{1,0:T(8,128)(2,1)}, u32[]{:S(2)}, u32[]{:S(2)}) collective-permute-start(bf16[256,1024]{1,0:T(8,128)(2,1)} %collective-permute-done.16.refs_1_), channel_id=1, source_target_pairs={{0,1},{1,0},{2,3},{3,2},{4,5},{5,4},{6,7},{7,6},{8,9},{9,8},{10,11... | collective-permute-start | bytes 1572872 | tf_op jit(solution)/shard_map/ppermute | solution.py:23
  81.5 4.3 %shard_map.76 = bf16[8,96,128]{2,1,0:T(8,128)(2,1)} custom-call(bf16[96,2048]{1,0:T(8,128)(2,1)S(1)} %pad_maximum_fusion.hidden, bf16[1024,256]{1,0:T(8,128)(2,1)} %refs_0_.2, bf16[1024,256]{1,0:T(8,128)(2,1)} %copy-done, bf16[512,256]{1,0:T(8,128)(2,1)} %collective-permute-done.8.refs_2_, bf16[512,256]{1,0:T(8,128)(2,1)} %copy-done.18, ...), custom_call_target="tpu_custom_call" | custom-call | tf_op jit(solution)/shard_map/pallas_call | solution.py:50
  85.8 8.2 %all-to-all-start.1 = ((bf16[8,96,128]{2,1,0:T(8,128)(2,1)}), bf16[8,96,128]{2,1,0:T(8,128)(2,1)S(1)}, u32[]{:S(2)}, u32[]{:S(2)}) async-start(bf16[8,96,128]{2,1,0:T(8,128)(2,1)} %shard_map.76), calls=%async_computation.1 | async-start | bytes 393216 | tf_op jit(solution)/shard_map/all_to_all | solution.py:19
  94.4 5.6 %collective-permute-done.18.refs_3_ = bf16[256,1024]{1,0:T(8,128)(2,1)} collective-permute-done((bf16[256,1024]{1,0:T(8,128)(2,1)}, bf16[256,1024]{1,0:T(8,128)(2,1)}, u32[]{:S(2)}, u32[]{:S(2)}) %collective-permute-start.18) | collective-permute-done | bytes 524320 | tf_op jit(solution)/shard_map/ppermute | solution.py:28
  103.3 2.5 %collective-permute-start.29 = (bf16[1024,256]{1,0:T(8,128)(2,1)S(1)}, bf16[1024,256]{1,0:T(8,128)(2,1)S(1)}, u32[]{:S(2)}, u32[]{:S(2)}) collective-permute-start(bf16[1024,256]{1,0:T(8,128)(2,1)S(1)} %copy-done.5), channel_id=1, source_target_pairs={{0,128},{64,192},{128,0},{192,64},{1,129},{65,193},{129,1},{193,65... | collective-permute-start | bytes 1572872 | tf_op jit(solution)/shard_map/ppermute | solution.py:28
  106.7 13.9 %all-to-all-start.2 = ((bf16[8,104,128]{2,1,0:T(8,128)(2,1)}), bf16[8,104,128]{2,1,0:T(8,128)(2,1)S(1)}, u32[]{:S(2)}, u32[]{:S(2)}) async-start(bf16[8,104,128]{2,1,0:T(8,128)(2,1)} %get-tuple-element.27), calls=%async_computation.2 | async-start | bytes 425984 | tf_op jit(solution)/shard_map/all_to_all | solution.py:19
  120.6 8.6 %all-to-all-done.2.x = bf16[8,104,128]{2,1,0:T(8,128)(2,1)S(1)} async-done(((bf16[8,104,128]{2,1,0:T(8,128)(2,1)}), bf16[8,104,128]{2,1,0:T(8,128)(2,1)S(1)}, u32[]{:S(2)}, u32[]{:S(2)}) %all-to-all-start.2) | async-done | bytes 213024 | tf_op jit(solution)/shard_map/all_to_all | solution.py:19
  129.2 2.5 %shard_map.78 = (bf16[24,2176]{1,0:T(8,128)(2,1)S(1)}, bf16[24,2176]{1,0:T(8,128)(2,1)S(1)}, bf16[24,2176]{1,0:T(8,128)(2,1)S(1)}, bf16[24,2176]{1,0:T(8,128)(2,1)S(1)}) custom-call(bf16[8,104,128]{2,1,0:T(8,128)(2,1)S(1)} %all-to-all-done.2.x, bf16[256,1024]{1,0:T(8,128)(2,1)} %refs_0_.3, bf16[256,1024]{1,0:T(8,128)(2,1)} %collective-permute-done.16.refs_1_, ...), custom_call_target="tpu_custom_call" | custom-call | tf_op jit(solution)/shard_map/pallas_call | solution.py:50
  131.7 3.1 %collective-permute-start.22 = (bf16[24,2176]{1,0:T(8,128)(2,1)S(1)}, bf16[24,2176]{1,0:T(8,128)(2,1)S(1)}, u32[]{:S(2)}, u32[]{:S(2)}) collective-permute-start(bf16[24,2176]{1,0:T(8,128)(2,1)S(1)} %get-tuple-element.29), channel_id=1, source_target_pairs={{0,48},{16,0},{32,16},{48,32},{1,49},{17,1},{33,17},{49,33},{2,50}... | collective-permute-start | bytes 313352 | tf_op jit(solution)/shard_map/ppermute | solution.py:33
  135.5 3.7 %collective-permute-start.31 = (bf16[1024,256]{1,0:T(8,128)(2,1)S(1)}, bf16[1024,256]{1,0:T(8,128)(2,1)S(1)}, u32[]{:S(2)}, u32[]{:S(2)}) collective-permute-start(bf16[1024,256]{1,0:T(8,128)(2,1)S(1)} %collective-permute-done.28.refs_1_), channel_id=1, source_target_pairs={{0,1},{1,0},{2,3},{3,2},{4,5},{5,4},{6,7},{7,6},{8,9},{9,8},{10,11... | collective-permute-start | bytes 1572872 | tf_op jit(solution)/shard_map/ppermute | solution.py:23
  142.3 4.2 %collective-permute-start.26 = (bf16[24,2048]{1,0:T(8,128)(2,1)S(1)}, bf16[24,2048]{1,0:T(8,128)(2,1)S(1)}, u32[]{:S(2)}, u32[]{:S(2)}) collective-permute-start(bf16[24,2048]{1,0:T(8,128)(2,1)S(1)} %shard_map.79), channel_id=1, source_target_pairs={{0,32},{16,48},{32,0},{48,16},{1,33},{17,49},{33,1},{49,17},{2,34}... | collective-permute-start | bytes 294920 | tf_op jit(solution)/shard_map/ppermute | solution.py:33
  153.0 3.6 %shard_map.80 = bf16[8,96,128]{2,1,0:T(8,128)(2,1)S(1)} custom-call(bf16[96,2048]{1,0:T(8,128)(2,1)S(1)} %pad_maximum_fusion.1.hidden, bf16[1024,256]{1,0:T(8,128)(2,1)} %refs_0_.4, bf16[1024,256]{1,0:T(8,128)(2,1)} %copy-done.8, bf16[1024,256]{1,0:T(8,128)(2,1)} %copy-done.9, bf16[1024,256]{1,0:T(8,128)(2,1)} %copy-done.10, bf16[1024,256]{1,0:T(8,128)(2,1)} %copy-done.6, ...), custom_call_target="tpu_custom_call" | custom-call | tf_op jit(solution)/shard_map/pallas_call | solution.py:50
  156.6 11.0 %all_to_all.25.parts = bf16[8,96,128]{2,1,0:T(8,128)(2,1)S(1)} all-to-all(bf16[8,96,128]{2,1,0:T(8,128)(2,1)S(1)} %shard_map.80), channel_id=1, replica_groups=mesh['y'=4,'x'=4,'z'=8,'c'=2] {'z'}, dimensions={0} | all-to-all | bytes 393216 | tf_op jit(solution)/shard_map/all_to_all | solution.py:19
  168.4 15.4 %all_to_all.26.own = bf16[8,96,128]{2,1,0:T(8,128)(2,1)S(1)} all-to-all(bf16[8,96,128]{2,1,0:T(8,128)(2,1)S(1)} %broadcast_in_dim.14), channel_id=1, replica_groups=mesh['y'=4,'x'=4,'z'=8,'c'=2] {'z'}, dimensions={0} | all-to-all | bytes 393216 | tf_op jit(solution)/shard_map/all_to_all | solution.py:19
  183.8 9.9 %collective-permute-start.35 = (bf16[8,96,128]{2,1,0:T(8,128)(2,1)S(1)}, bf16[8,96,128]{2,1,0:T(8,128)(2,1)S(1)}, u32[]{:S(2)}, u32[]{:S(2)}) collective-permute-start(bf16[8,96,128]{2,1,0:T(8,128)(2,1)S(1)} %all_to_all.26.own), channel_id=1, source_target_pairs={{0,1},{1,0},{2,3},{3,2},{4,5},{5,4},{6,7},{7,6},{8,9},{9,8},{10,11... | collective-permute-start | bytes 589832 | tf_op jit(solution)/shard_map/ppermute | solution.py:23
  (113 shorter events, 35.7 us)
Async XLA Ops:
  10.2 41.8 %all-to-all-start = ((bf16[16,24,2176]{2,1,0:T(8,128)(2,1)}), bf16[16,24,2176]{2,1,0:T(8,128)(2,1)S(1)}, u32[]{:S(2)}, u32[]{:S(2)}) async-start(bf16[16,24,2176]{2,1,0:T(8,128)(2,1)} %bitcast.2), calls=%async_computation | async-start | bytes 3342336 | tf_op jit(solution)/shard_map/all_to_all | solution.py:19
  18.3 30.1 %collective-permute-start.7 = (bf16[1024,256]{1,0:T(8,128)(2,1)S(1)}, bf16[1024,256]{1,0:T(8,128)(2,1)S(1)}, u32[]{:S(2)}, u32[]{:S(2)}) collective-permute-start(bf16[1024,256]{1,0:T(8,128)(2,1)S(1)} %copy-done.2), channel_id=1, source_target_pairs={{0,64},{64,128},{128,192},{192,0},{1,65},{65,129},{129,193},{193,1... | collective-permute-start | bytes 1572872 | tf_op jit(solution)/shard_map/ppermute | solution.py:28
  19.9 29.3 %collective-permute-start.9 = (bf16[1024,256]{1,0:T(8,128)(2,1)S(1)}, bf16[1024,256]{1,0:T(8,128)(2,1)S(1)}, u32[]{:S(2)}, u32[]{:S(2)}) collective-permute-start(bf16[1024,256]{1,0:T(8,128)(2,1)S(1)} %copy-done.2), channel_id=1, source_target_pairs={{0,192},{64,0},{128,64},{192,128},{1,193},{65,1},{129,65},{193,129... | collective-permute-start | bytes 1572872 | tf_op jit(solution)/shard_map/ppermute | solution.py:28
  21.1 47.5 %collective-permute-start.16 = (bf16[256,1024]{1,0:T(8,128)(2,1)}, bf16[256,1024]{1,0:T(8,128)(2,1)}, u32[]{:S(2)}, u32[]{:S(2)}) collective-permute-start(bf16[256,1024]{1,0:T(8,128)(2,1)} %refs_0_.3), channel_id=1, source_target_pairs={{0,64},{64,128},{128,192},{192,0},{1,65},{65,129},{129,193},{193,1... | collective-permute-start | bytes 1572872 | tf_op jit(solution)/shard_map/ppermute | solution.py:28
  49.2 16.2 %collective-permute-start.8 = (bf16[512,256]{1,0:T(8,128)(2,1)}, bf16[512,256]{1,0:T(8,128)(2,1)}, u32[]{:S(2)}, u32[]{:S(2)}) collective-permute-start(bf16[512,256]{1,0:T(8,128)(2,1)} %slice.8), channel_id=1, source_target_pairs={{0,64},{64,128},{128,192},{192,0},{1,65},{65,129},{129,193},{193,1... | collective-permute-start | bytes 786440 | tf_op jit(solution)/shard_map/ppermute | solution.py:28
  49.2 19.9 %collective-permute-start.10 = (bf16[512,256]{1,0:T(8,128)(2,1)S(1)}, bf16[512,256]{1,0:T(8,128)(2,1)S(1)}, u32[]{:S(2)}, u32[]{:S(2)}) collective-permute-start(bf16[512,256]{1,0:T(8,128)(2,1)S(1)} %slice.9), channel_id=1, source_target_pairs={{0,192},{64,0},{128,64},{192,128},{1,193},{65,1},{129,65},{193,129... | collective-permute-start | bytes 786440 | tf_op jit(solution)/shard_map/ppermute | solution.py:28
  52.4 16.6 %collective-permute-start.1 = (bf16[24,2048]{1,0:T(8,128)(2,1)S(1)}, bf16[24,2048]{1,0:T(8,128)(2,1)S(1)}, u32[]{:S(2)}, u32[]{:S(2)}) collective-permute-start(bf16[24,2048]{1,0:T(8,128)(2,1)S(1)} %shard_map.75), channel_id=1, source_target_pairs={{0,16},{16,32},{32,48},{48,0},{1,17},{17,33},{33,49},{49,1},{2,18}... | collective-permute-start | bytes 294920 | tf_op jit(solution)/shard_map/ppermute | solution.py:33
  65.4 11.0 %collective-permute-start.12 = (bf16[512,256]{1,0:T(8,128)(2,1)}, bf16[512,256]{1,0:T(8,128)(2,1)S(1)}, u32[]{:S(2)}, u32[]{:S(2)}) collective-permute-start(bf16[512,256]{1,0:T(8,128)(2,1)} %collective-permute-done.8.refs_2_), channel_id=1, source_target_pairs={{0,1},{1,0},{2,3},{3,2},{4,5},{5,4},{6,7},{7,6},{8,9},{9,8},{10,11... | collective-permute-start | bytes 786440 | tf_op jit(solution)/shard_map/ppermute | solution.py:23
  68.6 11.2 %collective-permute-start.11 = (bf16[1024,256]{1,0:T(8,128)(2,1)S(1)}, bf16[1024,256]{1,0:T(8,128)(2,1)S(1)}, u32[]{:S(2)}, u32[]{:S(2)}) collective-permute-start(bf16[1024,256]{1,0:T(8,128)(2,1)S(1)} %collective-permute-done.7.refs_1_), channel_id=1, source_target_pairs={{0,1},{1,0},{2,3},{3,2},{4,5},{5,4},{6,7},{7,6},{8,9},{9,8},{10,11... | collective-permute-start | bytes 1572872 | tf_op jit(solution)/shard_map/ppermute | solution.py:23
  68.9 10.9 %collective-permute-start.14 = (bf16[1024,256]{1,0:T(8,128)(2,1)S(1)}, bf16[1024,256]{1,0:T(8,128)(2,1)S(1)}, u32[]{:S(2)}, u32[]{:S(2)}) collective-permute-start(bf16[1024,256]{1,0:T(8,128)(2,1)S(1)} %collective-permute-done.9.refs_4_), channel_id=1, source_target_pairs={{0,1},{1,0},{2,3},{3,2},{4,5},{5,4},{6,7},{7,6},{8,9},{9,8},{10,11... | collective-permute-start | bytes 1572872 | tf_op jit(solution)/shard_map/ppermute | solution.py:23
  75.8 18.1 %collective-permute-start.17 = (bf16[256,1024]{1,0:T(8,128)(2,1)}, bf16[256,1024]{1,0:T(8,128)(2,1)S(1)}, u32[]{:S(2)}, u32[]{:S(2)}) collective-permute-start(bf16[256,1024]{1,0:T(8,128)(2,1)} %refs_0_.3), channel_id=1, source_target_pairs={{0,128},{64,192},{128,0},{192,64},{1,129},{65,193},{129,1},{193,65... | collective-permute-start | bytes 1572872 | tf_op jit(solution)/shard_map/ppermute | solution.py:28
  76.4 23.5 %collective-permute-start.18 = (bf16[256,1024]{1,0:T(8,128)(2,1)}, bf16[256,1024]{1,0:T(8,128)(2,1)}, u32[]{:S(2)}, u32[]{:S(2)}) collective-permute-start(bf16[256,1024]{1,0:T(8,128)(2,1)} %refs_0_.3), channel_id=1, source_target_pairs={{0,192},{64,0},{128,64},{192,128},{1,193},{65,1},{129,65},{193,129... | collective-permute-start | bytes 1572872 | tf_op jit(solution)/shard_map/ppermute | solution.py:28
  77.5 28.3 %collective-permute-start.19 = (bf16[256,1024]{1,0:T(8,128)(2,1)}, bf16[256,1024]{1,0:T(8,128)(2,1)}, u32[]{:S(2)}, u32[]{:S(2)}) collective-permute-start(bf16[256,1024]{1,0:T(8,128)(2,1)} %collective-permute-done.16.refs_1_), channel_id=1, source_target_pairs={{0,1},{1,0},{2,3},{3,2},{4,5},{5,4},{6,7},{7,6},{8,9},{9,8},{10,11... | collective-permute-start | bytes 1572872 | tf_op jit(solution)/shard_map/ppermute | solution.py:23
  85.8 20.2 %all-to-all-start.1 = ((bf16[8,96,128]{2,1,0:T(8,128)(2,1)}), bf16[8,96,128]{2,1,0:T(8,128)(2,1)S(1)}, u32[]{:S(2)}, u32[]{:S(2)}) async-start(bf16[8,96,128]{2,1,0:T(8,128)(2,1)} %shard_map.76), calls=%async_computation.1 | async-start | bytes 393216 | tf_op jit(solution)/shard_map/all_to_all | solution.py:19
  94.0 26.6 %collective-permute-start.20 = (bf16[256,1024]{1,0:T(8,128)(2,1)S(1)}, bf16[256,1024]{1,0:T(8,128)(2,1)}, u32[]{:S(2)}, u32[]{:S(2)}) collective-permute-start(bf16[256,1024]{1,0:T(8,128)(2,1)S(1)} %collective-permute-done.17.refs_2_), channel_id=1, source_target_pairs={{0,1},{1,0},{2,3},{3,2},{4,5},{5,4},{6,7},{7,6},{8,9},{9,8},{10,11... | collective-permute-start | bytes 1572872 | tf_op jit(solution)/shard_map/ppermute | solution.py:23
  99.9 20.6 %collective-permute-start.21 = (bf16[256,1024]{1,0:T(8,128)(2,1)}, bf16[256,1024]{1,0:T(8,128)(2,1)}, u32[]{:S(2)}, u32[]{:S(2)}) collective-permute-start(bf16[256,1024]{1,0:T(8,128)(2,1)} %collective-permute-done.18.refs_3_), channel_id=1, source_target_pairs={{0,1},{1,0},{2,3},{3,2},{4,5},{5,4},{6,7},{7,6},{8,9},{9,8},{10,11... | collective-permute-start | bytes 1572872 | tf_op jit(solution)/shard_map/ppermute | solution.py:23
  102.2 32.7 %collective-permute-start.28 = (bf16[1024,256]{1,0:T(8,128)(2,1)S(1)}, bf16[1024,256]{1,0:T(8,128)(2,1)S(1)}, u32[]{:S(2)}, u32[]{:S(2)}) collective-permute-start(bf16[1024,256]{1,0:T(8,128)(2,1)S(1)} %copy-done.5), channel_id=1, source_target_pairs={{0,64},{64,128},{128,192},{192,0},{1,65},{65,129},{129,193},{193,1... | collective-permute-start | bytes 1572872 | tf_op jit(solution)/shard_map/ppermute | solution.py:28
  103.3 32.2 %collective-permute-start.29 = (bf16[1024,256]{1,0:T(8,128)(2,1)S(1)}, bf16[1024,256]{1,0:T(8,128)(2,1)S(1)}, u32[]{:S(2)}, u32[]{:S(2)}) collective-permute-start(bf16[1024,256]{1,0:T(8,128)(2,1)S(1)} %copy-done.5), channel_id=1, source_target_pairs={{0,128},{64,192},{128,0},{192,64},{1,129},{65,193},{129,1},{193,65... | collective-permute-start | bytes 1572872 | tf_op jit(solution)/shard_map/ppermute | solution.py:28
  105.8 33.5 %collective-permute-start.30 = (bf16[1024,256]{1,0:T(8,128)(2,1)S(1)}, bf16[1024,256]{1,0:T(8,128)(2,1)S(1)}, u32[]{:S(2)}, u32[]{:S(2)}) collective-permute-start(bf16[1024,256]{1,0:T(8,128)(2,1)S(1)} %copy-done.5), channel_id=1, source_target_pairs={{0,192},{64,0},{128,64},{192,128},{1,193},{65,1},{129,65},{193,129... | collective-permute-start | bytes 1572872 | tf_op jit(solution)/shard_map/ppermute | solution.py:28
  106.7 22.5 %all-to-all-start.2 = ((bf16[8,104,128]{2,1,0:T(8,128)(2,1)}), bf16[8,104,128]{2,1,0:T(8,128)(2,1)S(1)}, u32[]{:S(2)}, u32[]{:S(2)}) async-start(bf16[8,104,128]{2,1,0:T(8,128)(2,1)} %get-tuple-element.27), calls=%async_computation.2 | async-start | bytes 425984 | tf_op jit(solution)/shard_map/all_to_all | solution.py:19
  135.5 15.7 %collective-permute-start.31 = (bf16[1024,256]{1,0:T(8,128)(2,1)S(1)}, bf16[1024,256]{1,0:T(8,128)(2,1)S(1)}, u32[]{:S(2)}, u32[]{:S(2)}) collective-permute-start(bf16[1024,256]{1,0:T(8,128)(2,1)S(1)} %collective-permute-done.28.refs_1_), channel_id=1, source_target_pairs={{0,1},{1,0},{2,3},{3,2},{4,5},{5,4},{6,7},{7,6},{8,9},{9,8},{10,11... | collective-permute-start | bytes 1572872 | tf_op jit(solution)/shard_map/ppermute | solution.py:23
  139.2 12.0 %collective-permute-start.32 = (bf16[1024,256]{1,0:T(8,128)(2,1)S(1)}, bf16[1024,256]{1,0:T(8,128)(2,1)S(1)}, u32[]{:S(2)}, u32[]{:S(2)}) collective-permute-start(bf16[1024,256]{1,0:T(8,128)(2,1)S(1)} %collective-permute-done.29.refs_2_), channel_id=1, source_target_pairs={{0,1},{1,0},{2,3},{3,2},{4,5},{5,4},{6,7},{7,6},{8,9},{9,8},{10,11... | collective-permute-start | bytes 1572872 | tf_op jit(solution)/shard_map/ppermute | solution.py:23
  139.4 11.9 %collective-permute-start.33 = (bf16[1024,256]{1,0:T(8,128)(2,1)S(1)}, bf16[1024,256]{1,0:T(8,128)(2,1)S(1)}, u32[]{:S(2)}, u32[]{:S(2)}) collective-permute-start(bf16[1024,256]{1,0:T(8,128)(2,1)S(1)} %collective-permute-done.30.refs_3_), channel_id=1, source_target_pairs={{0,1},{1,0},{2,3},{3,2},{4,5},{5,4},{6,7},{7,6},{8,9},{9,8},{10,11... | collective-permute-start | bytes 1572872 | tf_op jit(solution)/shard_map/ppermute | solution.py:23
  183.8 10.9 %collective-permute-start.35 = (bf16[8,96,128]{2,1,0:T(8,128)(2,1)S(1)}, bf16[8,96,128]{2,1,0:T(8,128)(2,1)S(1)}, u32[]{:S(2)}, u32[]{:S(2)}) collective-permute-start(bf16[8,96,128]{2,1,0:T(8,128)(2,1)S(1)} %all_to_all.26.own), channel_id=1, source_target_pairs={{0,1},{1,0},{2,3},{3,2},{4,5},{5,4},{6,7},{7,6},{8,9},{9,8},{10,11... | collective-permute-start | bytes 589832 | tf_op jit(solution)/shard_map/ppermute | solution.py:23
  (36 other events, 272.6 us)

commit v4 on v3

--- a/solution.py
+++ b/solution.py
@@ -139,39 +139,34 @@
     out[...] = (act * act).astype(BF)
 
 
-def spots(blocks, held):
-    pairs, i = [], 0
-    for block in blocks:
-        if isinstance(block, tuple):
-            rows = block[0].shape[0]
-            pairs += [(block[0], held.at[i, :rows]), (block[1], held.at[i, rows:])]
+def arriving(blocks, held, sems, order):
+    n, per = held.shape[0] // 2, len(blocks) // 2
+    far = n // 2
+    pairs, spans = [], {}
+    for side, d in order:
+        mine = blocks[side * per : (side + 1) * per]
+        spot = held.at[side * n + d]
+        first = len(pairs)
+        if d == far:
+            rows = mine[far].shape[0]
+            pairs += [(mine[far], spot.at[:rows]), (mine[far + 1], spot.at[rows:])]
         else:
-            pairs.append((block, held.at[i]))
-        i += 1
-    return pairs
-
-
-def grouped(refs, n):
-    if len(refs) == n:
-        return list(refs)
-    middle = n // 2
-    return [*refs[:middle], (refs[middle], refs[middle + 1]), *refs[middle + 2 :]]
+            pairs.append((mine[d + (d > far)], spot))
+        spans[side, d] = range(first, len(pairs))
+    copies = fetch(pairs, sems)
+
+    def ready(side, d):
+        for i in spans[side, d]:
+            copies[i].wait()
+        return held[side * n + d]
+
+    return ready
 
 
 def down_kernel(hidden, *refs):
     *blocks, out, held, sems = refs
     n, k = held.shape[0] // 2, held.shape[1]
-    per = len(blocks) // 2
-    copies = fetch(spots(grouped(blocks[:per], n) + grouped(blocks[per:], n), held), sems)
-    waited = [0, 0]
-
-    def ready(side, d):
-        upto = per if d == n - 1 else (d + 1 if d < n // 2 else d + 1 + per - n)
-        for i in range(waited[side], upto):
-            copies[side * per + i].wait()
-        waited[side] = upto
-        return held[side * n + d]
-
+    ready = arriving(blocks, held, sems, [(side, d) for d in range(n) for side in range(2)])
     for d in range(n):
         acc = jnp.dot(hidden[:, :k], ready(0, d), preferred_element_type=F32)
         acc += jnp.dot(hidden[:, k:], ready(1, d), preferred_element_type=F32)
@@ -198,10 +193,9 @@
 
 def up_second_kernel(x, *refs):
     *refs, held, sems = refs
-    blocks, outs = refs[: held.shape[0]], refs[held.shape[0] :]
-    copies = fetch(spots(blocks, held), sems)
-    n = len(blocks) // 2
-    depth, hid = blocks[0].shape
+    blocks, outs = refs[: held.shape[0] + 2], refs[held.shape[0] + 2 :]
+    n, depth, hid = held.shape[0] // 2, *held.shape[1:]
+    ready = arriving(blocks, held, sems, [(side, d) for side in range(2) for d in range(n)])
     few = outs[0].shape[0]
     rows = few * len(outs)
     scaled, sq = [], jnp.zeros((rows, 1), F32)
@@ -215,9 +209,8 @@
     for side in range(2):
         acc = jnp.zeros((rows, hid), F32)
         for d in range(n):
-            copies[side * n + d].wait()
             acc += jnp.dot(
-                scaled[:, d * depth : (d + 1) * depth], held[side * n + d], preferred_element_type=F32
+                scaled[:, d * depth : (d + 1) * depth], ready(side, d), preferred_element_type=F32
             )
         for j, out in enumerate(outs):
             out[:, side * hid : (side + 1) * hid] = acc[j * few : (j + 1) * few].astype(BF)
@@ -249,18 +242,13 @@
     return jnp.broadcast_to(x[None], (peers, *x.shape))
 
 
-def after(w, done):
-    return lax.optimization_barrier((w, done))
-
-
-def around(w, swapped, forward=False):
+def around(w, swapped):
     n = lax.axis_size("y")
-    own = [w] + [along_y(w, d) for d in range(1, n) if not (forward and d == n // 2)]
-    if forward:
-        half = w.shape[0] // 2
-        far = [along_y(own[1][:half], 1), along_y(own[-1][half:], n - 1)]
-        own[n // 2 : n // 2] = far
-    return own + [swapped] + [from_other_core(v) for v in own[1:]]
+    half = w.shape[0] // 2
+    near = [along_y(w, 1), along_y(w, n - 1)]
+    far = [along_y(near[0][:half], 1), along_y(near[1][half:], n - 1)]
+    moved = [near[0], *far, near[1]]
+    return [w, *moved, swapped] + [from_other_core(v) for v in moved]
 
 
 def from_x_ring(hidden, nx):
@@ -278,8 +266,8 @@
     wide = hid + LANES
     blocks = 2 * ny
 
-    def held(w, more=0):
-        return [pltpu.VMEM((blocks, *w.shape), BF), pltpu.SemaphoreType.DMA((blocks + more,))]
+    def held(w):
+        return [pltpu.VMEM((blocks, *w.shape), BF), pltpu.SemaphoreType.DMA((blocks + 2,))]
 
     activate = call(functools.partial(activate_kernel, width=width), sds((few, hid)))
     down_out = sds((nz, per_y, LANES))
@@ -309,20 +297,15 @@
     )(scaled, from_other_core(up_first), payload)
     parts = exchange(payload.reshape(ny * nx, few, wide), RA)
     kept = by_plane(kept, lambda z: z // 2)
-    swapped, order = [], payload
-    for w in (down_second, up_second, down_first):
-        w, order = after(w, order)
-        order = from_other_core(w)
-        swapped.append(order)
-    down_first, order = after(down_first, order)
-    downs = around(down_first, order, forward=True)
+    swapped = [from_other_core(w) for w in (down_first, up_second, down_second)]
+    downs = around(down_first, swapped[0])
     hidden = activate(parts)
 
     hidden = from_x_ring(hidden, nx)
-    branch = call(down_kernel, down_out, held(down_first, 2), whole=1)(hidden, *downs)
+    branch = call(down_kernel, down_out, held(down_first), whole=1)(hidden, *downs)
     ups = around(up_second, swapped[1])
     branch = exchange(branch, "z")
-    downs = around(down_second, swapped[0])
+    downs = around(down_second, swapped[2])
     middle, payload = call(finish_first_kernel, (sds((per_y, LANES)), sds((nz, per_y + 8, LANES))))(
         branch, kept
     )

time: 196 us -> 183 us (0.934)
  waiting for transfers between devices: 65.2 us -> 53.6 us
    ppermute x10 -> x12, waiting for transfers between devices: 45.1 us -> 34.3 us  [along_y(): return lax.ppermute(a, 'y', [(i, (i + shift) % n) for i in range(n)])]
    ppermute x9, starting transfers between devices: 15.5 us -> 9.4 us  [along_x(): return lax.ppermute(a, 'x', [(i, (i + shift) % n) for i in range(n)])]
    all_to_all x3, starting transfers between devices: 27.2 us -> 31.1 us  [exchange(): return lax.all_to_all(parts, axis, 0, 0, tiled=True)]
    ppermute x9, waiting for transfers between devices: 7.27 us -> 9.47 us  [along_x(): return lax.ppermute(a, 'x', [(i, (i + shift) % n) for i in range(n)])]
    unnamed x42 -> x38, local copies, waits for them, and re-layouts: 5.08 us -> 3.1 us
    ppermute x15 -> x17, waiting for transfers between devices: 4.25 us -> 2.51 us  [from_other_core(): return lax.ppermute(w, 'c', [(0, 1), (1, 0)])]
    ppermute x10 -> x12, starting transfers between devices: 11.4 us -> 13 us  [along_y(): return lax.ppermute(a, 'y', [(i, (i + shift) % n) for i in range(n)])]
    ppermute x15 -> x17, starting transfers between devices: 25.5 us -> 24.4 us  [from_other_core(): return lax.ppermute(w, 'c', [(0, 1), (1, 0)])]
  transfers between devices with their start and end apart: 39 -> 43, of which waited for: 12 -> 14; matrix products, arithmetic and copies ran while one was open for 0% -> 1% of each run, Pallas kernels for 6% -> 6%
where the time goes in v4:
time: 183 us
  starting transfers between devices  79.3 us (43%)
  waiting for transfers between devices  53.6 us (29%)
  blocking collectives  28.3 us (15%)
  Pallas kernels  15.8 us (9%)
  local copies, waits for them, and re-layouts  5.42 us (3%)
    ppermute x12, waiting for transfers between devices, along_y(): return lax.ppermute(a, 'y', [(i, (i + shift) % n) for i in range(n)])  34.3 us
    all_to_all x3, starting transfers between devices, exchange(): return lax.all_to_all(parts, axis, 0, 0, tiled=True)  31.1 us
    all_to_all x2, blocking collectives, exchange(): return lax.all_to_all(parts, axis, 0, 0, tiled=True)  28.3 us
    ppermute x17, starting transfers between devices, from_other_core(): return lax.ppermute(w, 'c', [(0, 1), (1, 0)])  24.4 us
    pallas_call x10, Pallas kernels, run(): pl.pallas_call(kernel, out_shape=out, in_specs=[vmem] * first + [lies] *...  15.8 us
    ppermute x12, starting transfers between devices, along_y(): return lax.ppermute(a, 'y', [(i, (i + shift) % n) for i in range(n)])  13 us
    ppermute x9, waiting for transfers between devices, along_x(): return lax.ppermute(a, 'x', [(i, (i + shift) % n) for i in range(n)])  9.47 us
    ppermute x9, starting transfers between devices, along_x(): return lax.ppermute(a, 'x', [(i, (i + shift) % n) for i in range(n)])  9.4 us
  transfers between devices with their start and end apart: 43, of which 14 were waited for; matrix products, arithmetic and copies ran while one was open for 1% of the time, Pallas kernels for 6%

profile of v4, /device:TPU:1, one launch (start us, length us, event | category | flops | bytes accessed | tf_op | source)
XLA Modules:
  0.0 182.9 jit_solution(12203060344522056616)
XLA Ops:
  0.0 3.2 %collective-permute-start = (bf16[256,1024]{1,0:T(8,128)(2,1)}, bf16[256,1024]{1,0:T(8,128)(2,1)S(1)}, u32[]{:S(2)}, u32[]{:S(2)}) collective-permute-start(bf16[256,1024]{1,0:T(8,128)(2,1)} %own.1), channel_id=1, source_target_pairs={{0,1},{1,0},{2,3},{3,2},{4,5},{5,4},{6,7},{7,6},{8,9},{9,8},{10,11... | collective-permute-start | bytes 1572872 | tf_op jit(solution)/shard_map/ppermute | solution.py:23
  3.2 2.8 %shard_map.73 = (bf16[384,2176]{1,0:T(8,128)(2,1)}, bf16[384,256]{1,0:T(8,128)(2,1)S(1)}, f32[104,128]{1,0:T(8,128)S(1)}) custom-call(bf16[768,256]{1,0:T(8,128)(2,1)} %tokens.1, f32[1,256]{1,0:T(1,128)} %bitcast.3, f32[1,256]{1,0:T(1,128)} %bitcast.4, bf16[256,1024]{1,0:T(8,128)(2,1)} %own.1), custom_call_target="tpu_custom_call" | custom-call | tf_op jit(solution)/shard_map/pallas_call | solution.py:50
  7.4 5.2 %all-to-all-start = ((bf16[16,24,2176]{2,1,0:T(8,128)(2,1)}), bf16[16,24,2176]{2,1,0:T(8,128)(2,1)S(1)}, u32[]{:S(2)}, u32[]{:S(2)}) async-start(bf16[16,24,2176]{2,1,0:T(8,128)(2,1)} %bitcast.2), calls=%async_computation | async-start | bytes 3342336 | tf_op jit(solution)/shard_map/all_to_all | solution.py:19
  16.3 28.8 %collective-permute-done.4.refs_1_ = bf16[1024,256]{1,0:T(8,128)(2,1)S(1)} collective-permute-done((bf16[1024,256]{1,0:T(8,128)(2,1)S(1)}, bf16[1024,256]{1,0:T(8,128)(2,1)S(1)}, u32[]{:S(2)}, u32[]{:S(2)}) %collective-permute-start.4) | collective-permute-done | bytes 524320 | tf_op jit(solution)/shard_map/ppermute | solution.py:28
  45.2 2.7 %collective-permute-start.7 = (bf16[512,256]{1,0:T(8,128)(2,1)S(1)}, bf16[512,256]{1,0:T(8,128)(2,1)}, u32[]{:S(2)}, u32[]{:S(2)}) collective-permute-start(bf16[512,256]{1,0:T(8,128)(2,1)S(1)} %slice.25), channel_id=1, source_target_pairs={{0,192},{64,0},{128,64},{192,128},{1,193},{65,1},{129,65},{193,129... | collective-permute-start | bytes 786440 | tf_op jit(solution)/shard_map/ppermute | solution.py:28
  49.7 3.6 %collective-permute-done.5.refs_2_ = bf16[512,256]{1,0:T(8,128)(2,1)} collective-permute-done((bf16[512,256]{1,0:T(8,128)(2,1)S(1)}, bf16[512,256]{1,0:T(8,128)(2,1)}, u32[]{:S(2)}, u32[]{:S(2)}) %collective-permute-start.5) | collective-permute-done | bytes 262176 | tf_op jit(solution)/shard_map/ppermute | solution.py:28
  53.2 2.0 %collective-permute-start.10 = (bf16[512,256]{1,0:T(8,128)(2,1)}, bf16[512,256]{1,0:T(8,128)(2,1)}, u32[]{:S(2)}, u32[]{:S(2)}) collective-permute-start(bf16[512,256]{1,0:T(8,128)(2,1)} %collective-permute-done.5.refs_2_), channel_id=1, source_target_pairs={{0,1},{1,0},{2,3},{3,2},{4,5},{5,4},{6,7},{7,6},{8,9},{9,8},{10,11... | collective-permute-start | bytes 786440 | tf_op jit(solution)/shard_map/ppermute | solution.py:23
  57.4 2.7 %collective-permute-start.2 = (bf16[24,2048]{1,0:T(8,128)(2,1)S(1)}, bf16[24,2048]{1,0:T(8,128)(2,1)S(1)}, u32[]{:S(2)}, u32[]{:S(2)}) collective-permute-start(bf16[24,2048]{1,0:T(8,128)(2,1)S(1)} %shard_map.75), channel_id=1, source_target_pairs={{0,32},{16,48},{32,0},{48,16},{1,33},{17,49},{33,1},{49,17},{2,34}... | collective-permute-start | bytes 294920 | tf_op jit(solution)/shard_map/ppermute | solution.py:33
  61.8 2.6 %collective-permute-start.16 = (bf16[256,1024]{1,0:T(8,128)(2,1)}, bf16[256,1024]{1,0:T(8,128)(2,1)S(1)}, u32[]{:S(2)}, u32[]{:S(2)}) collective-permute-start(bf16[256,1024]{1,0:T(8,128)(2,1)} %refs_0_.4), channel_id=1, source_target_pairs={{0,192},{64,0},{128,64},{192,128},{1,193},{65,1},{129,65},{193,129... | collective-permute-start | bytes 1572872 | tf_op jit(solution)/shard_map/ppermute | solution.py:28
  65.8 3.8 %shard_map.76 = bf16[8,96,128]{2,1,0:T(8,128)(2,1)} custom-call(bf16[96,2048]{1,0:T(8,128)(2,1)S(1)} %pad_maximum_fusion.hidden, bf16[1024,256]{1,0:T(8,128)(2,1)} %refs_0_.3, bf16[1024,256]{1,0:T(8,128)(2,1)} %copy-done.4, bf16[512,256]{1,0:T(8,128)(2,1)} %collective-permute-done.5.refs_2_, bf16[512,256]{1,0:T(8,128)(2,1)} %collective-permute-done.7.refs_3_, ...), custom_call_target="tpu_custom_call" | custom-call | tf_op jit(solution)/shard_map/pallas_call | solution.py:50
  69.6 8.2 %all-to-all-start.1 = ((bf16[8,96,128]{2,1,0:T(8,128)(2,1)}), bf16[8,96,128]{2,1,0:T(8,128)(2,1)S(1)}, u32[]{:S(2)}, u32[]{:S(2)}) async-start(bf16[8,96,128]{2,1,0:T(8,128)(2,1)} %shard_map.76), calls=%async_computation.1 | async-start | bytes 393216 | tf_op jit(solution)/shard_map/all_to_all | solution.py:19
  85.0 2.0 %collective-permute-done.29.refs_1_ = bf16[1024,256]{1,0:T(8,128)(2,1)S(1)} collective-permute-done((bf16[1024,256]{1,0:T(8,128)(2,1)}, bf16[1024,256]{1,0:T(8,128)(2,1)S(1)}, u32[]{:S(2)}, u32[]{:S(2)}) %collective-permute-start.29) | collective-permute-done | bytes 524320 | tf_op jit(solution)/shard_map/ppermute | solution.py:28
  88.2 17.8 %all-to-all-start.2 = ((bf16[8,104,128]{2,1,0:T(8,128)(2,1)}), bf16[8,104,128]{2,1,0:T(8,128)(2,1)S(1)}, u32[]{:S(2)}, u32[]{:S(2)}) async-start(bf16[8,104,128]{2,1,0:T(8,128)(2,1)} %get-tuple-element.17), calls=%async_computation.2 | async-start | bytes 425984 | tf_op jit(solution)/shard_map/all_to_all | solution.py:19
  109.9 7.3 %all-to-all-done.2.x = bf16[8,104,128]{2,1,0:T(8,128)(2,1)S(1)} async-done(((bf16[8,104,128]{2,1,0:T(8,128)(2,1)}), bf16[8,104,128]{2,1,0:T(8,128)(2,1)S(1)}, u32[]{:S(2)}, u32[]{:S(2)}) %all-to-all-start.2) | async-done | bytes 213024 | tf_op jit(solution)/shard_map/all_to_all | solution.py:19
  117.2 2.5 %shard_map.78 = (bf16[24,2176]{1,0:T(8,128)(2,1)S(1)}, bf16[24,2176]{1,0:T(8,128)(2,1)S(1)}, bf16[24,2176]{1,0:T(8,128)(2,1)S(1)}, bf16[24,2176]{1,0:T(8,128)(2,1)S(1)}) custom-call(bf16[8,104,128]{2,1,0:T(8,128)(2,1)S(1)} %all-to-all-done.2.x, bf16[256,1024]{1,0:T(8,128)(2,1)} %refs_0_.4, bf16[256,1024]{1,0:T(8,128)(2,1)} %copy-done.2, ...), custom_call_target="tpu_custom_call" | custom-call | tf_op jit(solution)/shard_map/pallas_call | solution.py:50
  121.4 2.3 %collective-permute-done.23.refs_1_ = bf16[24,2176]{1,0:T(8,128)(2,1)S(1)} collective-permute-done((bf16[24,2176]{1,0:T(8,128)(2,1)S(1)}, bf16[24,2176]{1,0:T(8,128)(2,1)S(1)}, u32[]{:S(2)}, u32[]{:S(2)}) %collective-permute-start.23) | collective-permute-done | bytes 104480 | tf_op jit(solution)/shard_map/ppermute | solution.py:33
  123.7 2.4 %collective-permute-start.33 = (bf16[1024,256]{1,0:T(8,128)(2,1)}, bf16[1024,256]{1,0:T(8,128)(2,1)S(1)}, u32[]{:S(2)}, u32[]{:S(2)}) collective-permute-start(bf16[1024,256]{1,0:T(8,128)(2,1)} %refs_0_.5), channel_id=1, source_target_pairs={{0,1},{1,0},{2,3},{3,2},{4,5},{5,4},{6,7},{7,6},{8,9},{9,8},{10,11... | collective-permute-start | bytes 1572872 | tf_op jit(solution)/shard_map/ppermute | solution.py:23
  129.3 2.3 %collective-permute-start.27 = (bf16[24,2048]{1,0:T(8,128)(2,1)S(1)}, bf16[24,2048]{1,0:T(8,128)(2,1)S(1)}, u32[]{:S(2)}, u32[]{:S(2)}) collective-permute-start(bf16[24,2048]{1,0:T(8,128)(2,1)S(1)} %shard_map.79), channel_id=1, source_target_pairs={{0,32},{16,48},{32,0},{48,16},{1,33},{17,49},{33,1},{49,17},{2,34}... | collective-permute-start | bytes 294920 | tf_op jit(solution)/shard_map/ppermute | solution.py:33
  131.6 3.8 %collective-permute-done.26 = bf16[24,2048]{1,0:T(8,128)(2,1)S(1)} collective-permute-done((bf16[24,2048]{1,0:T(8,128)(2,1)S(1)}, bf16[24,2048]{1,0:T(8,128)(2,1)S(1)}, u32[]{:S(2)}, u32[]{:S(2)}) %collective-permute-start.26) | collective-permute-done | bytes 98336 | tf_op jit(solution)/shard_map/ppermute | solution.py:33
  138.9 3.5 %collective-permute-start.36 = (bf16[512,256]{1,0:T(8,128)(2,1)S(1)}, bf16[512,256]{1,0:T(8,128)(2,1)S(1)}, u32[]{:S(2)}, u32[]{:S(2)}) collective-permute-start(bf16[512,256]{1,0:T(8,128)(2,1)S(1)} %collective-permute-done.32.refs_3_), channel_id=1, source_target_pairs={{0,1},{1,0},{2,3},{3,2},{4,5},{5,4},{6,7},{7,6},{8,9},{9,8},{10,11... | collective-permute-start | bytes 786440 | tf_op jit(solution)/shard_map/ppermute | solution.py:23
  145.3 3.1 %shard_map.80 = bf16[8,96,128]{2,1,0:T(8,128)(2,1)S(1)} custom-call(bf16[96,2048]{1,0:T(8,128)(2,1)S(1)} %pad_maximum_fusion.1.hidden, bf16[1024,256]{1,0:T(8,128)(2,1)} %refs_0_.5, bf16[1024,256]{1,0:T(8,128)(2,1)} %copy-done, bf16[512,256]{1,0:T(8,128)(2,1)} %copy-done.12, bf16[512,256]{1,0:T(8,128)(2,1)} %copy-done.14, bf16[1024,256]{1,0:T(8,128)(2,1)} %copy-done.1, ...), custom_call_target="tpu_custom_call" | custom-call | tf_op jit(solution)/shard_map/pallas_call | solution.py:50
  148.4 12.4 %all_to_all.25.parts = bf16[8,96,128]{2,1,0:T(8,128)(2,1)S(1)} all-to-all(bf16[8,96,128]{2,1,0:T(8,128)(2,1)S(1)} %shard_map.80), channel_id=1, replica_groups=mesh['y'=4,'x'=4,'z'=8,'c'=2] {'z'}, dimensions={0} | all-to-all | bytes 393216 | tf_op jit(solution)/shard_map/all_to_all | solution.py:19
  161.6 15.9 %all_to_all.26.own = bf16[8,96,128]{2,1,0:T(8,128)(2,1)S(1)} all-to-all(bf16[8,96,128]{2,1,0:T(8,128)(2,1)S(1)} %broadcast_in_dim.14), channel_id=1, replica_groups=mesh['y'=4,'x'=4,'z'=8,'c'=2] {'z'}, dimensions={0} | all-to-all | bytes 393216 | tf_op jit(solution)/shard_map/all_to_all | solution.py:19
  177.4 3.5 %collective-permute-start.39 = (bf16[8,96,128]{2,1,0:T(8,128)(2,1)S(1)}, bf16[8,96,128]{2,1,0:T(8,128)(2,1)S(1)}, u32[]{:S(2)}, u32[]{:S(2)}) collective-permute-start(bf16[8,96,128]{2,1,0:T(8,128)(2,1)S(1)} %all_to_all.26.own), channel_id=1, source_target_pairs={{0,1},{1,0},{2,3},{3,2},{4,5},{5,4},{6,7},{7,6},{8,9},{9,8},{10,11... | collective-permute-start | bytes 589832 | tf_op jit(solution)/shard_map/ppermute | solution.py:23
  (121 shorter events, 38.1 us)
Async XLA Ops:
  7.4 48.3 %all-to-all-start = ((bf16[16,24,2176]{2,1,0:T(8,128)(2,1)}), bf16[16,24,2176]{2,1,0:T(8,128)(2,1)S(1)}, u32[]{:S(2)}, u32[]{:S(2)}) async-start(bf16[16,24,2176]{2,1,0:T(8,128)(2,1)} %bitcast.2), calls=%async_computation | async-start | bytes 3342336 | tf_op jit(solution)/shard_map/all_to_all | solution.py:19
  12.7 32.4 %collective-permute-start.4 = (bf16[1024,256]{1,0:T(8,128)(2,1)S(1)}, bf16[1024,256]{1,0:T(8,128)(2,1)S(1)}, u32[]{:S(2)}, u32[]{:S(2)}) collective-permute-start(bf16[1024,256]{1,0:T(8,128)(2,1)S(1)} %copy-done.6), channel_id=1, source_target_pairs={{0,64},{64,128},{128,192},{192,0},{1,65},{65,129},{129,193},{193,1... | collective-permute-start | bytes 1572872 | tf_op jit(solution)/shard_map/ppermute | solution.py:28
  14.1 31.1 %collective-permute-start.6 = (bf16[1024,256]{1,0:T(8,128)(2,1)S(1)}, bf16[1024,256]{1,0:T(8,128)(2,1)S(1)}, u32[]{:S(2)}, u32[]{:S(2)}) collective-permute-start(bf16[1024,256]{1,0:T(8,128)(2,1)S(1)} %copy-done.6), channel_id=1, source_target_pairs={{0,192},{64,0},{128,64},{192,128},{1,193},{65,1},{129,65},{193,129... | collective-permute-start | bytes 1572872 | tf_op jit(solution)/shard_map/ppermute | solution.py:28
  15.4 40.7 %collective-permute-start.8 = (bf16[1024,256]{1,0:T(8,128)(2,1)S(1)}, bf16[1024,256]{1,0:T(8,128)(2,1)}, u32[]{:S(2)}, u32[]{:S(2)}) collective-permute-start(bf16[1024,256]{1,0:T(8,128)(2,1)S(1)} %copy-done.6), channel_id=1, source_target_pairs={{0,1},{1,0},{2,3},{3,2},{4,5},{5,4},{6,7},{7,6},{8,9},{9,8},{10,11... | collective-permute-start | bytes 1572872 | tf_op jit(solution)/shard_map/ppermute | solution.py:23
  45.1 8.1 %collective-permute-start.5 = (bf16[512,256]{1,0:T(8,128)(2,1)S(1)}, bf16[512,256]{1,0:T(8,128)(2,1)}, u32[]{:S(2)}, u32[]{:S(2)}) collective-permute-start(bf16[512,256]{1,0:T(8,128)(2,1)S(1)} %slice.24), channel_id=1, source_target_pairs={{0,64},{64,128},{128,192},{192,0},{1,65},{65,129},{129,193},{193,1... | collective-permute-start | bytes 786440 | tf_op jit(solution)/shard_map/ppermute | solution.py:28
  45.2 10.0 %collective-permute-start.7 = (bf16[512,256]{1,0:T(8,128)(2,1)S(1)}, bf16[512,256]{1,0:T(8,128)(2,1)}, u32[]{:S(2)}, u32[]{:S(2)}) collective-permute-start(bf16[512,256]{1,0:T(8,128)(2,1)S(1)} %slice.25), channel_id=1, source_target_pairs={{0,192},{64,0},{128,64},{192,128},{1,193},{65,1},{129,65},{193,129... | collective-permute-start | bytes 786440 | tf_op jit(solution)/shard_map/ppermute | solution.py:28
  48.0 13.7 %collective-permute-start.12 = (bf16[1024,256]{1,0:T(8,128)(2,1)S(1)}, bf16[1024,256]{1,0:T(8,128)(2,1)}, u32[]{:S(2)}, u32[]{:S(2)}) collective-permute-start(bf16[1024,256]{1,0:T(8,128)(2,1)S(1)} %collective-permute-done.6.refs_4_), channel_id=1, source_target_pairs={{0,1},{1,0},{2,3},{3,2},{4,5},{5,4},{6,7},{7,6},{8,9},{9,8},{10,11... | collective-permute-start | bytes 1572872 | tf_op jit(solution)/shard_map/ppermute | solution.py:23
  55.2 10.6 %collective-permute-start.9 = (bf16[1024,256]{1,0:T(8,128)(2,1)S(1)}, bf16[1024,256]{1,0:T(8,128)(2,1)}, u32[]{:S(2)}, u32[]{:S(2)}) collective-permute-start(bf16[1024,256]{1,0:T(8,128)(2,1)S(1)} %collective-permute-done.4.refs_1_), channel_id=1, source_target_pairs={{0,1},{1,0},{2,3},{3,2},{4,5},{5,4},{6,7},{7,6},{8,9},{9,8},{10,11... | collective-permute-start | bytes 1572872 | tf_op jit(solution)/shard_map/ppermute | solution.py:23
  61.6 16.2 %collective-permute-start.14 = (bf16[256,1024]{1,0:T(8,128)(2,1)}, bf16[256,1024]{1,0:T(8,128)(2,1)S(1)}, u32[]{:S(2)}, u32[]{:S(2)}) collective-permute-start(bf16[256,1024]{1,0:T(8,128)(2,1)} %refs_0_.4), channel_id=1, source_target_pairs={{0,64},{64,128},{128,192},{192,0},{1,65},{65,129},{129,193},{193,1... | collective-permute-start | bytes 1572872 | tf_op jit(solution)/shard_map/ppermute | solution.py:28
  61.8 18.3 %collective-permute-start.16 = (bf16[256,1024]{1,0:T(8,128)(2,1)}, bf16[256,1024]{1,0:T(8,128)(2,1)S(1)}, u32[]{:S(2)}, u32[]{:S(2)}) collective-permute-start(bf16[256,1024]{1,0:T(8,128)(2,1)} %refs_0_.4), channel_id=1, source_target_pairs={{0,192},{64,0},{128,64},{192,128},{1,193},{65,1},{129,65},{193,129... | collective-permute-start | bytes 1572872 | tf_op jit(solution)/shard_map/ppermute | solution.py:28
  64.8 19.4 %collective-permute-start.18 = (bf16[256,1024]{1,0:T(8,128)(2,1)}, bf16[256,1024]{1,0:T(8,128)(2,1)S(1)}, u32[]{:S(2)}, u32[]{:S(2)}) collective-permute-start(bf16[256,1024]{1,0:T(8,128)(2,1)} %refs_0_.4), channel_id=1, source_target_pairs={{0,1},{1,0},{2,3},{3,2},{4,5},{5,4},{6,7},{7,6},{8,9},{9,8},{10,11... | collective-permute-start | bytes 1572872 | tf_op jit(solution)/shard_map/ppermute | solution.py:23
  65.7 21.2 %collective-permute-start.29 = (bf16[1024,256]{1,0:T(8,128)(2,1)}, bf16[1024,256]{1,0:T(8,128)(2,1)S(1)}, u32[]{:S(2)}, u32[]{:S(2)}) collective-permute-start(bf16[1024,256]{1,0:T(8,128)(2,1)} %refs_0_.5), channel_id=1, source_target_pairs={{0,64},{64,128},{128,192},{192,0},{1,65},{65,129},{129,193},{193,1... | collective-permute-start | bytes 1572872 | tf_op jit(solution)/shard_map/ppermute | solution.py:28
  69.6 17.9 %all-to-all-start.1 = ((bf16[8,96,128]{2,1,0:T(8,128)(2,1)}), bf16[8,96,128]{2,1,0:T(8,128)(2,1)S(1)}, u32[]{:S(2)}, u32[]{:S(2)}) async-start(bf16[8,96,128]{2,1,0:T(8,128)(2,1)} %shard_map.76), calls=%async_computation.1 | async-start | bytes 393216 | tf_op jit(solution)/shard_map/all_to_all | solution.py:19
  78.6 27.4 %collective-permute-start.15 = (bf16[128,1024]{1,0:T(8,128)(2,1)}, bf16[128,1024]{1,0:T(8,128)(2,1)S(1)}, u32[]{:S(2)}, u32[]{:S(2)}) collective-permute-start(bf16[128,1024]{1,0:T(8,128)(2,1)} %slice.26), channel_id=1, source_target_pairs={{0,64},{64,128},{128,192},{192,0},{1,65},{65,129},{129,193},{193,1... | collective-permute-start | bytes 786440 | tf_op jit(solution)/shard_map/ppermute | solution.py:28
  80.8 25.6 %collective-permute-start.17 = (bf16[128,1024]{1,0:T(8,128)(2,1)}, bf16[128,1024]{1,0:T(8,128)(2,1)}, u32[]{:S(2)}, u32[]{:S(2)}) collective-permute-start(bf16[128,1024]{1,0:T(8,128)(2,1)} %slice.27), channel_id=1, source_target_pairs={{0,192},{64,0},{128,64},{192,128},{1,193},{65,1},{129,65},{193,129... | collective-permute-start | bytes 786440 | tf_op jit(solution)/shard_map/ppermute | solution.py:28
  82.7 26.5 %collective-permute-start.19 = (bf16[256,1024]{1,0:T(8,128)(2,1)S(1)}, bf16[256,1024]{1,0:T(8,128)(2,1)S(1)}, u32[]{:S(2)}, u32[]{:S(2)}) collective-permute-start(bf16[256,1024]{1,0:T(8,128)(2,1)S(1)} %collective-permute-done.14.refs_1_), channel_id=1, source_target_pairs={{0,1},{1,0},{2,3},{3,2},{4,5},{5,4},{6,7},{7,6},{8,9},{9,8},{10,11... | collective-permute-start | bytes 1572872 | tf_op jit(solution)/shard_map/ppermute | solution.py:23
  84.2 25.8 %collective-permute-start.22 = (bf16[256,1024]{1,0:T(8,128)(2,1)S(1)}, bf16[256,1024]{1,0:T(8,128)(2,1)}, u32[]{:S(2)}, u32[]{:S(2)}) collective-permute-start(bf16[256,1024]{1,0:T(8,128)(2,1)S(1)} %collective-permute-done.16.refs_4_), channel_id=1, source_target_pairs={{0,1},{1,0},{2,3},{3,2},{4,5},{5,4},{6,7},{7,6},{8,9},{9,8},{10,11... | collective-permute-start | bytes 1572872 | tf_op jit(solution)/shard_map/ppermute | solution.py:23
  86.9 34.4 %collective-permute-start.31 = (bf16[1024,256]{1,0:T(8,128)(2,1)}, bf16[1024,256]{1,0:T(8,128)(2,1)S(1)}, u32[]{:S(2)}, u32[]{:S(2)}) collective-permute-start(bf16[1024,256]{1,0:T(8,128)(2,1)} %refs_0_.5), channel_id=1, source_target_pairs={{0,192},{64,0},{128,64},{192,128},{1,193},{65,1},{129,65},{193,129... | collective-permute-start | bytes 1572872 | tf_op jit(solution)/shard_map/ppermute | solution.py:28
  88.2 29.0 %all-to-all-start.2 = ((bf16[8,104,128]{2,1,0:T(8,128)(2,1)}), bf16[8,104,128]{2,1,0:T(8,128)(2,1)S(1)}, u32[]{:S(2)}, u32[]{:S(2)}) async-start(bf16[8,104,128]{2,1,0:T(8,128)(2,1)} %get-tuple-element.17), calls=%async_computation.2 | async-start | bytes 425984 | tf_op jit(solution)/shard_map/all_to_all | solution.py:19
  107.6 21.6 %collective-permute-start.30 = (bf16[512,256]{1,0:T(8,128)(2,1)}, bf16[512,256]{1,0:T(8,128)(2,1)S(1)}, u32[]{:S(2)}, u32[]{:S(2)}) collective-permute-start(bf16[512,256]{1,0:T(8,128)(2,1)} %slice.28), channel_id=1, source_target_pairs={{0,64},{64,128},{128,192},{192,0},{1,65},{65,129},{129,193},{193,1... | collective-permute-start | bytes 786440 | tf_op jit(solution)/shard_map/ppermute | solution.py:28
  121.3 8.0 %collective-permute-start.32 = (bf16[512,256]{1,0:T(8,128)(2,1)S(1)}, bf16[512,256]{1,0:T(8,128)(2,1)S(1)}, u32[]{:S(2)}, u32[]{:S(2)}) collective-permute-start(bf16[512,256]{1,0:T(8,128)(2,1)S(1)} %slice.29), channel_id=1, source_target_pairs={{0,192},{64,0},{128,64},{192,128},{1,193},{65,1},{129,65},{193,129... | collective-permute-start | bytes 786440 | tf_op jit(solution)/shard_map/ppermute | solution.py:28
  123.7 18.7 %collective-permute-start.33 = (bf16[1024,256]{1,0:T(8,128)(2,1)}, bf16[1024,256]{1,0:T(8,128)(2,1)S(1)}, u32[]{:S(2)}, u32[]{:S(2)}) collective-permute-start(bf16[1024,256]{1,0:T(8,128)(2,1)} %refs_0_.5), channel_id=1, source_target_pairs={{0,1},{1,0},{2,3},{3,2},{4,5},{5,4},{6,7},{7,6},{8,9},{9,8},{10,11... | collective-permute-start | bytes 1572872 | tf_op jit(solution)/shard_map/ppermute | solution.py:23
  126.2 17.4 %collective-permute-start.34 = (bf16[1024,256]{1,0:T(8,128)(2,1)S(1)}, bf16[1024,256]{1,0:T(8,128)(2,1)S(1)}, u32[]{:S(2)}, u32[]{:S(2)}) collective-permute-start(bf16[1024,256]{1,0:T(8,128)(2,1)S(1)} %collective-permute-done.29.refs_1_), channel_id=1, source_target_pairs={{0,1},{1,0},{2,3},{3,2},{4,5},{5,4},{6,7},{7,6},{8,9},{9,8},{10,11... | collective-permute-start | bytes 1572872 | tf_op jit(solution)/shard_map/ppermute | solution.py:23
  128.1 15.5 %collective-permute-start.37 = (bf16[1024,256]{1,0:T(8,128)(2,1)S(1)}, bf16[1024,256]{1,0:T(8,128)(2,1)S(1)}, u32[]{:S(2)}, u32[]{:S(2)}) collective-permute-start(bf16[1024,256]{1,0:T(8,128)(2,1)S(1)} %collective-permute-done.31.refs_4_), channel_id=1, source_target_pairs={{0,1},{1,0},{2,3},{3,2},{4,5},{5,4},{6,7},{7,6},{8,9},{9,8},{10,11... | collective-permute-start | bytes 1572872 | tf_op jit(solution)/shard_map/ppermute | solution.py:23
  (38 other events, 317.2 us)

commit v5 on v4

--- a/solution.py
+++ b/solution.py
@@ -274,7 +274,7 @@
 
     block = pltpu.VMEM(up_first.shape, BF)
     row = pltpu.VMEM((1, channels), F32)
-    payload, scaled, kept = call(
+    up_own = call(
         up_own_kernel,
         (sds((half, wide)), sds((half, channels)), sds((per_y + 8, LANES), F32)),
         [
@@ -287,7 +287,8 @@
             pltpu.SemaphoreType.DMA((5,)),
         ],
         whole=0,
-    )(tokens, gain_first[None, :], gain_second[None, :], up_first)
+    )
+    payload, scaled, kept = up_own(tokens, gain_first[None, :], gain_second[None, :], up_first)
     payload = call(
         up_other_kernel,
         sds((half, wide)),

time: 183 us -> 183 us (level)
  no operation moved by 1% of the time
where the time goes in v5:
time: 183 us
  starting transfers between devices  79.3 us (43%)
  waiting for transfers between devices  53.6 us (29%)
  blocking collectives  28.3 us (15%)
  Pallas kernels  15.8 us (9%)
  local copies, waits for them, and re-layouts  5.42 us (3%)
    ppermute x12, waiting for transfers between devices, along_y(): return lax.ppermute(a, 'y', [(i, (i + shift) % n) for i in range(n)])  34.3 us
    all_to_all x3, starting transfers between devices, exchange(): return lax.all_to_all(parts, axis, 0, 0, tiled=True)  31.1 us
    all_to_all x2, blocking collectives, exchange(): return lax.all_to_all(parts, axis, 0, 0, tiled=True)  28.3 us
    ppermute x17, starting transfers between devices, from_other_core(): return lax.ppermute(w, 'c', [(0, 1), (1, 0)])  24.4 us
    pallas_call x10, Pallas kernels, run(): pl.pallas_call(kernel, out_shape=out, in_specs=[vmem] * first + [lies] *...  15.8 us
    ppermute x12, starting transfers between devices, along_y(): return lax.ppermute(a, 'y', [(i, (i + shift) % n) for i in range(n)])  13 us
    ppermute x9, waiting for transfers between devices, along_x(): return lax.ppermute(a, 'x', [(i, (i + shift) % n) for i in range(n)])  9.47 us
    ppermute x9, starting transfers between devices, along_x(): return lax.ppermute(a, 'x', [(i, (i + shift) % n) for i in range(n)])  9.4 us
  transfers between devices with their start and end apart: 43, of which 14 were waited for; matrix products, arithmetic and copies ran while one was open for 1% of the time, Pallas kernels for 6%

profile of v5, /device:TPU:1, one launch (start us, length us, event | category | flops | bytes accessed | tf_op | source)
XLA Modules:
  0.0 182.9 jit_solution(12203060344522056616)
XLA Ops:
  0.0 3.2 %collective-permute-start = (bf16[256,1024]{1,0:T(8,128)(2,1)}, bf16[256,1024]{1,0:T(8,128)(2,1)S(1)}, u32[]{:S(2)}, u32[]{:S(2)}) collective-permute-start(bf16[256,1024]{1,0:T(8,128)(2,1)} %own.1), channel_id=1, source_target_pairs={{0,1},{1,0},{2,3},{3,2},{4,5},{5,4},{6,7},{7,6},{8,9},{9,8},{10,11... | collective-permute-start | bytes 1572872 | tf_op jit(solution)/shard_map/ppermute | solution.py:23
  3.2 2.8 %shard_map.73 = (bf16[384,2176]{1,0:T(8,128)(2,1)}, bf16[384,256]{1,0:T(8,128)(2,1)S(1)}, f32[104,128]{1,0:T(8,128)S(1)}) custom-call(bf16[768,256]{1,0:T(8,128)(2,1)} %tokens.1, f32[1,256]{1,0:T(1,128)} %bitcast.3, f32[1,256]{1,0:T(1,128)} %bitcast.4, bf16[256,1024]{1,0:T(8,128)(2,1)} %own.1), custom_call_target="tpu_custom_call" | custom-call | tf_op jit(solution)/shard_map/pallas_call | solution.py:50
  7.4 5.2 %all-to-all-start = ((bf16[16,24,2176]{2,1,0:T(8,128)(2,1)}), bf16[16,24,2176]{2,1,0:T(8,128)(2,1)S(1)}, u32[]{:S(2)}, u32[]{:S(2)}) async-start(bf16[16,24,2176]{2,1,0:T(8,128)(2,1)} %bitcast.2), calls=%async_computation | async-start | bytes 3342336 | tf_op jit(solution)/shard_map/all_to_all | solution.py:19
  16.3 28.8 %collective-permute-done.4.refs_1_ = bf16[1024,256]{1,0:T(8,128)(2,1)S(1)} collective-permute-done((bf16[1024,256]{1,0:T(8,128)(2,1)S(1)}, bf16[1024,256]{1,0:T(8,128)(2,1)S(1)}, u32[]{:S(2)}, u32[]{:S(2)}) %collective-permute-start.4) | collective-permute-done | bytes 524320 | tf_op jit(solution)/shard_map/ppermute | solution.py:28
  45.2 2.7 %collective-permute-start.7 = (bf16[512,256]{1,0:T(8,128)(2,1)S(1)}, bf16[512,256]{1,0:T(8,128)(2,1)}, u32[]{:S(2)}, u32[]{:S(2)}) collective-permute-start(bf16[512,256]{1,0:T(8,128)(2,1)S(1)} %slice.25), channel_id=1, source_target_pairs={{0,192},{64,0},{128,64},{192,128},{1,193},{65,1},{129,65},{193,129... | collective-permute-start | bytes 786440 | tf_op jit(solution)/shard_map/ppermute | solution.py:28
  49.7 3.6 %collective-permute-done.5.refs_2_ = bf16[512,256]{1,0:T(8,128)(2,1)} collective-permute-done((bf16[512,256]{1,0:T(8,128)(2,1)S(1)}, bf16[512,256]{1,0:T(8,128)(2,1)}, u32[]{:S(2)}, u32[]{:S(2)}) %collective-permute-start.5) | collective-permute-done | bytes 262176 | tf_op jit(solution)/shard_map/ppermute | solution.py:28
  53.2 2.0 %collective-permute-start.10 = (bf16[512,256]{1,0:T(8,128)(2,1)}, bf16[512,256]{1,0:T(8,128)(2,1)}, u32[]{:S(2)}, u32[]{:S(2)}) collective-permute-start(bf16[512,256]{1,0:T(8,128)(2,1)} %collective-permute-done.5.refs_2_), channel_id=1, source_target_pairs={{0,1},{1,0},{2,3},{3,2},{4,5},{5,4},{6,7},{7,6},{8,9},{9,8},{10,11... | collective-permute-start | bytes 786440 | tf_op jit(solution)/shard_map/ppermute | solution.py:23
  57.4 2.7 %collective-permute-start.2 = (bf16[24,2048]{1,0:T(8,128)(2,1)S(1)}, bf16[24,2048]{1,0:T(8,128)(2,1)S(1)}, u32[]{:S(2)}, u32[]{:S(2)}) collective-permute-start(bf16[24,2048]{1,0:T(8,128)(2,1)S(1)} %shard_map.75), channel_id=1, source_target_pairs={{0,32},{16,48},{32,0},{48,16},{1,33},{17,49},{33,1},{49,17},{2,34}... | collective-permute-start | bytes 294920 | tf_op jit(solution)/shard_map/ppermute | solution.py:33
  61.8 2.6 %collective-permute-start.16 = (bf16[256,1024]{1,0:T(8,128)(2,1)}, bf16[256,1024]{1,0:T(8,128)(2,1)S(1)}, u32[]{:S(2)}, u32[]{:S(2)}) collective-permute-start(bf16[256,1024]{1,0:T(8,128)(2,1)} %refs_0_.4), channel_id=1, source_target_pairs={{0,192},{64,0},{128,64},{192,128},{1,193},{65,1},{129,65},{193,129... | collective-permute-start | bytes 1572872 | tf_op jit(solution)/shard_map/ppermute | solution.py:28
  65.8 3.8 %shard_map.76 = bf16[8,96,128]{2,1,0:T(8,128)(2,1)} custom-call(bf16[96,2048]{1,0:T(8,128)(2,1)S(1)} %pad_maximum_fusion.hidden, bf16[1024,256]{1,0:T(8,128)(2,1)} %refs_0_.3, bf16[1024,256]{1,0:T(8,128)(2,1)} %copy-done.4, bf16[512,256]{1,0:T(8,128)(2,1)} %collective-permute-done.5.refs_2_, bf16[512,256]{1,0:T(8,128)(2,1)} %collective-permute-done.7.refs_3_, ...), custom_call_target="tpu_custom_call" | custom-call | tf_op jit(solution)/shard_map/pallas_call | solution.py:50
  69.6 8.2 %all-to-all-start.1 = ((bf16[8,96,128]{2,1,0:T(8,128)(2,1)}), bf16[8,96,128]{2,1,0:T(8,128)(2,1)S(1)}, u32[]{:S(2)}, u32[]{:S(2)}) async-start(bf16[8,96,128]{2,1,0:T(8,128)(2,1)} %shard_map.76), calls=%async_computation.1 | async-start | bytes 393216 | tf_op jit(solution)/shard_map/all_to_all | solution.py:19
  85.0 2.0 %collective-permute-done.29.refs_1_ = bf16[1024,256]{1,0:T(8,128)(2,1)S(1)} collective-permute-done((bf16[1024,256]{1,0:T(8,128)(2,1)}, bf16[1024,256]{1,0:T(8,128)(2,1)S(1)}, u32[]{:S(2)}, u32[]{:S(2)}) %collective-permute-start.29) | collective-permute-done | bytes 524320 | tf_op jit(solution)/shard_map/ppermute | solution.py:28
  88.2 17.8 %all-to-all-start.2 = ((bf16[8,104,128]{2,1,0:T(8,128)(2,1)}), bf16[8,104,128]{2,1,0:T(8,128)(2,1)S(1)}, u32[]{:S(2)}, u32[]{:S(2)}) async-start(bf16[8,104,128]{2,1,0:T(8,128)(2,1)} %get-tuple-element.17), calls=%async_computation.2 | async-start | bytes 425984 | tf_op jit(solution)/shard_map/all_to_all | solution.py:19
  109.9 7.3 %all-to-all-done.2.x = bf16[8,104,128]{2,1,0:T(8,128)(2,1)S(1)} async-done(((bf16[8,104,128]{2,1,0:T(8,128)(2,1)}), bf16[8,104,128]{2,1,0:T(8,128)(2,1)S(1)}, u32[]{:S(2)}, u32[]{:S(2)}) %all-to-all-start.2) | async-done | bytes 213024 | tf_op jit(solution)/shard_map/all_to_all | solution.py:19
  117.2 2.5 %shard_map.78 = (bf16[24,2176]{1,0:T(8,128)(2,1)S(1)}, bf16[24,2176]{1,0:T(8,128)(2,1)S(1)}, bf16[24,2176]{1,0:T(8,128)(2,1)S(1)}, bf16[24,2176]{1,0:T(8,128)(2,1)S(1)}) custom-call(bf16[8,104,128]{2,1,0:T(8,128)(2,1)S(1)} %all-to-all-done.2.x, bf16[256,1024]{1,0:T(8,128)(2,1)} %refs_0_.4, bf16[256,1024]{1,0:T(8,128)(2,1)} %copy-done.2, ...), custom_call_target="tpu_custom_call" | custom-call | tf_op jit(solution)/shard_map/pallas_call | solution.py:50
  121.4 2.3 %collective-permute-done.23.refs_1_ = bf16[24,2176]{1,0:T(8,128)(2,1)S(1)} collective-permute-done((bf16[24,2176]{1,0:T(8,128)(2,1)S(1)}, bf16[24,2176]{1,0:T(8,128)(2,1)S(1)}, u32[]{:S(2)}, u32[]{:S(2)}) %collective-permute-start.23) | collective-permute-done | bytes 104480 | tf_op jit(solution)/shard_map/ppermute | solution.py:33
  123.7 2.4 %collective-permute-start.33 = (bf16[1024,256]{1,0:T(8,128)(2,1)}, bf16[1024,256]{1,0:T(8,128)(2,1)S(1)}, u32[]{:S(2)}, u32[]{:S(2)}) collective-permute-start(bf16[1024,256]{1,0:T(8,128)(2,1)} %refs_0_.5), channel_id=1, source_target_pairs={{0,1},{1,0},{2,3},{3,2},{4,5},{5,4},{6,7},{7,6},{8,9},{9,8},{10,11... | collective-permute-start | bytes 1572872 | tf_op jit(solution)/shard_map/ppermute | solution.py:23
  129.3 2.3 %collective-permute-start.27 = (bf16[24,2048]{1,0:T(8,128)(2,1)S(1)}, bf16[24,2048]{1,0:T(8,128)(2,1)S(1)}, u32[]{:S(2)}, u32[]{:S(2)}) collective-permute-start(bf16[24,2048]{1,0:T(8,128)(2,1)S(1)} %shard_map.79), channel_id=1, source_target_pairs={{0,32},{16,48},{32,0},{48,16},{1,33},{17,49},{33,1},{49,17},{2,34}... | collective-permute-start | bytes 294920 | tf_op jit(solution)/shard_map/ppermute | solution.py:33
  131.6 3.8 %collective-permute-done.26 = bf16[24,2048]{1,0:T(8,128)(2,1)S(1)} collective-permute-done((bf16[24,2048]{1,0:T(8,128)(2,1)S(1)}, bf16[24,2048]{1,0:T(8,128)(2,1)S(1)}, u32[]{:S(2)}, u32[]{:S(2)}) %collective-permute-start.26) | collective-permute-done | bytes 98336 | tf_op jit(solution)/shard_map/ppermute | solution.py:33
  138.9 3.5 %collective-permute-start.36 = (bf16[512,256]{1,0:T(8,128)(2,1)S(1)}, bf16[512,256]{1,0:T(8,128)(2,1)S(1)}, u32[]{:S(2)}, u32[]{:S(2)}) collective-permute-start(bf16[512,256]{1,0:T(8,128)(2,1)S(1)} %collective-permute-done.32.refs_3_), channel_id=1, source_target_pairs={{0,1},{1,0},{2,3},{3,2},{4,5},{5,4},{6,7},{7,6},{8,9},{9,8},{10,11... | collective-permute-start | bytes 786440 | tf_op jit(solution)/shard_map/ppermute | solution.py:23
  145.3 3.1 %shard_map.80 = bf16[8,96,128]{2,1,0:T(8,128)(2,1)S(1)} custom-call(bf16[96,2048]{1,0:T(8,128)(2,1)S(1)} %pad_maximum_fusion.1.hidden, bf16[1024,256]{1,0:T(8,128)(2,1)} %refs_0_.5, bf16[1024,256]{1,0:T(8,128)(2,1)} %copy-done, bf16[512,256]{1,0:T(8,128)(2,1)} %copy-done.12, bf16[512,256]{1,0:T(8,128)(2,1)} %copy-done.14, bf16[1024,256]{1,0:T(8,128)(2,1)} %copy-done.1, ...), custom_call_target="tpu_custom_call" | custom-call | tf_op jit(solution)/shard_map/pallas_call | solution.py:50
  148.4 12.4 %all_to_all.25.parts = bf16[8,96,128]{2,1,0:T(8,128)(2,1)S(1)} all-to-all(bf16[8,96,128]{2,1,0:T(8,128)(2,1)S(1)} %shard_map.80), channel_id=1, replica_groups=mesh['y'=4,'x'=4,'z'=8,'c'=2] {'z'}, dimensions={0} | all-to-all | bytes 393216 | tf_op jit(solution)/shard_map/all_to_all | solution.py:19
  161.6 15.9 %all_to_all.26.own = bf16[8,96,128]{2,1,0:T(8,128)(2,1)S(1)} all-to-all(bf16[8,96,128]{2,1,0:T(8,128)(2,1)S(1)} %broadcast_in_dim.14), channel_id=1, replica_groups=mesh['y'=4,'x'=4,'z'=8,'c'=2] {'z'}, dimensions={0} | all-to-all | bytes 393216 | tf_op jit(solution)/shard_map/all_to_all | solution.py:19
  177.4 3.5 %collective-permute-start.39 = (bf16[8,96,128]{2,1,0:T(8,128)(2,1)S(1)}, bf16[8,96,128]{2,1,0:T(8,128)(2,1)S(1)}, u32[]{:S(2)}, u32[]{:S(2)}) collective-permute-start(bf16[8,96,128]{2,1,0:T(8,128)(2,1)S(1)} %all_to_all.26.own), channel_id=1, source_target_pairs={{0,1},{1,0},{2,3},{3,2},{4,5},{5,4},{6,7},{7,6},{8,9},{9,8},{10,11... | collective-permute-start | bytes 589832 | tf_op jit(solution)/shard_map/ppermute | solution.py:23
  (121 shorter events, 38.1 us)
Async XLA Ops:
  7.4 48.3 %all-to-all-start = ((bf16[16,24,2176]{2,1,0:T(8,128)(2,1)}), bf16[16,24,2176]{2,1,0:T(8,128)(2,1)S(1)}, u32[]{:S(2)}, u32[]{:S(2)}) async-start(bf16[16,24,2176]{2,1,0:T(8,128)(2,1)} %bitcast.2), calls=%async_computation | async-start | bytes 3342336 | tf_op jit(solution)/shard_map/all_to_all | solution.py:19
  12.7 32.4 %collective-permute-start.4 = (bf16[1024,256]{1,0:T(8,128)(2,1)S(1)}, bf16[1024,256]{1,0:T(8,128)(2,1)S(1)}, u32[]{:S(2)}, u32[]{:S(2)}) collective-permute-start(bf16[1024,256]{1,0:T(8,128)(2,1)S(1)} %copy-done.6), channel_id=1, source_target_pairs={{0,64},{64,128},{128,192},{192,0},{1,65},{65,129},{129,193},{193,1... | collective-permute-start | bytes 1572872 | tf_op jit(solution)/shard_map/ppermute | solution.py:28
  14.1 31.1 %collective-permute-start.6 = (bf16[1024,256]{1,0:T(8,128)(2,1)S(1)}, bf16[1024,256]{1,0:T(8,128)(2,1)S(1)}, u32[]{:S(2)}, u32[]{:S(2)}) collective-permute-start(bf16[1024,256]{1,0:T(8,128)(2,1)S(1)} %copy-done.6), channel_id=1, source_target_pairs={{0,192},{64,0},{128,64},{192,128},{1,193},{65,1},{129,65},{193,129... | collective-permute-start | bytes 1572872 | tf_op jit(solution)/shard_map/ppermute | solution.py:28
  15.4 40.7 %collective-permute-start.8 = (bf16[1024,256]{1,0:T(8,128)(2,1)S(1)}, bf16[1024,256]{1,0:T(8,128)(2,1)}, u32[]{:S(2)}, u32[]{:S(2)}) collective-permute-start(bf16[1024,256]{1,0:T(8,128)(2,1)S(1)} %copy-done.6), channel_id=1, source_target_pairs={{0,1},{1,0},{2,3},{3,2},{4,5},{5,4},{6,7},{7,6},{8,9},{9,8},{10,11... | collective-permute-start | bytes 1572872 | tf_op jit(solution)/shard_map/ppermute | solution.py:23
  45.1 8.1 %collective-permute-start.5 = (bf16[512,256]{1,0:T(8,128)(2,1)S(1)}, bf16[512,256]{1,0:T(8,128)(2,1)}, u32[]{:S(2)}, u32[]{:S(2)}) collective-permute-start(bf16[512,256]{1,0:T(8,128)(2,1)S(1)} %slice.24), channel_id=1, source_target_pairs={{0,64},{64,128},{128,192},{192,0},{1,65},{65,129},{129,193},{193,1... | collective-permute-start | bytes 786440 | tf_op jit(solution)/shard_map/ppermute | solution.py:28
  45.2 10.0 %collective-permute-start.7 = (bf16[512,256]{1,0:T(8,128)(2,1)S(1)}, bf16[512,256]{1,0:T(8,128)(2,1)}, u32[]{:S(2)}, u32[]{:S(2)}) collective-permute-start(bf16[512,256]{1,0:T(8,128)(2,1)S(1)} %slice.25), channel_id=1, source_target_pairs={{0,192},{64,0},{128,64},{192,128},{1,193},{65,1},{129,65},{193,129... | collective-permute-start | bytes 786440 | tf_op jit(solution)/shard_map/ppermute | solution.py:28
  48.0 13.7 %collective-permute-start.12 = (bf16[1024,256]{1,0:T(8,128)(2,1)S(1)}, bf16[1024,256]{1,0:T(8,128)(2,1)}, u32[]{:S(2)}, u32[]{:S(2)}) collective-permute-start(bf16[1024,256]{1,0:T(8,128)(2,1)S(1)} %collective-permute-done.6.refs_4_), channel_id=1, source_target_pairs={{0,1},{1,0},{2,3},{3,2},{4,5},{5,4},{6,7},{7,6},{8,9},{9,8},{10,11... | collective-permute-start | bytes 1572872 | tf_op jit(solution)/shard_map/ppermute | solution.py:23
  55.2 10.6 %collective-permute-start.9 = (bf16[1024,256]{1,0:T(8,128)(2,1)S(1)}, bf16[1024,256]{1,0:T(8,128)(2,1)}, u32[]{:S(2)}, u32[]{:S(2)}) collective-permute-start(bf16[1024,256]{1,0:T(8,128)(2,1)S(1)} %collective-permute-done.4.refs_1_), channel_id=1, source_target_pairs={{0,1},{1,0},{2,3},{3,2},{4,5},{5,4},{6,7},{7,6},{8,9},{9,8},{10,11... | collective-permute-start | bytes 1572872 | tf_op jit(solution)/shard_map/ppermute | solution.py:23
  61.6 16.2 %collective-permute-start.14 = (bf16[256,1024]{1,0:T(8,128)(2,1)}, bf16[256,1024]{1,0:T(8,128)(2,1)S(1)}, u32[]{:S(2)}, u32[]{:S(2)}) collective-permute-start(bf16[256,1024]{1,0:T(8,128)(2,1)} %refs_0_.4), channel_id=1, source_target_pairs={{0,64},{64,128},{128,192},{192,0},{1,65},{65,129},{129,193},{193,1... | collective-permute-start | bytes 1572872 | tf_op jit(solution)/shard_map/ppermute | solution.py:28
  61.8 18.3 %collective-permute-start.16 = (bf16[256,1024]{1,0:T(8,128)(2,1)}, bf16[256,1024]{1,0:T(8,128)(2,1)S(1)}, u32[]{:S(2)}, u32[]{:S(2)}) collective-permute-start(bf16[256,1024]{1,0:T(8,128)(2,1)} %refs_0_.4), channel_id=1, source_target_pairs={{0,192},{64,0},{128,64},{192,128},{1,193},{65,1},{129,65},{193,129... | collective-permute-start | bytes 1572872 | tf_op jit(solution)/shard_map/ppermute | solution.py:28
  64.8 19.4 %collective-permute-start.18 = (bf16[256,1024]{1,0:T(8,128)(2,1)}, bf16[256,1024]{1,0:T(8,128)(2,1)S(1)}, u32[]{:S(2)}, u32[]{:S(2)}) collective-permute-start(bf16[256,1024]{1,0:T(8,128)(2,1)} %refs_0_.4), channel_id=1, source_target_pairs={{0,1},{1,0},{2,3},{3,2},{4,5},{5,4},{6,7},{7,6},{8,9},{9,8},{10,11... | collective-permute-start | bytes 1572872 | tf_op jit(solution)/shard_map/ppermute | solution.py:23
  65.7 21.2 %collective-permute-start.29 = (bf16[1024,256]{1,0:T(8,128)(2,1)}, bf16[1024,256]{1,0:T(8,128)(2,1)S(1)}, u32[]{:S(2)}, u32[]{:S(2)}) collective-permute-start(bf16[1024,256]{1,0:T(8,128)(2,1)} %refs_0_.5), channel_id=1, source_target_pairs={{0,64},{64,128},{128,192},{192,0},{1,65},{65,129},{129,193},{193,1... | collective-permute-start | bytes 1572872 | tf_op jit(solution)/shard_map/ppermute | solution.py:28
  69.6 17.9 %all-to-all-start.1 = ((bf16[8,96,128]{2,1,0:T(8,128)(2,1)}), bf16[8,96,128]{2,1,0:T(8,128)(2,1)S(1)}, u32[]{:S(2)}, u32[]{:S(2)}) async-start(bf16[8,96,128]{2,1,0:T(8,128)(2,1)} %shard_map.76), calls=%async_computation.1 | async-start | bytes 393216 | tf_op jit(solution)/shard_map/all_to_all | solution.py:19
  78.6 27.4 %collective-permute-start.15 = (bf16[128,1024]{1,0:T(8,128)(2,1)}, bf16[128,1024]{1,0:T(8,128)(2,1)S(1)}, u32[]{:S(2)}, u32[]{:S(2)}) collective-permute-start(bf16[128,1024]{1,0:T(8,128)(2,1)} %slice.26), channel_id=1, source_target_pairs={{0,64},{64,128},{128,192},{192,0},{1,65},{65,129},{129,193},{193,1... | collective-permute-start | bytes 786440 | tf_op jit(solution)/shard_map/ppermute | solution.py:28
  80.8 25.6 %collective-permute-start.17 = (bf16[128,1024]{1,0:T(8,128)(2,1)}, bf16[128,1024]{1,0:T(8,128)(2,1)}, u32[]{:S(2)}, u32[]{:S(2)}) collective-permute-start(bf16[128,1024]{1,0:T(8,128)(2,1)} %slice.27), channel_id=1, source_target_pairs={{0,192},{64,0},{128,64},{192,128},{1,193},{65,1},{129,65},{193,129... | collective-permute-start | bytes 786440 | tf_op jit(solution)/shard_map/ppermute | solution.py:28
  82.7 26.5 %collective-permute-start.19 = (bf16[256,1024]{1,0:T(8,128)(2,1)S(1)}, bf16[256,1024]{1,0:T(8,128)(2,1)S(1)}, u32[]{:S(2)}, u32[]{:S(2)}) collective-permute-start(bf16[256,1024]{1,0:T(8,128)(2,1)S(1)} %collective-permute-done.14.refs_1_), channel_id=1, source_target_pairs={{0,1},{1,0},{2,3},{3,2},{4,5},{5,4},{6,7},{7,6},{8,9},{9,8},{10,11... | collective-permute-start | bytes 1572872 | tf_op jit(solution)/shard_map/ppermute | solution.py:23
  84.2 25.8 %collective-permute-start.22 = (bf16[256,1024]{1,0:T(8,128)(2,1)S(1)}, bf16[256,1024]{1,0:T(8,128)(2,1)}, u32[]{:S(2)}, u32[]{:S(2)}) collective-permute-start(bf16[256,1024]{1,0:T(8,128)(2,1)S(1)} %collective-permute-done.16.refs_4_), channel_id=1, source_target_pairs={{0,1},{1,0},{2,3},{3,2},{4,5},{5,4},{6,7},{7,6},{8,9},{9,8},{10,11... | collective-permute-start | bytes 1572872 | tf_op jit(solution)/shard_map/ppermute | solution.py:23
  86.9 34.4 %collective-permute-start.31 = (bf16[1024,256]{1,0:T(8,128)(2,1)}, bf16[1024,256]{1,0:T(8,128)(2,1)S(1)}, u32[]{:S(2)}, u32[]{:S(2)}) collective-permute-start(bf16[1024,256]{1,0:T(8,128)(2,1)} %refs_0_.5), channel_id=1, source_target_pairs={{0,192},{64,0},{128,64},{192,128},{1,193},{65,1},{129,65},{193,129... | collective-permute-start | bytes 1572872 | tf_op jit(solution)/shard_map/ppermute | solution.py:28
  88.2 29.0 %all-to-all-start.2 = ((bf16[8,104,128]{2,1,0:T(8,128)(2,1)}), bf16[8,104,128]{2,1,0:T(8,128)(2,1)S(1)}, u32[]{:S(2)}, u32[]{:S(2)}) async-start(bf16[8,104,128]{2,1,0:T(8,128)(2,1)} %get-tuple-element.17), calls=%async_computation.2 | async-start | bytes 425984 | tf_op jit(solution)/shard_map/all_to_all | solution.py:19
  107.6 21.6 %collective-permute-start.30 = (bf16[512,256]{1,0:T(8,128)(2,1)}, bf16[512,256]{1,0:T(8,128)(2,1)S(1)}, u32[]{:S(2)}, u32[]{:S(2)}) collective-permute-start(bf16[512,256]{1,0:T(8,128)(2,1)} %slice.28), channel_id=1, source_target_pairs={{0,64},{64,128},{128,192},{192,0},{1,65},{65,129},{129,193},{193,1... | collective-permute-start | bytes 786440 | tf_op jit(solution)/shard_map/ppermute | solution.py:28
  121.3 8.0 %collective-permute-start.32 = (bf16[512,256]{1,0:T(8,128)(2,1)S(1)}, bf16[512,256]{1,0:T(8,128)(2,1)S(1)}, u32[]{:S(2)}, u32[]{:S(2)}) collective-permute-start(bf16[512,256]{1,0:T(8,128)(2,1)S(1)} %slice.29), channel_id=1, source_target_pairs={{0,192},{64,0},{128,64},{192,128},{1,193},{65,1},{129,65},{193,129... | collective-permute-start | bytes 786440 | tf_op jit(solution)/shard_map/ppermute | solution.py:28
  123.7 18.7 %collective-permute-start.33 = (bf16[1024,256]{1,0:T(8,128)(2,1)}, bf16[1024,256]{1,0:T(8,128)(2,1)S(1)}, u32[]{:S(2)}, u32[]{:S(2)}) collective-permute-start(bf16[1024,256]{1,0:T(8,128)(2,1)} %refs_0_.5), channel_id=1, source_target_pairs={{0,1},{1,0},{2,3},{3,2},{4,5},{5,4},{6,7},{7,6},{8,9},{9,8},{10,11... | collective-permute-start | bytes 1572872 | tf_op jit(solution)/shard_map/ppermute | solution.py:23
  126.2 17.4 %collective-permute-start.34 = (bf16[1024,256]{1,0:T(8,128)(2,1)S(1)}, bf16[1024,256]{1,0:T(8,128)(2,1)S(1)}, u32[]{:S(2)}, u32[]{:S(2)}) collective-permute-start(bf16[1024,256]{1,0:T(8,128)(2,1)S(1)} %collective-permute-done.29.refs_1_), channel_id=1, source_target_pairs={{0,1},{1,0},{2,3},{3,2},{4,5},{5,4},{6,7},{7,6},{8,9},{9,8},{10,11... | collective-permute-start | bytes 1572872 | tf_op jit(solution)/shard_map/ppermute | solution.py:23
  128.1 15.5 %collective-permute-start.37 = (bf16[1024,256]{1,0:T(8,128)(2,1)S(1)}, bf16[1024,256]{1,0:T(8,128)(2,1)S(1)}, u32[]{:S(2)}, u32[]{:S(2)}) collective-permute-start(bf16[1024,256]{1,0:T(8,128)(2,1)S(1)} %collective-permute-done.31.refs_4_), channel_id=1, source_target_pairs={{0,1},{1,0},{2,3},{3,2},{4,5},{5,4},{6,7},{7,6},{8,9},{9,8},{10,11... | collective-permute-start | bytes 1572872 | tf_op jit(solution)/shard_map/ppermute | solution.py:23
  (38 other events, 317.2 us)

commit v6 on v5

--- a/solution.py
+++ b/solution.py
@@ -251,8 +251,13 @@
     return [w, *moved, swapped] + [from_other_core(v) for v in moved]
 
 
+def far_first(n):
+    return sorted(range(1, n), key=lambda j: -min(j, n - j))
+
+
 def from_x_ring(hidden, nx):
-    return jnp.concatenate([hidden] + [along_x(hidden, j) for j in range(1, nx)], axis=0)
+    moved = {j: along_x(hidden, j) for j in far_first(nx)}
+    return jnp.concatenate([hidden] + [moved[j] for j in range(1, nx)], axis=0)
 
 
 def body(tokens, gain_first, up_first, down_first, gain_second, up_second, down_second):
@@ -307,12 +312,11 @@
     ups = around(up_second, swapped[1])
     branch = exchange(branch, "z")
     downs = around(down_second, swapped[2])
-    middle, payload = call(finish_first_kernel, (sds((per_y, LANES)), sds((nz, per_y + 8, LANES))))(
-        branch, kept
-    )
+    finish_first = call(finish_first_kernel, (sds((per_y, LANES)), sds((nz, per_y + 8, LANES))))
+    middle, payload = finish_first(branch, kept)
     payload = exchange(payload, "z")
     parts = call(up_second_kernel, (sds((few, wide)),) * nx, held(up_second), whole=1)(payload, *ups)
-    parts = [parts[0]] + [along_x(parts[j], nx - j) for j in range(1, nx)]
+    parts = [parts[0]] + [along_x(parts[j], nx - j) for j in far_first(nx)]
     hidden = activate(*parts)
     hidden = from_x_ring(hidden, nx)
     branch = call(down_kernel, down_out, held(down_second), whole=1)(hidden, *downs)

time: 183 us -> 183 us (level)
  waiting for transfers between devices: 53.6 us -> 56.7 us
  starting transfers between devices: 79.3 us -> 76.2 us
    ppermute x9, waiting for transfers between devices: 9.47 us -> 12.6 us  [along_x(): return lax.ppermute(a, 'x', [(i, (i + shift) % n) for i in range(n)])]
    ppermute x17, starting transfers between devices: 24.4 us -> 21.3 us  [from_other_core(): return lax.ppermute(w, 'c', [(0, 1), (1, 0)])]
  transfers between devices with their start and end apart: 43 -> 43, of which waited for: 14 -> 13; matrix products, arithmetic and copies ran while one was open for 1% -> 1% of each run, Pallas kernels for 6% -> 6%
where the time goes in v6:
time: 183 us
  starting transfers between devices  76.2 us (42%)
  waiting for transfers between devices  56.7 us (31%)
  blocking collectives  28.3 us (15%)
  Pallas kernels  15.8 us (9%)
  local copies, waits for them, and re-layouts  5.42 us (3%)
    ppermute x12, waiting for transfers between devices, along_y(): return lax.ppermute(a, 'y', [(i, (i + shift) % n) for i in range(n)])  34.3 us
    all_to_all x3, starting transfers between devices, exchange(): return lax.all_to_all(parts, axis, 0, 0, tiled=True)  31.1 us
    all_to_all x2, blocking collectives, exchange(): return lax.all_to_all(parts, axis, 0, 0, tiled=True)  28.3 us
    ppermute x17, starting transfers between devices, from_other_core(): return lax.ppermute(w, 'c', [(0, 1), (1, 0)])  21.3 us
    pallas_call x10, Pallas kernels, run(): pl.pallas_call(kernel, out_shape=out, in_specs=[vmem] * first + [lies] *...  15.8 us
    ppermute x12, starting transfers between devices, along_y(): return lax.ppermute(a, 'y', [(i, (i + shift) % n) for i in range(n)])  13 us
    ppermute x9, waiting for transfers between devices, along_x(): return lax.ppermute(a, 'x', [(i, (i + shift) % n) for i in range(n)])  12.6 us
    ppermute x9, starting transfers between devices, along_x(): return lax.ppermute(a, 'x', [(i, (i + shift) % n) for i in range(n)])  9.33 us
  transfers between devices with their start and end apart: 43, of which 13 were waited for; matrix products, arithmetic and copies ran while one was open for 1% of the time, Pallas kernels for 6%

profile of v6, /device:TPU:1, one launch (start us, length us, event | category | flops | bytes accessed | tf_op | source)
XLA Modules:
  0.0 182.9 jit_solution(1266768614805573926)
XLA Ops:
  0.0 3.2 %collective-permute-start = (bf16[256,1024]{1,0:T(8,128)(2,1)}, bf16[256,1024]{1,0:T(8,128)(2,1)S(1)}, u32[]{:S(2)}, u32[]{:S(2)}) collective-permute-start(bf16[256,1024]{1,0:T(8,128)(2,1)} %own.1), channel_id=1, source_target_pairs={{0,1},{1,0},{2,3},{3,2},{4,5},{5,4},{6,7},{7,6},{8,9},{9,8},{10,11... | collective-permute-start | bytes 1572872 | tf_op jit(solution)/shard_map/ppermute | solution.py:23
  3.2 2.8 %shard_map.73 = (bf16[384,2176]{1,0:T(8,128)(2,1)}, bf16[384,256]{1,0:T(8,128)(2,1)S(1)}, f32[104,128]{1,0:T(8,128)S(1)}) custom-call(bf16[768,256]{1,0:T(8,128)(2,1)} %tokens.1, f32[1,256]{1,0:T(1,128)} %bitcast.3, f32[1,256]{1,0:T(1,128)} %bitcast.4, bf16[256,1024]{1,0:T(8,128)(2,1)} %own.1), custom_call_target="tpu_custom_call" | custom-call | tf_op jit(solution)/shard_map/pallas_call | solution.py:50
  7.4 5.2 %all-to-all-start = ((bf16[16,24,2176]{2,1,0:T(8,128)(2,1)}), bf16[16,24,2176]{2,1,0:T(8,128)(2,1)S(1)}, u32[]{:S(2)}, u32[]{:S(2)}) async-start(bf16[16,24,2176]{2,1,0:T(8,128)(2,1)} %bitcast.2), calls=%async_computation | async-start | bytes 3342336 | tf_op jit(solution)/shard_map/all_to_all | solution.py:19
  16.3 28.8 %collective-permute-done.4.refs_1_ = bf16[1024,256]{1,0:T(8,128)(2,1)S(1)} collective-permute-done((bf16[1024,256]{1,0:T(8,128)(2,1)S(1)}, bf16[1024,256]{1,0:T(8,128)(2,1)S(1)}, u32[]{:S(2)}, u32[]{:S(2)}) %collective-permute-start.4) | collective-permute-done | bytes 524320 | tf_op jit(solution)/shard_map/ppermute | solution.py:28
  45.2 2.7 %collective-permute-start.7 = (bf16[512,256]{1,0:T(8,128)(2,1)S(1)}, bf16[512,256]{1,0:T(8,128)(2,1)}, u32[]{:S(2)}, u32[]{:S(2)}) collective-permute-start(bf16[512,256]{1,0:T(8,128)(2,1)S(1)} %slice.25), channel_id=1, source_target_pairs={{0,192},{64,0},{128,64},{192,128},{1,193},{65,1},{129,65},{193,129... | collective-permute-start | bytes 786440 | tf_op jit(solution)/shard_map/ppermute | solution.py:28
  49.7 3.6 %collective-permute-done.5.refs_2_ = bf16[512,256]{1,0:T(8,128)(2,1)} collective-permute-done((bf16[512,256]{1,0:T(8,128)(2,1)S(1)}, bf16[512,256]{1,0:T(8,128)(2,1)}, u32[]{:S(2)}, u32[]{:S(2)}) %collective-permute-start.5) | collective-permute-done | bytes 262176 | tf_op jit(solution)/shard_map/ppermute | solution.py:28
  53.2 2.0 %collective-permute-start.10 = (bf16[512,256]{1,0:T(8,128)(2,1)}, bf16[512,256]{1,0:T(8,128)(2,1)}, u32[]{:S(2)}, u32[]{:S(2)}) collective-permute-start(bf16[512,256]{1,0:T(8,128)(2,1)} %collective-permute-done.5.refs_2_), channel_id=1, source_target_pairs={{0,1},{1,0},{2,3},{3,2},{4,5},{5,4},{6,7},{7,6},{8,9},{9,8},{10,11... | collective-permute-start | bytes 786440 | tf_op jit(solution)/shard_map/ppermute | solution.py:23
  57.4 2.7 %collective-permute-start.2 = (bf16[24,2048]{1,0:T(8,128)(2,1)S(1)}, bf16[24,2048]{1,0:T(8,128)(2,1)S(1)}, u32[]{:S(2)}, u32[]{:S(2)}) collective-permute-start(bf16[24,2048]{1,0:T(8,128)(2,1)S(1)} %shard_map.75), channel_id=1, source_target_pairs={{0,32},{16,48},{32,0},{48,16},{1,33},{17,49},{33,1},{49,17},{2,34}... | collective-permute-start | bytes 294920 | tf_op jit(solution)/shard_map/ppermute | solution.py:33
  61.8 2.6 %collective-permute-start.16 = (bf16[256,1024]{1,0:T(8,128)(2,1)}, bf16[256,1024]{1,0:T(8,128)(2,1)S(1)}, u32[]{:S(2)}, u32[]{:S(2)}) collective-permute-start(bf16[256,1024]{1,0:T(8,128)(2,1)} %refs_0_.4), channel_id=1, source_target_pairs={{0,192},{64,0},{128,64},{192,128},{1,193},{65,1},{129,65},{193,129... | collective-permute-start | bytes 1572872 | tf_op jit(solution)/shard_map/ppermute | solution.py:28
  65.8 3.8 %shard_map.76 = bf16[8,96,128]{2,1,0:T(8,128)(2,1)} custom-call(bf16[96,2048]{1,0:T(8,128)(2,1)S(1)} %pad_maximum_fusion.hidden, bf16[1024,256]{1,0:T(8,128)(2,1)} %refs_0_.3, bf16[1024,256]{1,0:T(8,128)(2,1)} %copy-done.4, bf16[512,256]{1,0:T(8,128)(2,1)} %collective-permute-done.5.refs_2_, bf16[512,256]{1,0:T(8,128)(2,1)} %collective-permute-done.7.refs_3_, ...), custom_call_target="tpu_custom_call" | custom-call | tf_op jit(solution)/shard_map/pallas_call | solution.py:50
  69.6 8.2 %all-to-all-start.1 = ((bf16[8,96,128]{2,1,0:T(8,128)(2,1)}), bf16[8,96,128]{2,1,0:T(8,128)(2,1)S(1)}, u32[]{:S(2)}, u32[]{:S(2)}) async-start(bf16[8,96,128]{2,1,0:T(8,128)(2,1)} %shard_map.76), calls=%async_computation.1 | async-start | bytes 393216 | tf_op jit(solution)/shard_map/all_to_all | solution.py:19
  88.2 17.8 %all-to-all-start.2 = ((bf16[8,104,128]{2,1,0:T(8,128)(2,1)}), bf16[8,104,128]{2,1,0:T(8,128)(2,1)S(1)}, u32[]{:S(2)}, u32[]{:S(2)}) async-start(bf16[8,104,128]{2,1,0:T(8,128)(2,1)} %get-tuple-element.17), calls=%async_computation.2 | async-start | bytes 425984 | tf_op jit(solution)/shard_map/all_to_all | solution.py:19
  109.9 7.3 %all-to-all-done.2.x = bf16[8,104,128]{2,1,0:T(8,128)(2,1)S(1)} async-done(((bf16[8,104,128]{2,1,0:T(8,128)(2,1)}), bf16[8,104,128]{2,1,0:T(8,128)(2,1)S(1)}, u32[]{:S(2)}, u32[]{:S(2)}) %all-to-all-start.2) | async-done | bytes 213024 | tf_op jit(solution)/shard_map/all_to_all | solution.py:19
  117.2 2.5 %shard_map.78 = (bf16[24,2176]{1,0:T(8,128)(2,1)S(1)}, bf16[24,2176]{1,0:T(8,128)(2,1)S(1)}, bf16[24,2176]{1,0:T(8,128)(2,1)S(1)}, bf16[24,2176]{1,0:T(8,128)(2,1)S(1)}) custom-call(bf16[8,104,128]{2,1,0:T(8,128)(2,1)S(1)} %all-to-all-done.2.x, bf16[256,1024]{1,0:T(8,128)(2,1)} %refs_0_.4, bf16[256,1024]{1,0:T(8,128)(2,1)} %copy-done.2, ...), custom_call_target="tpu_custom_call" | custom-call | tf_op jit(solution)/shard_map/pallas_call | solution.py:50
  119.8 2.0 %collective-permute-start.24 = (bf16[24,2176]{1,0:T(8,128)(2,1)S(1)}, bf16[24,2176]{1,0:T(8,128)(2,1)S(1)}, u32[]{:S(2)}, u32[]{:S(2)}) collective-permute-start(bf16[24,2176]{1,0:T(8,128)(2,1)S(1)} %get-tuple-element.20), channel_id=1, source_target_pairs={{0,48},{16,0},{32,16},{48,32},{1,49},{17,1},{33,17},{49,33},{2,50}... | collective-permute-start | bytes 313352 | tf_op jit(solution)/shard_map/ppermute | solution.py:33
  122.0 3.3 %collective-permute-done.23.refs_1_ = bf16[24,2176]{1,0:T(8,128)(2,1)S(1)} collective-permute-done((bf16[24,2176]{1,0:T(8,128)(2,1)S(1)}, bf16[24,2176]{1,0:T(8,128)(2,1)S(1)}, u32[]{:S(2)}, u32[]{:S(2)}) %collective-permute-start.23) | collective-permute-done | bytes 104480 | tf_op jit(solution)/shard_map/ppermute | solution.py:33
  125.2 2.2 %collective-permute-start.33 = (bf16[1024,256]{1,0:T(8,128)(2,1)}, bf16[1024,256]{1,0:T(8,128)(2,1)S(1)}, u32[]{:S(2)}, u32[]{:S(2)}) collective-permute-start(bf16[1024,256]{1,0:T(8,128)(2,1)} %refs_0_.5), channel_id=1, source_target_pairs={{0,1},{1,0},{2,3},{3,2},{4,5},{5,4},{6,7},{7,6},{8,9},{9,8},{10,11... | collective-permute-start | bytes 1572872 | tf_op jit(solution)/shard_map/ppermute | solution.py:23
  131.0 6.0 %collective-permute-done.26 = bf16[24,2048]{1,0:T(8,128)(2,1)S(1)} collective-permute-done((bf16[24,2048]{1,0:T(8,128)(2,1)S(1)}, bf16[24,2048]{1,0:T(8,128)(2,1)S(1)}, u32[]{:S(2)}, u32[]{:S(2)}) %collective-permute-start.26) | collective-permute-done | bytes 98336 | tf_op jit(solution)/shard_map/ppermute | solution.py:33
  137.8 2.6 %collective-permute-done.28 = bf16[24,2048]{1,0:T(8,128)(2,1)S(1)} collective-permute-done((bf16[24,2048]{1,0:T(8,128)(2,1)S(1)}, bf16[24,2048]{1,0:T(8,128)(2,1)S(1)}, u32[]{:S(2)}, u32[]{:S(2)}) %collective-permute-start.28) | collective-permute-done | bytes 98336 | tf_op jit(solution)/shard_map/ppermute | solution.py:33
  140.5 2.0 %collective-permute-start.36 = (bf16[512,256]{1,0:T(8,128)(2,1)S(1)}, bf16[512,256]{1,0:T(8,128)(2,1)S(1)}, u32[]{:S(2)}, u32[]{:S(2)}) collective-permute-start(bf16[512,256]{1,0:T(8,128)(2,1)S(1)} %collective-permute-done.32.refs_3_), channel_id=1, source_target_pairs={{0,1},{1,0},{2,3},{3,2},{4,5},{5,4},{6,7},{7,6},{8,9},{9,8},{10,11... | collective-permute-start | bytes 786440 | tf_op jit(solution)/shard_map/ppermute | solution.py:23
  145.3 3.1 %shard_map.80 = bf16[8,96,128]{2,1,0:T(8,128)(2,1)S(1)} custom-call(bf16[96,2048]{1,0:T(8,128)(2,1)S(1)} %pad_maximum_fusion.1.hidden, bf16[1024,256]{1,0:T(8,128)(2,1)} %refs_0_.5, bf16[1024,256]{1,0:T(8,128)(2,1)} %copy-done, bf16[512,256]{1,0:T(8,128)(2,1)} %copy-done.12, bf16[512,256]{1,0:T(8,128)(2,1)} %copy-done.14, bf16[1024,256]{1,0:T(8,128)(2,1)} %copy-done.1, ...), custom_call_target="tpu_custom_call" | custom-call | tf_op jit(solution)/shard_map/pallas_call | solution.py:50
  148.4 12.4 %all_to_all.25.parts = bf16[8,96,128]{2,1,0:T(8,128)(2,1)S(1)} all-to-all(bf16[8,96,128]{2,1,0:T(8,128)(2,1)S(1)} %shard_map.80), channel_id=1, replica_groups=mesh['y'=4,'x'=4,'z'=8,'c'=2] {'z'}, dimensions={0} | all-to-all | bytes 393216 | tf_op jit(solution)/shard_map/all_to_all | solution.py:19
  161.6 15.8 %all_to_all.26.own = bf16[8,96,128]{2,1,0:T(8,128)(2,1)S(1)} all-to-all(bf16[8,96,128]{2,1,0:T(8,128)(2,1)S(1)} %broadcast_in_dim.14), channel_id=1, replica_groups=mesh['y'=4,'x'=4,'z'=8,'c'=2] {'z'}, dimensions={0} | all-to-all | bytes 393216 | tf_op jit(solution)/shard_map/all_to_all | solution.py:19
  177.5 3.5 %collective-permute-start.39 = (bf16[8,96,128]{2,1,0:T(8,128)(2,1)S(1)}, bf16[8,96,128]{2,1,0:T(8,128)(2,1)S(1)}, u32[]{:S(2)}, u32[]{:S(2)}) collective-permute-start(bf16[8,96,128]{2,1,0:T(8,128)(2,1)S(1)} %all_to_all.26.own), channel_id=1, source_target_pairs={{0,1},{1,0},{2,3},{3,2},{4,5},{5,4},{6,7},{7,6},{8,9},{9,8},{10,11... | collective-permute-start | bytes 589832 | tf_op jit(solution)/shard_map/ppermute | solution.py:23
  (121 shorter events, 36.4 us)
Async XLA Ops:
  7.4 48.3 %all-to-all-start = ((bf16[16,24,2176]{2,1,0:T(8,128)(2,1)}), bf16[16,24,2176]{2,1,0:T(8,128)(2,1)S(1)}, u32[]{:S(2)}, u32[]{:S(2)}) async-start(bf16[16,24,2176]{2,1,0:T(8,128)(2,1)} %bitcast.2), calls=%async_computation | async-start | bytes 3342336 | tf_op jit(solution)/shard_map/all_to_all | solution.py:19
  12.7 32.4 %collective-permute-start.4 = (bf16[1024,256]{1,0:T(8,128)(2,1)S(1)}, bf16[1024,256]{1,0:T(8,128)(2,1)S(1)}, u32[]{:S(2)}, u32[]{:S(2)}) collective-permute-start(bf16[1024,256]{1,0:T(8,128)(2,1)S(1)} %copy-done.6), channel_id=1, source_target_pairs={{0,64},{64,128},{128,192},{192,0},{1,65},{65,129},{129,193},{193,1... | collective-permute-start | bytes 1572872 | tf_op jit(solution)/shard_map/ppermute | solution.py:28
  14.1 31.1 %collective-permute-start.6 = (bf16[1024,256]{1,0:T(8,128)(2,1)S(1)}, bf16[1024,256]{1,0:T(8,128)(2,1)S(1)}, u32[]{:S(2)}, u32[]{:S(2)}) collective-permute-start(bf16[1024,256]{1,0:T(8,128)(2,1)S(1)} %copy-done.6), channel_id=1, source_target_pairs={{0,192},{64,0},{128,64},{192,128},{1,193},{65,1},{129,65},{193,129... | collective-permute-start | bytes 1572872 | tf_op jit(solution)/shard_map/ppermute | solution.py:28
  15.4 40.7 %collective-permute-start.8 = (bf16[1024,256]{1,0:T(8,128)(2,1)S(1)}, bf16[1024,256]{1,0:T(8,128)(2,1)}, u32[]{:S(2)}, u32[]{:S(2)}) collective-permute-start(bf16[1024,256]{1,0:T(8,128)(2,1)S(1)} %copy-done.6), channel_id=1, source_target_pairs={{0,1},{1,0},{2,3},{3,2},{4,5},{5,4},{6,7},{7,6},{8,9},{9,8},{10,11... | collective-permute-start | bytes 1572872 | tf_op jit(solution)/shard_map/ppermute | solution.py:23
  45.1 8.1 %collective-permute-start.5 = (bf16[512,256]{1,0:T(8,128)(2,1)S(1)}, bf16[512,256]{1,0:T(8,128)(2,1)}, u32[]{:S(2)}, u32[]{:S(2)}) collective-permute-start(bf16[512,256]{1,0:T(8,128)(2,1)S(1)} %slice.24), channel_id=1, source_target_pairs={{0,64},{64,128},{128,192},{192,0},{1,65},{65,129},{129,193},{193,1... | collective-permute-start | bytes 786440 | tf_op jit(solution)/shard_map/ppermute | solution.py:28
  45.2 10.0 %collective-permute-start.7 = (bf16[512,256]{1,0:T(8,128)(2,1)S(1)}, bf16[512,256]{1,0:T(8,128)(2,1)}, u32[]{:S(2)}, u32[]{:S(2)}) collective-permute-start(bf16[512,256]{1,0:T(8,128)(2,1)S(1)} %slice.25), channel_id=1, source_target_pairs={{0,192},{64,0},{128,64},{192,128},{1,193},{65,1},{129,65},{193,129... | collective-permute-start | bytes 786440 | tf_op jit(solution)/shard_map/ppermute | solution.py:28
  48.0 13.7 %collective-permute-start.12 = (bf16[1024,256]{1,0:T(8,128)(2,1)S(1)}, bf16[1024,256]{1,0:T(8,128)(2,1)}, u32[]{:S(2)}, u32[]{:S(2)}) collective-permute-start(bf16[1024,256]{1,0:T(8,128)(2,1)S(1)} %collective-permute-done.6.refs_4_), channel_id=1, source_target_pairs={{0,1},{1,0},{2,3},{3,2},{4,5},{5,4},{6,7},{7,6},{8,9},{9,8},{10,11... | collective-permute-start | bytes 1572872 | tf_op jit(solution)/shard_map/ppermute | solution.py:23
  55.2 10.6 %collective-permute-start.9 = (bf16[1024,256]{1,0:T(8,128)(2,1)S(1)}, bf16[1024,256]{1,0:T(8,128)(2,1)}, u32[]{:S(2)}, u32[]{:S(2)}) collective-permute-start(bf16[1024,256]{1,0:T(8,128)(2,1)S(1)} %collective-permute-done.4.refs_1_), channel_id=1, source_target_pairs={{0,1},{1,0},{2,3},{3,2},{4,5},{5,4},{6,7},{7,6},{8,9},{9,8},{10,11... | collective-permute-start | bytes 1572872 | tf_op jit(solution)/shard_map/ppermute | solution.py:23
  61.6 16.2 %collective-permute-start.14 = (bf16[256,1024]{1,0:T(8,128)(2,1)}, bf16[256,1024]{1,0:T(8,128)(2,1)S(1)}, u32[]{:S(2)}, u32[]{:S(2)}) collective-permute-start(bf16[256,1024]{1,0:T(8,128)(2,1)} %refs_0_.4), channel_id=1, source_target_pairs={{0,64},{64,128},{128,192},{192,0},{1,65},{65,129},{129,193},{193,1... | collective-permute-start | bytes 1572872 | tf_op jit(solution)/shard_map/ppermute | solution.py:28
  61.8 18.3 %collective-permute-start.16 = (bf16[256,1024]{1,0:T(8,128)(2,1)}, bf16[256,1024]{1,0:T(8,128)(2,1)S(1)}, u32[]{:S(2)}, u32[]{:S(2)}) collective-permute-start(bf16[256,1024]{1,0:T(8,128)(2,1)} %refs_0_.4), channel_id=1, source_target_pairs={{0,192},{64,0},{128,64},{192,128},{1,193},{65,1},{129,65},{193,129... | collective-permute-start | bytes 1572872 | tf_op jit(solution)/shard_map/ppermute | solution.py:28
  64.8 19.4 %collective-permute-start.18 = (bf16[256,1024]{1,0:T(8,128)(2,1)}, bf16[256,1024]{1,0:T(8,128)(2,1)S(1)}, u32[]{:S(2)}, u32[]{:S(2)}) collective-permute-start(bf16[256,1024]{1,0:T(8,128)(2,1)} %refs_0_.4), channel_id=1, source_target_pairs={{0,1},{1,0},{2,3},{3,2},{4,5},{5,4},{6,7},{7,6},{8,9},{9,8},{10,11... | collective-permute-start | bytes 1572872 | tf_op jit(solution)/shard_map/ppermute | solution.py:23
  65.7 21.2 %collective-permute-start.29 = (bf16[1024,256]{1,0:T(8,128)(2,1)}, bf16[1024,256]{1,0:T(8,128)(2,1)S(1)}, u32[]{:S(2)}, u32[]{:S(2)}) collective-permute-start(bf16[1024,256]{1,0:T(8,128)(2,1)} %refs_0_.5), channel_id=1, source_target_pairs={{0,64},{64,128},{128,192},{192,0},{1,65},{65,129},{129,193},{193,1... | collective-permute-start | bytes 1572872 | tf_op jit(solution)/shard_map/ppermute | solution.py:28
  69.6 17.9 %all-to-all-start.1 = ((bf16[8,96,128]{2,1,0:T(8,128)(2,1)}), bf16[8,96,128]{2,1,0:T(8,128)(2,1)S(1)}, u32[]{:S(2)}, u32[]{:S(2)}) async-start(bf16[8,96,128]{2,1,0:T(8,128)(2,1)} %shard_map.76), calls=%async_computation.1 | async-start | bytes 393216 | tf_op jit(solution)/shard_map/all_to_all | solution.py:19
  78.6 27.4 %collective-permute-start.15 = (bf16[128,1024]{1,0:T(8,128)(2,1)}, bf16[128,1024]{1,0:T(8,128)(2,1)S(1)}, u32[]{:S(2)}, u32[]{:S(2)}) collective-permute-start(bf16[128,1024]{1,0:T(8,128)(2,1)} %slice.26), channel_id=1, source_target_pairs={{0,64},{64,128},{128,192},{192,0},{1,65},{65,129},{129,193},{193,1... | collective-permute-start | bytes 786440 | tf_op jit(solution)/shard_map/ppermute | solution.py:28
  80.8 25.6 %collective-permute-start.17 = (bf16[128,1024]{1,0:T(8,128)(2,1)}, bf16[128,1024]{1,0:T(8,128)(2,1)}, u32[]{:S(2)}, u32[]{:S(2)}) collective-permute-start(bf16[128,1024]{1,0:T(8,128)(2,1)} %slice.27), channel_id=1, source_target_pairs={{0,192},{64,0},{128,64},{192,128},{1,193},{65,1},{129,65},{193,129... | collective-permute-start | bytes 786440 | tf_op jit(solution)/shard_map/ppermute | solution.py:28
  82.7 26.5 %collective-permute-start.19 = (bf16[256,1024]{1,0:T(8,128)(2,1)S(1)}, bf16[256,1024]{1,0:T(8,128)(2,1)S(1)}, u32[]{:S(2)}, u32[]{:S(2)}) collective-permute-start(bf16[256,1024]{1,0:T(8,128)(2,1)S(1)} %collective-permute-done.14.refs_1_), channel_id=1, source_target_pairs={{0,1},{1,0},{2,3},{3,2},{4,5},{5,4},{6,7},{7,6},{8,9},{9,8},{10,11... | collective-permute-start | bytes 1572872 | tf_op jit(solution)/shard_map/ppermute | solution.py:23
  84.2 25.8 %collective-permute-start.22 = (bf16[256,1024]{1,0:T(8,128)(2,1)S(1)}, bf16[256,1024]{1,0:T(8,128)(2,1)}, u32[]{:S(2)}, u32[]{:S(2)}) collective-permute-start(bf16[256,1024]{1,0:T(8,128)(2,1)S(1)} %collective-permute-done.16.refs_4_), channel_id=1, source_target_pairs={{0,1},{1,0},{2,3},{3,2},{4,5},{5,4},{6,7},{7,6},{8,9},{9,8},{10,11... | collective-permute-start | bytes 1572872 | tf_op jit(solution)/shard_map/ppermute | solution.py:23
  86.9 34.9 %collective-permute-start.31 = (bf16[1024,256]{1,0:T(8,128)(2,1)}, bf16[1024,256]{1,0:T(8,128)(2,1)S(1)}, u32[]{:S(2)}, u32[]{:S(2)}) collective-permute-start(bf16[1024,256]{1,0:T(8,128)(2,1)} %refs_0_.5), channel_id=1, source_target_pairs={{0,192},{64,0},{128,64},{192,128},{1,193},{65,1},{129,65},{193,129... | collective-permute-start | bytes 1572872 | tf_op jit(solution)/shard_map/ppermute | solution.py:28
  88.2 29.0 %all-to-all-start.2 = ((bf16[8,104,128]{2,1,0:T(8,128)(2,1)}), bf16[8,104,128]{2,1,0:T(8,128)(2,1)S(1)}, u32[]{:S(2)}, u32[]{:S(2)}) async-start(bf16[8,104,128]{2,1,0:T(8,128)(2,1)} %get-tuple-element.17), calls=%async_computation.2 | async-start | bytes 425984 | tf_op jit(solution)/shard_map/all_to_all | solution.py:19
  107.6 21.6 %collective-permute-start.30 = (bf16[512,256]{1,0:T(8,128)(2,1)}, bf16[512,256]{1,0:T(8,128)(2,1)S(1)}, u32[]{:S(2)}, u32[]{:S(2)}) collective-permute-start(bf16[512,256]{1,0:T(8,128)(2,1)} %slice.28), channel_id=1, source_target_pairs={{0,64},{64,128},{128,192},{192,0},{1,65},{65,129},{129,193},{193,1... | collective-permute-start | bytes 786440 | tf_op jit(solution)/shard_map/ppermute | solution.py:28
  125.2 17.2 %collective-permute-start.33 = (bf16[1024,256]{1,0:T(8,128)(2,1)}, bf16[1024,256]{1,0:T(8,128)(2,1)S(1)}, u32[]{:S(2)}, u32[]{:S(2)}) collective-permute-start(bf16[1024,256]{1,0:T(8,128)(2,1)} %refs_0_.5), channel_id=1, source_target_pairs={{0,1},{1,0},{2,3},{3,2},{4,5},{5,4},{6,7},{7,6},{8,9},{9,8},{10,11... | collective-permute-start | bytes 1572872 | tf_op jit(solution)/shard_map/ppermute | solution.py:23
  127.4 16.2 %collective-permute-start.34 = (bf16[1024,256]{1,0:T(8,128)(2,1)S(1)}, bf16[1024,256]{1,0:T(8,128)(2,1)S(1)}, u32[]{:S(2)}, u32[]{:S(2)}) collective-permute-start(bf16[1024,256]{1,0:T(8,128)(2,1)S(1)} %collective-permute-done.29.refs_1_), channel_id=1, source_target_pairs={{0,1},{1,0},{2,3},{3,2},{4,5},{5,4},{6,7},{7,6},{8,9},{9,8},{10,11... | collective-permute-start | bytes 1572872 | tf_op jit(solution)/shard_map/ppermute | solution.py:23
  127.7 15.9 %collective-permute-start.37 = (bf16[1024,256]{1,0:T(8,128)(2,1)S(1)}, bf16[1024,256]{1,0:T(8,128)(2,1)S(1)}, u32[]{:S(2)}, u32[]{:S(2)}) collective-permute-start(bf16[1024,256]{1,0:T(8,128)(2,1)S(1)} %collective-permute-done.31.refs_4_), channel_id=1, source_target_pairs={{0,1},{1,0},{2,3},{3,2},{4,5},{5,4},{6,7},{7,6},{8,9},{9,8},{10,11... | collective-permute-start | bytes 1572872 | tf_op jit(solution)/shard_map/ppermute | solution.py:23
  129.2 7.8 %collective-permute-start.26 = (bf16[24,2048]{1,0:T(8,128)(2,1)S(1)}, bf16[24,2048]{1,0:T(8,128)(2,1)S(1)}, u32[]{:S(2)}, u32[]{:S(2)}) collective-permute-start(bf16[24,2048]{1,0:T(8,128)(2,1)S(1)} %shard_map.79), channel_id=1, source_target_pairs={{0,16},{16,32},{32,48},{48,0},{1,17},{17,33},{33,49},{49,1},{2,18}... | collective-permute-start | bytes 294920 | tf_op jit(solution)/shard_map/ppermute | solution.py:33
  (38 other events, 319.5 us)

commit v7 on v6

--- a/solution.py
+++ b/solution.py
@@ -147,11 +147,11 @@
         mine = blocks[side * per : (side + 1) * per]
         spot = held.at[side * n + d]
         first = len(pairs)
-        if d == far:
+        if d == far and per > n:
             rows = mine[far].shape[0]
             pairs += [(mine[far], spot.at[:rows]), (mine[far + 1], spot.at[rows:])]
         else:
-            pairs.append((mine[d + (d > far)], spot))
+            pairs.append((mine[d + (d > far) * (per - n)], spot))
         spans[side, d] = range(first, len(pairs))
     copies = fetch(pairs, sems)
 
@@ -193,7 +193,8 @@
 
 def up_second_kernel(x, *refs):
     *refs, held, sems = refs
-    blocks, outs = refs[: held.shape[0] + 2], refs[held.shape[0] + 2 :]
+    count = sems.shape[0]
+    blocks, outs = refs[:count], refs[count:]
     n, depth, hid = held.shape[0] // 2, *held.shape[1:]
     ready = arriving(blocks, held, sems, [(side, d) for side in range(2) for d in range(n)])
     few = outs[0].shape[0]
@@ -242,11 +243,14 @@
     return jnp.broadcast_to(x[None], (peers, *x.shape))
 
 
-def around(w, swapped):
+def around(w, swapped, halves=False):
     n = lax.axis_size("y")
     half = w.shape[0] // 2
     near = [along_y(w, 1), along_y(w, n - 1)]
-    far = [along_y(near[0][:half], 1), along_y(near[1][half:], n - 1)]
+    if halves:
+        far = [along_y(near[0][:half], 1), along_y(near[1][half:], n - 1)]
+    else:
+        far = [along_y(w, n // 2)]
     moved = [near[0], *far, near[1]]
     return [w, *moved, swapped] + [from_other_core(v) for v in moved]
 
@@ -271,8 +275,8 @@
     wide = hid + LANES
     blocks = 2 * ny
 
-    def held(w):
-        return [pltpu.VMEM((blocks, *w.shape), BF), pltpu.SemaphoreType.DMA((blocks + 2,))]
+    def held(w, more=0):
+        return [pltpu.VMEM((blocks, *w.shape), BF), pltpu.SemaphoreType.DMA((blocks + more,))]
 
     activate = call(functools.partial(activate_kernel, width=width), sds((few, hid)))
     down_out = sds((nz, per_y, LANES))
@@ -304,11 +308,11 @@
     parts = exchange(payload.reshape(ny * nx, few, wide), RA)
     kept = by_plane(kept, lambda z: z // 2)
     swapped = [from_other_core(w) for w in (down_first, up_second, down_second)]
-    downs = around(down_first, swapped[0])
+    downs = around(down_first, swapped[0], halves=True)
     hidden = activate(parts)
 
     hidden = from_x_ring(hidden, nx)
-    branch = call(down_kernel, down_out, held(down_first), whole=1)(hidden, *downs)
+    branch = call(down_kernel, down_out, held(down_first, 2), whole=1)(hidden, *downs)
     ups = around(up_second, swapped[1])
     branch = exchange(branch, "z")
     downs = around(down_second, swapped[2])

time: 183 us -> 195 us (1.066)
  waiting for transfers between devices: 56.7 us -> 68.9 us
  local copies, waits for them, and re-layouts: 5.42 us -> 2.72 us
  starting transfers between devices: 76.2 us -> 78.2 us
    ppermute x12 -> x10, waiting for transfers between devices: 34.3 us -> 46.4 us  [along_y(): return lax.ppermute(a, 'y', [(i, (i + shift) % n) for i in range(n)])]
    ppermute x17 -> x15, starting transfers between devices: 21.3 us -> 26.9 us  [from_other_core(): return lax.ppermute(w, 'c', [(0, 1), (1, 0)])]
    all_to_all x3, starting transfers between devices: 31.1 us -> 27.7 us  [exchange(): return lax.all_to_all(parts, axis, 0, 0, tiled=True)]
    ppermute x9, waiting for transfers between devices: 12.6 us -> 15.8 us  [along_x(): return lax.ppermute(a, 'x', [(i, (i + shift) % n) for i in range(n)])]
    ppermute x12 -> x10, starting transfers between devices: 13 us -> 10.7 us  [along_y(): return lax.ppermute(a, 'y', [(i, (i + shift) % n) for i in range(n)])]
    slice x6 -> x2, local copies, waits for them, and re-layouts: 2.29 us -> 0.04 us  [around(): far = [along_y(near[0][:half], 1), along_y(near[1][half:], n - 1)]]
    ppermute x9, starting transfers between devices: 9.33 us -> 11.6 us  [along_x(): return lax.ppermute(a, 'x', [(i, (i + shift) % n) for i in range(n)])]
  transfers between devices with their start and end apart: 43 -> 39, of which waited for: 13 -> 11; matrix products, arithmetic and copies ran while one was open for 1% -> 0% of each run, Pallas kernels for 6% -> 5%
where the time goes in v7:
time: 195 us
  starting transfers between devices  78.2 us (40%)
  waiting for transfers between devices  68.9 us (35%)
  blocking collectives  28.6 us (15%)
  Pallas kernels  15.8 us (8%)
  local copies, waits for them, and re-layouts  2.72 us (1%)
    ppermute x10, waiting for transfers between devices, along_y(): return lax.ppermute(a, 'y', [(i, (i + shift) % n) for i in range(n)])  46.4 us
    all_to_all x2, blocking collectives, exchange(): return lax.all_to_all(parts, axis, 0, 0, tiled=True)  28.6 us
    all_to_all x3, starting transfers between devices, exchange(): return lax.all_to_all(parts, axis, 0, 0, tiled=True)  27.7 us
    ppermute x15, starting transfers between devices, from_other_core(): return lax.ppermute(w, 'c', [(0, 1), (1, 0)])  26.9 us
    ppermute x9, waiting for transfers between devices, along_x(): return lax.ppermute(a, 'x', [(i, (i + shift) % n) for i in range(n)])  15.8 us
    pallas_call x10, Pallas kernels, run(): pl.pallas_call(kernel, out_shape=out, in_specs=[vmem] * first + [lies] *...  15.8 us
    ppermute x9, starting transfers between devices, along_x(): return lax.ppermute(a, 'x', [(i, (i + shift) % n) for i in range(n)])  11.6 us
    ppermute x10, starting transfers between devices, along_y(): return lax.ppermute(a, 'y', [(i, (i + shift) % n) for i in range(n)])  10.7 us
  transfers between devices with their start and end apart: 39, of which 11 were waited for; matrix products, arithmetic and copies ran while one was open for 0% of the time, Pallas kernels for 5%

profile of v7, /device:TPU:1, one launch (start us, length us, event | category | flops | bytes accessed | tf_op | source)
XLA Modules:
  0.0 194.7 jit_solution(10303247636218720179)
XLA Ops:
  0.0 3.2 %collective-permute-start = (bf16[256,1024]{1,0:T(8,128)(2,1)}, bf16[256,1024]{1,0:T(8,128)(2,1)S(1)}, u32[]{:S(2)}, u32[]{:S(2)}) collective-permute-start(bf16[256,1024]{1,0:T(8,128)(2,1)} %own.1), channel_id=1, source_target_pairs={{0,1},{1,0},{2,3},{3,2},{4,5},{5,4},{6,7},{7,6},{8,9},{9,8},{10,11... | collective-permute-start | bytes 1572872 | tf_op jit(solution)/shard_map/ppermute | solution.py:23
  3.2 2.8 %shard_map.73 = (bf16[384,2176]{1,0:T(8,128)(2,1)}, bf16[384,256]{1,0:T(8,128)(2,1)S(1)}, f32[104,128]{1,0:T(8,128)S(1)}) custom-call(bf16[768,256]{1,0:T(8,128)(2,1)} %tokens.1, f32[1,256]{1,0:T(1,128)} %bitcast.3, f32[1,256]{1,0:T(1,128)} %bitcast.4, bf16[256,1024]{1,0:T(8,128)(2,1)} %own.1), custom_call_target="tpu_custom_call" | custom-call | tf_op jit(solution)/shard_map/pallas_call | solution.py:50
  7.4 5.2 %all-to-all-start = ((bf16[16,24,2176]{2,1,0:T(8,128)(2,1)}), bf16[16,24,2176]{2,1,0:T(8,128)(2,1)S(1)}, u32[]{:S(2)}, u32[]{:S(2)}) async-start(bf16[16,24,2176]{2,1,0:T(8,128)(2,1)} %bitcast.2), calls=%async_computation | async-start | bytes 3342336 | tf_op jit(solution)/shard_map/all_to_all | solution.py:19
  16.6 28.4 %collective-permute-done.4.refs_1_ = bf16[1024,256]{1,0:T(8,128)(2,1)S(1)} collective-permute-done((bf16[1024,256]{1,0:T(8,128)(2,1)S(1)}, bf16[1024,256]{1,0:T(8,128)(2,1)S(1)}, u32[]{:S(2)}, u32[]{:S(2)}) %collective-permute-start.4) | collective-permute-done | bytes 524320 | tf_op jit(solution)/shard_map/ppermute | solution.py:28
  45.2 2.7 %collective-permute-start.7 = (bf16[512,256]{1,0:T(8,128)(2,1)S(1)}, bf16[512,256]{1,0:T(8,128)(2,1)}, u32[]{:S(2)}, u32[]{:S(2)}) collective-permute-start(bf16[512,256]{1,0:T(8,128)(2,1)S(1)} %slice.9), channel_id=1, source_target_pairs={{0,192},{64,0},{128,64},{192,128},{1,193},{65,1},{129,65},{193,129... | collective-permute-start | bytes 786440 | tf_op jit(solution)/shard_map/ppermute | solution.py:28
  47.9 2.4 %collective-permute-start.12 = (bf16[1024,256]{1,0:T(8,128)(2,1)S(1)}, bf16[1024,256]{1,0:T(8,128)(2,1)}, u32[]{:S(2)}, u32[]{:S(2)}) collective-permute-start(bf16[1024,256]{1,0:T(8,128)(2,1)S(1)} %collective-permute-done.6.refs_4_), channel_id=1, source_target_pairs={{0,1},{1,0},{2,3},{3,2},{4,5},{5,4},{6,7},{7,6},{8,9},{9,8},{10,11... | collective-permute-start | bytes 1572872 | tf_op jit(solution)/shard_map/ppermute | solution.py:23
  50.4 11.6 %collective-permute-done.5.refs_2_ = bf16[512,256]{1,0:T(8,128)(2,1)} collective-permute-done((bf16[512,256]{1,0:T(8,128)(2,1)S(1)}, bf16[512,256]{1,0:T(8,128)(2,1)}, u32[]{:S(2)}, u32[]{:S(2)}) %collective-permute-start.5) | collective-permute-done | bytes 262176 | tf_op jit(solution)/shard_map/ppermute | solution.py:28
  71.0 2.4 %collective-permute-done.2 = bf16[24,2048]{1,0:T(8,128)(2,1)S(1)} collective-permute-done((bf16[24,2048]{1,0:T(8,128)(2,1)S(1)}, bf16[24,2048]{1,0:T(8,128)(2,1)S(1)}, u32[]{:S(2)}, u32[]{:S(2)}) %collective-permute-start.2) | collective-permute-done | bytes 98336 | tf_op jit(solution)/shard_map/ppermute | solution.py:33
  74.4 3.9 %shard_map.76 = bf16[8,96,128]{2,1,0:T(8,128)(2,1)} custom-call(bf16[96,2048]{1,0:T(8,128)(2,1)S(1)} %pad_maximum_fusion.hidden, bf16[1024,256]{1,0:T(8,128)(2,1)} %refs_0_.3, bf16[1024,256]{1,0:T(8,128)(2,1)} %copy-done, bf16[512,256]{1,0:T(8,128)(2,1)} %collective-permute-done.5.refs_2_, bf16[512,256]{1,0:T(8,128)(2,1)} %collective-permute-done.7.refs_3_, ...), custom_call_target="tpu_custom_call" | custom-call | tf_op jit(solution)/shard_map/pallas_call | solution.py:50
  78.3 8.2 %all-to-all-start.1 = ((bf16[8,96,128]{2,1,0:T(8,128)(2,1)}), bf16[8,96,128]{2,1,0:T(8,128)(2,1)S(1)}, u32[]{:S(2)}, u32[]{:S(2)}) async-start(bf16[8,96,128]{2,1,0:T(8,128)(2,1)} %shard_map.76), calls=%async_computation.1 | async-start | bytes 393216 | tf_op jit(solution)/shard_map/all_to_all | solution.py:19
  87.4 6.4 %collective-permute-done.16.refs_3_ = bf16[256,1024]{1,0:T(8,128)(2,1)} collective-permute-done((bf16[256,1024]{1,0:T(8,128)(2,1)}, bf16[256,1024]{1,0:T(8,128)(2,1)}, u32[]{:S(2)}, u32[]{:S(2)}) %collective-permute-start.16) | collective-permute-done | bytes 524320 | tf_op jit(solution)/shard_map/ppermute | solution.py:28
  96.7 14.3 %all-to-all-start.2 = ((bf16[8,104,128]{2,1,0:T(8,128)(2,1)}), bf16[8,104,128]{2,1,0:T(8,128)(2,1)S(1)}, u32[]{:S(2)}, u32[]{:S(2)}) async-start(bf16[8,104,128]{2,1,0:T(8,128)(2,1)} %get-tuple-element.17), calls=%async_computation.2 | async-start | bytes 425984 | tf_op jit(solution)/shard_map/all_to_all | solution.py:19
  111.7 2.9 %collective-permute-start.28 = (bf16[1024,256]{1,0:T(8,128)(2,1)S(1)}, bf16[1024,256]{1,0:T(8,128)(2,1)S(1)}, u32[]{:S(2)}, u32[]{:S(2)}) collective-permute-start(bf16[1024,256]{1,0:T(8,128)(2,1)S(1)} %copy-done.3), channel_id=1, source_target_pairs={{0,128},{64,192},{128,0},{192,64},{1,129},{65,193},{129,1},{193,65... | collective-permute-start | bytes 1572872 | tf_op jit(solution)/shard_map/ppermute | solution.py:28
  114.6 5.6 %all-to-all-done.2.x = bf16[8,104,128]{2,1,0:T(8,128)(2,1)S(1)} async-done(((bf16[8,104,128]{2,1,0:T(8,128)(2,1)}), bf16[8,104,128]{2,1,0:T(8,128)(2,1)S(1)}, u32[]{:S(2)}, u32[]{:S(2)}) %all-to-all-start.2) | async-done | bytes 213024 | tf_op jit(solution)/shard_map/all_to_all | solution.py:19
  120.2 2.5 %shard_map.78 = (bf16[24,2176]{1,0:T(8,128)(2,1)S(1)}, bf16[24,2176]{1,0:T(8,128)(2,1)S(1)}, bf16[24,2176]{1,0:T(8,128)(2,1)S(1)}, bf16[24,2176]{1,0:T(8,128)(2,1)S(1)}) custom-call(bf16[8,104,128]{2,1,0:T(8,128)(2,1)S(1)} %all-to-all-done.2.x, bf16[256,1024]{1,0:T(8,128)(2,1)} %refs_0_.4, bf16[256,1024]{1,0:T(8,128)(2,1)} %collective-permute-done.14.refs_1_, ...), custom_call_target="tpu_custom_call" | custom-call | tf_op jit(solution)/shard_map/pallas_call | solution.py:50
  123.1 2.5 %collective-permute-start.22 = (bf16[24,2176]{1,0:T(8,128)(2,1)S(1)}, bf16[24,2176]{1,0:T(8,128)(2,1)S(1)}, u32[]{:S(2)}, u32[]{:S(2)}) collective-permute-start(bf16[24,2176]{1,0:T(8,128)(2,1)S(1)} %get-tuple-element.20), channel_id=1, source_target_pairs={{0,48},{16,0},{32,16},{48,32},{1,49},{17,1},{33,17},{49,33},{2,50}... | collective-permute-start | bytes 313352 | tf_op jit(solution)/shard_map/ppermute | solution.py:33
  128.3 4.7 %collective-permute-done.23.refs_3_ = bf16[24,2176]{1,0:T(8,128)(2,1)S(1)} collective-permute-done((bf16[24,2176]{1,0:T(8,128)(2,1)S(1)}, bf16[24,2176]{1,0:T(8,128)(2,1)S(1)}, u32[]{:S(2)}, u32[]{:S(2)}) %collective-permute-start.23) | collective-permute-done | bytes 104480 | tf_op jit(solution)/shard_map/ppermute | solution.py:33
  133.2 6.0 %collective-permute-start.30 = (bf16[1024,256]{1,0:T(8,128)(2,1)S(1)}, bf16[1024,256]{1,0:T(8,128)(2,1)S(1)}, u32[]{:S(2)}, u32[]{:S(2)}) collective-permute-start(bf16[1024,256]{1,0:T(8,128)(2,1)S(1)} %copy-done.3), channel_id=1, source_target_pairs={{0,1},{1,0},{2,3},{3,2},{4,5},{5,4},{6,7},{7,6},{8,9},{9,8},{10,11... | collective-permute-start | bytes 1572872 | tf_op jit(solution)/shard_map/ppermute | solution.py:23
  140.5 4.5 %collective-permute-done.25 = bf16[24,2048]{1,0:T(8,128)(2,1)S(1)} collective-permute-done((bf16[24,2048]{1,0:T(8,128)(2,1)S(1)}, bf16[24,2048]{1,0:T(8,128)(2,1)S(1)}, u32[]{:S(2)}, u32[]{:S(2)}) %collective-permute-start.25) | collective-permute-done | bytes 98336 | tf_op jit(solution)/shard_map/ppermute | solution.py:33
  145.0 2.7 %collective-permute-start.26 = (bf16[24,2048]{1,0:T(8,128)(2,1)S(1)}, bf16[24,2048]{1,0:T(8,128)(2,1)S(1)}, u32[]{:S(2)}, u32[]{:S(2)}) collective-permute-start(bf16[24,2048]{1,0:T(8,128)(2,1)S(1)} %shard_map.79), channel_id=1, source_target_pairs={{0,48},{16,0},{32,16},{48,32},{1,49},{17,1},{33,17},{49,33},{2,50}... | collective-permute-start | bytes 294920 | tf_op jit(solution)/shard_map/ppermute | solution.py:33
  151.5 3.1 %shard_map.80 = bf16[8,96,128]{2,1,0:T(8,128)(2,1)S(1)} custom-call(bf16[96,2048]{1,0:T(8,128)(2,1)S(1)} %pad_maximum_fusion.1.hidden, bf16[1024,256]{1,0:T(8,128)(2,1)} %refs_0_.5, bf16[1024,256]{1,0:T(8,128)(2,1)} %copy-done.4, bf16[1024,256]{1,0:T(8,128)(2,1)} %copy-done.5, bf16[1024,256]{1,0:T(8,128)(2,1)} %copy-done.6, bf16[1024,256]{1,0:T(8,128)(2,1)} %copy-done.9, ...), custom_call_target="tpu_custom_call" | custom-call | tf_op jit(solution)/shard_map/pallas_call | solution.py:50
  154.6 13.2 %all_to_all.25.parts = bf16[8,96,128]{2,1,0:T(8,128)(2,1)S(1)} all-to-all(bf16[8,96,128]{2,1,0:T(8,128)(2,1)S(1)} %shard_map.80), channel_id=1, replica_groups=mesh['y'=4,'x'=4,'z'=8,'c'=2] {'z'}, dimensions={0} | all-to-all | bytes 393216 | tf_op jit(solution)/shard_map/all_to_all | solution.py:19
  168.5 15.4 %all_to_all.26.own = bf16[8,96,128]{2,1,0:T(8,128)(2,1)S(1)} all-to-all(bf16[8,96,128]{2,1,0:T(8,128)(2,1)S(1)} %broadcast_in_dim.14), channel_id=1, replica_groups=mesh['y'=4,'x'=4,'z'=8,'c'=2] {'z'}, dimensions={0} | all-to-all | bytes 393216 | tf_op jit(solution)/shard_map/all_to_all | solution.py:19
  183.9 8.8 %collective-permute-start.35 = (bf16[8,96,128]{2,1,0:T(8,128)(2,1)S(1)}, bf16[8,96,128]{2,1,0:T(8,128)(2,1)S(1)}, u32[]{:S(2)}, u32[]{:S(2)}) collective-permute-start(bf16[8,96,128]{2,1,0:T(8,128)(2,1)S(1)} %all_to_all.26.own), channel_id=1, source_target_pairs={{0,1},{1,0},{2,3},{3,2},{4,5},{5,4},{6,7},{7,6},{8,9},{9,8},{10,11... | collective-permute-start | bytes 589832 | tf_op jit(solution)/shard_map/ppermute | solution.py:23
  (97 shorter events, 30.9 us)
Async XLA Ops:
  7.4 57.0 %all-to-all-start = ((bf16[16,24,2176]{2,1,0:T(8,128)(2,1)}), bf16[16,24,2176]{2,1,0:T(8,128)(2,1)S(1)}, u32[]{:S(2)}, u32[]{:S(2)}) async-start(bf16[16,24,2176]{2,1,0:T(8,128)(2,1)} %bitcast.2), calls=%async_computation | async-start | bytes 3342336 | tf_op jit(solution)/shard_map/all_to_all | solution.py:19
  12.6 32.4 %collective-permute-start.4 = (bf16[1024,256]{1,0:T(8,128)(2,1)S(1)}, bf16[1024,256]{1,0:T(8,128)(2,1)S(1)}, u32[]{:S(2)}, u32[]{:S(2)}) collective-permute-start(bf16[1024,256]{1,0:T(8,128)(2,1)S(1)} %copy-done.2), channel_id=1, source_target_pairs={{0,64},{64,128},{128,192},{192,0},{1,65},{65,129},{129,193},{193,1... | collective-permute-start | bytes 1572872 | tf_op jit(solution)/shard_map/ppermute | solution.py:28
  14.1 31.1 %collective-permute-start.6 = (bf16[1024,256]{1,0:T(8,128)(2,1)S(1)}, bf16[1024,256]{1,0:T(8,128)(2,1)S(1)}, u32[]{:S(2)}, u32[]{:S(2)}) collective-permute-start(bf16[1024,256]{1,0:T(8,128)(2,1)S(1)} %copy-done.2), channel_id=1, source_target_pairs={{0,192},{64,0},{128,64},{192,128},{1,193},{65,1},{129,65},{193,129... | collective-permute-start | bytes 1572872 | tf_op jit(solution)/shard_map/ppermute | solution.py:28
  15.4 47.8 %collective-permute-start.8 = (bf16[1024,256]{1,0:T(8,128)(2,1)S(1)}, bf16[1024,256]{1,0:T(8,128)(2,1)S(1)}, u32[]{:S(2)}, u32[]{:S(2)}) collective-permute-start(bf16[1024,256]{1,0:T(8,128)(2,1)S(1)} %copy-done.2), channel_id=1, source_target_pairs={{0,1},{1,0},{2,3},{3,2},{4,5},{5,4},{6,7},{7,6},{8,9},{9,8},{10,11... | collective-permute-start | bytes 1572872 | tf_op jit(solution)/shard_map/ppermute | solution.py:23
  16.2 48.6 %collective-permute-start.14 = (bf16[256,1024]{1,0:T(8,128)(2,1)}, bf16[256,1024]{1,0:T(8,128)(2,1)}, u32[]{:S(2)}, u32[]{:S(2)}) collective-permute-start(bf16[256,1024]{1,0:T(8,128)(2,1)} %refs_0_.4), channel_id=1, source_target_pairs={{0,64},{64,128},{128,192},{192,0},{1,65},{65,129},{129,193},{193,1... | collective-permute-start | bytes 1572872 | tf_op jit(solution)/shard_map/ppermute | solution.py:28
  45.1 16.9 %collective-permute-start.5 = (bf16[512,256]{1,0:T(8,128)(2,1)S(1)}, bf16[512,256]{1,0:T(8,128)(2,1)}, u32[]{:S(2)}, u32[]{:S(2)}) collective-permute-start(bf16[512,256]{1,0:T(8,128)(2,1)S(1)} %slice.8), channel_id=1, source_target_pairs={{0,64},{64,128},{128,192},{192,0},{1,65},{65,129},{129,193},{193,1... | collective-permute-start | bytes 786440 | tf_op jit(solution)/shard_map/ppermute | solution.py:28
  45.2 17.9 %collective-permute-start.7 = (bf16[512,256]{1,0:T(8,128)(2,1)S(1)}, bf16[512,256]{1,0:T(8,128)(2,1)}, u32[]{:S(2)}, u32[]{:S(2)}) collective-permute-start(bf16[512,256]{1,0:T(8,128)(2,1)S(1)} %slice.9), channel_id=1, source_target_pairs={{0,192},{64,0},{128,64},{192,128},{1,193},{65,1},{129,65},{193,129... | collective-permute-start | bytes 786440 | tf_op jit(solution)/shard_map/ppermute | solution.py:28
  47.9 21.8 %collective-permute-start.12 = (bf16[1024,256]{1,0:T(8,128)(2,1)S(1)}, bf16[1024,256]{1,0:T(8,128)(2,1)}, u32[]{:S(2)}, u32[]{:S(2)}) collective-permute-start(bf16[1024,256]{1,0:T(8,128)(2,1)S(1)} %collective-permute-done.6.refs_4_), channel_id=1, source_target_pairs={{0,1},{1,0},{2,3},{3,2},{4,5},{5,4},{6,7},{7,6},{8,9},{9,8},{10,11... | collective-permute-start | bytes 1572872 | tf_op jit(solution)/shard_map/ppermute | solution.py:23
  63.9 10.5 %collective-permute-start.9 = (bf16[1024,256]{1,0:T(8,128)(2,1)S(1)}, bf16[1024,256]{1,0:T(8,128)(2,1)}, u32[]{:S(2)}, u32[]{:S(2)}) collective-permute-start(bf16[1024,256]{1,0:T(8,128)(2,1)S(1)} %collective-permute-done.4.refs_1_), channel_id=1, source_target_pairs={{0,1},{1,0},{2,3},{3,2},{4,5},{5,4},{6,7},{7,6},{8,9},{9,8},{10,11... | collective-permute-start | bytes 1572872 | tf_op jit(solution)/shard_map/ppermute | solution.py:23
  69.7 16.8 %collective-permute-start.15 = (bf16[256,1024]{1,0:T(8,128)(2,1)}, bf16[256,1024]{1,0:T(8,128)(2,1)S(1)}, u32[]{:S(2)}, u32[]{:S(2)}) collective-permute-start(bf16[256,1024]{1,0:T(8,128)(2,1)} %refs_0_.4), channel_id=1, source_target_pairs={{0,128},{64,192},{128,0},{192,64},{1,129},{65,193},{129,1},{193,65... | collective-permute-start | bytes 1572872 | tf_op jit(solution)/shard_map/ppermute | solution.py:28
  70.5 23.3 %collective-permute-start.16 = (bf16[256,1024]{1,0:T(8,128)(2,1)}, bf16[256,1024]{1,0:T(8,128)(2,1)}, u32[]{:S(2)}, u32[]{:S(2)}) collective-permute-start(bf16[256,1024]{1,0:T(8,128)(2,1)} %refs_0_.4), channel_id=1, source_target_pairs={{0,192},{64,0},{128,64},{192,128},{1,193},{65,1},{129,65},{193,129... | collective-permute-start | bytes 1572872 | tf_op jit(solution)/shard_map/ppermute | solution.py:28
  73.5 38.2 %collective-permute-start.17 = (bf16[256,1024]{1,0:T(8,128)(2,1)}, bf16[256,1024]{1,0:T(8,128)(2,1)}, u32[]{:S(2)}, u32[]{:S(2)}) collective-permute-start(bf16[256,1024]{1,0:T(8,128)(2,1)} %refs_0_.4), channel_id=1, source_target_pairs={{0,1},{1,0},{2,3},{3,2},{4,5},{5,4},{6,7},{7,6},{8,9},{9,8},{10,11... | collective-permute-start | bytes 1572872 | tf_op jit(solution)/shard_map/ppermute | solution.py:23
  74.3 40.2 %collective-permute-start.18 = (bf16[256,1024]{1,0:T(8,128)(2,1)}, bf16[256,1024]{1,0:T(8,128)(2,1)}, u32[]{:S(2)}, u32[]{:S(2)}) collective-permute-start(bf16[256,1024]{1,0:T(8,128)(2,1)} %collective-permute-done.14.refs_1_), channel_id=1, source_target_pairs={{0,1},{1,0},{2,3},{3,2},{4,5},{5,4},{6,7},{7,6},{8,9},{9,8},{10,11... | collective-permute-start | bytes 1572872 | tf_op jit(solution)/shard_map/ppermute | solution.py:23
  78.3 17.7 %all-to-all-start.1 = ((bf16[8,96,128]{2,1,0:T(8,128)(2,1)}), bf16[8,96,128]{2,1,0:T(8,128)(2,1)S(1)}, u32[]{:S(2)}, u32[]{:S(2)}) async-start(bf16[8,96,128]{2,1,0:T(8,128)(2,1)} %shard_map.76), calls=%async_computation.1 | async-start | bytes 393216 | tf_op jit(solution)/shard_map/all_to_all | solution.py:19
  86.5 28.1 %collective-permute-start.19 = (bf16[256,1024]{1,0:T(8,128)(2,1)S(1)}, bf16[256,1024]{1,0:T(8,128)(2,1)}, u32[]{:S(2)}, u32[]{:S(2)}) collective-permute-start(bf16[256,1024]{1,0:T(8,128)(2,1)S(1)} %collective-permute-done.15.refs_2_), channel_id=1, source_target_pairs={{0,1},{1,0},{2,3},{3,2},{4,5},{5,4},{6,7},{7,6},{8,9},{9,8},{10,11... | collective-permute-start | bytes 1572872 | tf_op jit(solution)/shard_map/ppermute | solution.py:23
  93.7 20.9 %collective-permute-start.20 = (bf16[256,1024]{1,0:T(8,128)(2,1)}, bf16[256,1024]{1,0:T(8,128)(2,1)}, u32[]{:S(2)}, u32[]{:S(2)}) collective-permute-start(bf16[256,1024]{1,0:T(8,128)(2,1)} %collective-permute-done.16.refs_3_), channel_id=1, source_target_pairs={{0,1},{1,0},{2,3},{3,2},{4,5},{5,4},{6,7},{7,6},{8,9},{9,8},{10,11... | collective-permute-start | bytes 1572872 | tf_op jit(solution)/shard_map/ppermute | solution.py:23
  96.7 23.5 %all-to-all-start.2 = ((bf16[8,104,128]{2,1,0:T(8,128)(2,1)}), bf16[8,104,128]{2,1,0:T(8,128)(2,1)S(1)}, u32[]{:S(2)}, u32[]{:S(2)}) async-start(bf16[8,104,128]{2,1,0:T(8,128)(2,1)} %get-tuple-element.17), calls=%async_computation.2 | async-start | bytes 425984 | tf_op jit(solution)/shard_map/all_to_all | solution.py:19
  111.0 28.3 %collective-permute-start.27 = (bf16[1024,256]{1,0:T(8,128)(2,1)S(1)}, bf16[1024,256]{1,0:T(8,128)(2,1)S(1)}, u32[]{:S(2)}, u32[]{:S(2)}) collective-permute-start(bf16[1024,256]{1,0:T(8,128)(2,1)S(1)} %copy-done.3), channel_id=1, source_target_pairs={{0,64},{64,128},{128,192},{192,0},{1,65},{65,129},{129,193},{193,1... | collective-permute-start | bytes 1572872 | tf_op jit(solution)/shard_map/ppermute | solution.py:28
  111.7 27.7 %collective-permute-start.28 = (bf16[1024,256]{1,0:T(8,128)(2,1)S(1)}, bf16[1024,256]{1,0:T(8,128)(2,1)S(1)}, u32[]{:S(2)}, u32[]{:S(2)}) collective-permute-start(bf16[1024,256]{1,0:T(8,128)(2,1)S(1)} %copy-done.3), channel_id=1, source_target_pairs={{0,128},{64,192},{128,0},{192,64},{1,129},{65,193},{129,1},{193,65... | collective-permute-start | bytes 1572872 | tf_op jit(solution)/shard_map/ppermute | solution.py:28
  114.6 25.2 %collective-permute-start.29 = (bf16[1024,256]{1,0:T(8,128)(2,1)S(1)}, bf16[1024,256]{1,0:T(8,128)(2,1)S(1)}, u32[]{:S(2)}, u32[]{:S(2)}) collective-permute-start(bf16[1024,256]{1,0:T(8,128)(2,1)S(1)} %copy-done.3), channel_id=1, source_target_pairs={{0,192},{64,0},{128,64},{192,128},{1,193},{65,1},{129,65},{193,129... | collective-permute-start | bytes 1572872 | tf_op jit(solution)/shard_map/ppermute | solution.py:28
  133.2 16.3 %collective-permute-start.30 = (bf16[1024,256]{1,0:T(8,128)(2,1)S(1)}, bf16[1024,256]{1,0:T(8,128)(2,1)S(1)}, u32[]{:S(2)}, u32[]{:S(2)}) collective-permute-start(bf16[1024,256]{1,0:T(8,128)(2,1)S(1)} %copy-done.3), channel_id=1, source_target_pairs={{0,1},{1,0},{2,3},{3,2},{4,5},{5,4},{6,7},{7,6},{8,9},{9,8},{10,11... | collective-permute-start | bytes 1572872 | tf_op jit(solution)/shard_map/ppermute | solution.py:23
  139.3 10.3 %collective-permute-start.31 = (bf16[1024,256]{1,0:T(8,128)(2,1)S(1)}, bf16[1024,256]{1,0:T(8,128)(2,1)S(1)}, u32[]{:S(2)}, u32[]{:S(2)}) collective-permute-start(bf16[1024,256]{1,0:T(8,128)(2,1)S(1)} %collective-permute-done.27.refs_1_), channel_id=1, source_target_pairs={{0,1},{1,0},{2,3},{3,2},{4,5},{5,4},{6,7},{7,6},{8,9},{9,8},{10,11... | collective-permute-start | bytes 1572872 | tf_op jit(solution)/shard_map/ppermute | solution.py:23
  139.4 10.2 %collective-permute-start.32 = (bf16[1024,256]{1,0:T(8,128)(2,1)S(1)}, bf16[1024,256]{1,0:T(8,128)(2,1)S(1)}, u32[]{:S(2)}, u32[]{:S(2)}) collective-permute-start(bf16[1024,256]{1,0:T(8,128)(2,1)S(1)} %collective-permute-done.28.refs_2_), channel_id=1, source_target_pairs={{0,1},{1,0},{2,3},{3,2},{4,5},{5,4},{6,7},{7,6},{8,9},{9,8},{10,11... | collective-permute-start | bytes 1572872 | tf_op jit(solution)/shard_map/ppermute | solution.py:23
  183.9 9.9 %collective-permute-start.35 = (bf16[8,96,128]{2,1,0:T(8,128)(2,1)S(1)}, bf16[8,96,128]{2,1,0:T(8,128)(2,1)S(1)}, u32[]{:S(2)}, u32[]{:S(2)}) collective-permute-start(bf16[8,96,128]{2,1,0:T(8,128)(2,1)S(1)} %all_to_all.26.own), channel_id=1, source_target_pairs={{0,1},{1,0},{2,3},{3,2},{4,5},{5,4},{6,7},{7,6},{8,9},{9,8},{10,11... | collective-permute-start | bytes 589832 | tf_op jit(solution)/shard_map/ppermute | solution.py:23
  (28 other events, 246.2 us)

commit v8 on v7

--- a/solution.py
+++ b/solution.py
@@ -39,18 +39,24 @@
     return lax.ppermute(a, ("y", "z"), perm)
 
 
-def call(kernel, out, scratch=(), limit=16, whole=None, update=None):
+def call(kernel, out, scratch=(), limit=16, whole=None, update=None, loose=0):
     vmem = pl.BlockSpec(memory_space=pltpu.VMEM)
     lies = pl.BlockSpec(memory_space=pltpu.HBM if update is None else pl.ANY)
 
     def run(*args):
         first = len(args) if whole is None else whole
         if update is None:
-            args = [*args[:first], *(pltpu.with_memory_space_constraint(a, pltpu.HBM) for a in args[first:])]
+            firm = len(args) - loose
+            args = [
+                pltpu.with_memory_space_constraint(a, pltpu.HBM) if first <= i < firm else a
+                for i, a in enumerate(args)
+            ]
         return pl.pallas_call(
             kernel,
             out_shape=out,
-            in_specs=[vmem] * first + [lies] * (len(args) - first),
+            in_specs=[vmem] * first
+            + [lies] * (len(args) - first - loose)
+            + [pl.BlockSpec(memory_space=pl.ANY)] * loose,
             out_specs=jax.tree.map(lambda _: vmem if update is None else lies, out),
             scratch_shapes=list(scratch),
             input_output_aliases={} if update is None else {update: 0},
@@ -312,18 +318,18 @@
     hidden = activate(parts)
 
     hidden = from_x_ring(hidden, nx)
-    branch = call(down_kernel, down_out, held(down_first, 2), whole=1)(hidden, *downs)
+    branch = call(down_kernel, down_out, held(down_first, 2), whole=1, loose=ny)(hidden, *downs)
     ups = around(up_second, swapped[1])
     branch = exchange(branch, "z")
     downs = around(down_second, swapped[2])
     finish_first = call(finish_first_kernel, (sds((per_y, LANES)), sds((nz, per_y + 8, LANES))))
     middle, payload = finish_first(branch, kept)
     payload = exchange(payload, "z")
-    parts = call(up_second_kernel, (sds((few, wide)),) * nx, held(up_second), whole=1)(payload, *ups)
+    parts = call(up_second_kernel, (sds((few, wide)),) * nx, held(up_second), whole=1, loose=ny - 1)(payload, *ups)
     parts = [parts[0]] + [along_x(parts[j], nx - j) for j in far_first(nx)]
     hidden = activate(*parts)
     hidden = from_x_ring(hidden, nx)
-    branch = call(down_kernel, down_out, held(down_second), whole=1)(hidden, *downs)
+    branch = call(down_kernel, down_out, held(down_second), whole=1, loose=ny - 1)(hidden, *downs)
     finished = call(finish_second_kernel, sds((per_y, LANES)))(exchange(branch, "z"), middle)
     rows = exchange(spread(by_plane(finished, lambda z: -(z // 2)), nz), "z")
     placed = pltpu.VMEM((2 * ny * nx, few, channels), F32)

time: 195 us -> 194 us (level)
  transfers between devices with their start and end apart: 39 -> 39, of which waited for: 11 -> 11; matrix products, arithmetic and copies ran while one was open for 0% -> 1% of each run, Pallas kernels for 5% -> 5%
where the time goes in v8:
time: 194 us; the launch traced here: 193 us
  starting transfers between devices  77.7 us (40%)
  waiting for transfers between devices  67 us (35%)
  blocking collectives  29.2 us (15%)
  Pallas kernels  15.6 us (8%)
  local copies, waits for them, and re-layouts  3.52 us (2%)
    ppermute x10, waiting for transfers between devices, along_y(): return lax.ppermute(a, 'y', [(i, (i + shift) % n) for i in range(n)])  44.6 us
    all_to_all x2, blocking collectives, exchange(): return lax.all_to_all(parts, axis, 0, 0, tiled=True)  29.2 us
    all_to_all x3, starting transfers between devices, exchange(): return lax.all_to_all(parts, axis, 0, 0, tiled=True)  27.7 us
    ppermute x15, starting transfers between devices, from_other_core(): return lax.ppermute(w, 'c', [(0, 1), (1, 0)])  26.2 us
    ppermute x9, waiting for transfers between devices, along_x(): return lax.ppermute(a, 'x', [(i, (i + shift) % n) for i in range(n)])  15.7 us
    pallas_call x10, Pallas kernels, run(): pl.pallas_call(kernel, out_shape=out, in_specs=[vmem] * first + [lies] *...  15.6 us
    ppermute x9, starting transfers between devices, along_x(): return lax.ppermute(a, 'x', [(i, (i + shift) % n) for i in range(n)])  11.8 us
    ppermute x10, starting transfers between devices, along_y(): return lax.ppermute(a, 'y', [(i, (i + shift) % n) for i in range(n)])  10.8 us
  transfers between devices with their start and end apart: 39, of which 11 were waited for; matrix products, arithmetic and copies ran while one was open for 1% of the time, Pallas kernels for 5%

profile of v8, /device:TPU:1, one launch (start us, length us, event | category | flops | bytes accessed | tf_op | source)
XLA Modules:
  0.0 193.5 jit_solution(5943721499329633622)
XLA Ops:
  0.0 3.2 %collective-permute-start = (bf16[256,1024]{1,0:T(8,128)(2,1)}, bf16[256,1024]{1,0:T(8,128)(2,1)S(1)}, u32[]{:S(2)}, u32[]{:S(2)}) collective-permute-start(bf16[256,1024]{1,0:T(8,128)(2,1)} %own.1), channel_id=1, source_target_pairs={{0,1},{1,0},{2,3},{3,2},{4,5},{5,4},{6,7},{7,6},{8,9},{9,8},{10,11... | collective-permute-start | bytes 1572872 | tf_op jit(solution)/shard_map/ppermute | solution.py:23
  3.2 2.8 %shard_map.73 = (bf16[384,2176]{1,0:T(8,128)(2,1)}, bf16[384,256]{1,0:T(8,128)(2,1)S(1)}, f32[104,128]{1,0:T(8,128)S(1)}) custom-call(bf16[768,256]{1,0:T(8,128)(2,1)} %tokens.1, f32[1,256]{1,0:T(1,128)} %bitcast.3, f32[1,256]{1,0:T(1,128)} %bitcast.4, bf16[256,1024]{1,0:T(8,128)(2,1)} %own.1), custom_call_target="tpu_custom_call" | custom-call | tf_op jit(solution)/shard_map/pallas_call | solution.py:54
  7.4 5.2 %all-to-all-start = ((bf16[16,24,2176]{2,1,0:T(8,128)(2,1)}), bf16[16,24,2176]{2,1,0:T(8,128)(2,1)S(1)}, u32[]{:S(2)}, u32[]{:S(2)}) async-start(bf16[16,24,2176]{2,1,0:T(8,128)(2,1)} %bitcast.2), calls=%async_computation | async-start | bytes 3342336 | tf_op jit(solution)/shard_map/all_to_all | solution.py:19
  16.7 28.5 %collective-permute-done.4.refs_1_ = bf16[1024,256]{1,0:T(8,128)(2,1)} collective-permute-done((bf16[1024,256]{1,0:T(8,128)(2,1)S(1)}, bf16[1024,256]{1,0:T(8,128)(2,1)}, u32[]{:S(2)}, u32[]{:S(2)}) %collective-permute-start.4) | collective-permute-done | bytes 524320 | tf_op jit(solution)/shard_map/ppermute | solution.py:28
  47.2 2.7 %collective-permute-start.7 = (bf16[512,256]{1,0:T(8,128)(2,1)S(1)}, bf16[512,256]{1,0:T(8,128)(2,1)}, u32[]{:S(2)}, u32[]{:S(2)}) collective-permute-start(bf16[512,256]{1,0:T(8,128)(2,1)S(1)} %slice.9), channel_id=1, source_target_pairs={{0,192},{64,0},{128,64},{192,128},{1,193},{65,1},{129,65},{193,129... | collective-permute-start | bytes 786440 | tf_op jit(solution)/shard_map/ppermute | solution.py:28
  49.9 2.4 %collective-permute-start.12 = (bf16[1024,256]{1,0:T(8,128)(2,1)}, bf16[1024,256]{1,0:T(8,128)(2,1)S(1)}, u32[]{:S(2)}, u32[]{:S(2)}) collective-permute-start(bf16[1024,256]{1,0:T(8,128)(2,1)} %collective-permute-done.6.refs_4_), channel_id=1, source_target_pairs={{0,1},{1,0},{2,3},{3,2},{4,5},{5,4},{6,7},{7,6},{8,9},{9,8},{10,11... | collective-permute-start | bytes 1572872 | tf_op jit(solution)/shard_map/ppermute | solution.py:23
  52.4 9.6 %collective-permute-done.5.refs_2_ = bf16[512,256]{1,0:T(8,128)(2,1)} collective-permute-done((bf16[512,256]{1,0:T(8,128)(2,1)S(1)}, bf16[512,256]{1,0:T(8,128)(2,1)}, u32[]{:S(2)}, u32[]{:S(2)}) %collective-permute-start.5) | collective-permute-done | bytes 262176 | tf_op jit(solution)/shard_map/ppermute | solution.py:28
  66.1 2.4 %collective-permute-start.2 = (bf16[24,2048]{1,0:T(8,128)(2,1)S(1)}, bf16[24,2048]{1,0:T(8,128)(2,1)S(1)}, u32[]{:S(2)}, u32[]{:S(2)}) collective-permute-start(bf16[24,2048]{1,0:T(8,128)(2,1)S(1)} %shard_map.75), channel_id=1, source_target_pairs={{0,32},{16,48},{32,0},{48,16},{1,33},{17,49},{33,1},{49,17},{2,34}... | collective-permute-start | bytes 294920 | tf_op jit(solution)/shard_map/ppermute | solution.py:33
  71.1 2.4 %collective-permute-done.2 = bf16[24,2048]{1,0:T(8,128)(2,1)S(1)} collective-permute-done((bf16[24,2048]{1,0:T(8,128)(2,1)S(1)}, bf16[24,2048]{1,0:T(8,128)(2,1)S(1)}, u32[]{:S(2)}, u32[]{:S(2)}) %collective-permute-start.2) | collective-permute-done | bytes 98336 | tf_op jit(solution)/shard_map/ppermute | solution.py:33
  74.4 3.8 %shard_map.76 = bf16[8,96,128]{2,1,0:T(8,128)(2,1)} custom-call(bf16[96,2048]{1,0:T(8,128)(2,1)S(1)} %pad_maximum_fusion.hidden, bf16[1024,256]{1,0:T(8,128)(2,1)} %refs_0_.3, bf16[1024,256]{1,0:T(8,128)(2,1)} %collective-permute-done.4.refs_1_, bf16[512,256]{1,0:T(8,128)(2,1)} %collective-permute-done.5.refs_2_, ...), custom_call_target="tpu_custom_call" | custom-call | tf_op jit(solution)/shard_map/pallas_call | solution.py:54
  78.2 8.2 %all-to-all-start.1 = ((bf16[8,96,128]{2,1,0:T(8,128)(2,1)}), bf16[8,96,128]{2,1,0:T(8,128)(2,1)S(1)}, u32[]{:S(2)}, u32[]{:S(2)}) async-start(bf16[8,96,128]{2,1,0:T(8,128)(2,1)} %shard_map.76), calls=%async_computation.1 | async-start | bytes 393216 | tf_op jit(solution)/shard_map/all_to_all | solution.py:19
  87.3 6.5 %collective-permute-done.16.refs_3_ = bf16[256,1024]{1,0:T(8,128)(2,1)} collective-permute-done((bf16[256,1024]{1,0:T(8,128)(2,1)}, bf16[256,1024]{1,0:T(8,128)(2,1)}, u32[]{:S(2)}, u32[]{:S(2)}) %collective-permute-start.16) | collective-permute-done | bytes 524320 | tf_op jit(solution)/shard_map/ppermute | solution.py:28
  96.7 14.3 %all-to-all-start.2 = ((bf16[8,104,128]{2,1,0:T(8,128)(2,1)}), bf16[8,104,128]{2,1,0:T(8,128)(2,1)S(1)}, u32[]{:S(2)}, u32[]{:S(2)}) async-start(bf16[8,104,128]{2,1,0:T(8,128)(2,1)} %get-tuple-element.17), calls=%async_computation.2 | async-start | bytes 425984 | tf_op jit(solution)/shard_map/all_to_all | solution.py:19
  111.7 2.9 %collective-permute-start.28 = (bf16[1024,256]{1,0:T(8,128)(2,1)}, bf16[1024,256]{1,0:T(8,128)(2,1)S(1)}, u32[]{:S(2)}, u32[]{:S(2)}) collective-permute-start(bf16[1024,256]{1,0:T(8,128)(2,1)} %refs_0_.5), channel_id=1, source_target_pairs={{0,128},{64,192},{128,0},{192,64},{1,129},{65,193},{129,1},{193,65... | collective-permute-start | bytes 1572872 | tf_op jit(solution)/shard_map/ppermute | solution.py:28
  114.6 5.6 %all-to-all-done.2.x = bf16[8,104,128]{2,1,0:T(8,128)(2,1)S(1)} async-done(((bf16[8,104,128]{2,1,0:T(8,128)(2,1)}), bf16[8,104,128]{2,1,0:T(8,128)(2,1)S(1)}, u32[]{:S(2)}, u32[]{:S(2)}) %all-to-all-start.2) | async-done | bytes 213024 | tf_op jit(solution)/shard_map/all_to_all | solution.py:19
  123.0 2.5 %collective-permute-start.22 = (bf16[24,2176]{1,0:T(8,128)(2,1)S(1)}, bf16[24,2176]{1,0:T(8,128)(2,1)S(1)}, u32[]{:S(2)}, u32[]{:S(2)}) collective-permute-start(bf16[24,2176]{1,0:T(8,128)(2,1)S(1)} %get-tuple-element.20), channel_id=1, source_target_pairs={{0,48},{16,0},{32,16},{48,32},{1,49},{17,1},{33,17},{49,33},{2,50}... | collective-permute-start | bytes 313352 | tf_op jit(solution)/shard_map/ppermute | solution.py:33
  128.2 4.7 %collective-permute-done.23.refs_3_ = bf16[24,2176]{1,0:T(8,128)(2,1)S(1)} collective-permute-done((bf16[24,2176]{1,0:T(8,128)(2,1)S(1)}, bf16[24,2176]{1,0:T(8,128)(2,1)S(1)}, u32[]{:S(2)}, u32[]{:S(2)}) %collective-permute-start.23) | collective-permute-done | bytes 104480 | tf_op jit(solution)/shard_map/ppermute | solution.py:33
  133.1 6.0 %collective-permute-start.30 = (bf16[1024,256]{1,0:T(8,128)(2,1)S(1)}, bf16[1024,256]{1,0:T(8,128)(2,1)S(1)}, u32[]{:S(2)}, u32[]{:S(2)}) collective-permute-start(bf16[1024,256]{1,0:T(8,128)(2,1)S(1)} %copy-done.1), channel_id=1, source_target_pairs={{0,1},{1,0},{2,3},{3,2},{4,5},{5,4},{6,7},{7,6},{8,9},{9,8},{10,11... | collective-permute-start | bytes 1572872 | tf_op jit(solution)/shard_map/ppermute | solution.py:23
  140.6 4.5 %collective-permute-done.25 = bf16[24,2048]{1,0:T(8,128)(2,1)S(1)} collective-permute-done((bf16[24,2048]{1,0:T(8,128)(2,1)S(1)}, bf16[24,2048]{1,0:T(8,128)(2,1)S(1)}, u32[]{:S(2)}, u32[]{:S(2)}) %collective-permute-start.25) | collective-permute-done | bytes 98336 | tf_op jit(solution)/shard_map/ppermute | solution.py:33
  145.1 2.7 %collective-permute-start.26 = (bf16[24,2048]{1,0:T(8,128)(2,1)S(1)}, bf16[24,2048]{1,0:T(8,128)(2,1)S(1)}, u32[]{:S(2)}, u32[]{:S(2)}) collective-permute-start(bf16[24,2048]{1,0:T(8,128)(2,1)S(1)} %shard_map.79), channel_id=1, source_target_pairs={{0,48},{16,0},{32,16},{48,32},{1,49},{17,1},{33,17},{49,33},{2,50}... | collective-permute-start | bytes 294920 | tf_op jit(solution)/shard_map/ppermute | solution.py:33
  150.3 3.1 %shard_map.80 = bf16[8,96,128]{2,1,0:T(8,128)(2,1)S(1)} custom-call(bf16[96,2048]{1,0:T(8,128)(2,1)S(1)} %pad_maximum_fusion.1.hidden, bf16[1024,256]{1,0:T(8,128)(2,1)} %refs_0_.5, bf16[1024,256]{1,0:T(8,128)(2,1)} %copy-done.2, bf16[1024,256]{1,0:T(8,128)(2,1)} %copy-done.3, bf16[1024,256]{1,0:T(8,128)(2,1)} %collective-permute-done.29.refs_3_, ...), custom_call_target="tpu_custom_call" | custom-call | tf_op jit(solution)/shard_map/pallas_call | solution.py:54
  153.4 13.9 %all_to_all.25.parts = bf16[8,96,128]{2,1,0:T(8,128)(2,1)S(1)} all-to-all(bf16[8,96,128]{2,1,0:T(8,128)(2,1)S(1)} %shard_map.80), channel_id=1, replica_groups=mesh['y'=4,'x'=4,'z'=8,'c'=2] {'z'}, dimensions={0} | all-to-all | bytes 393216 | tf_op jit(solution)/shard_map/all_to_all | solution.py:19
  168.1 15.4 %all_to_all.26.own = bf16[8,96,128]{2,1,0:T(8,128)(2,1)S(1)} all-to-all(bf16[8,96,128]{2,1,0:T(8,128)(2,1)S(1)} %broadcast_in_dim.14), channel_id=1, replica_groups=mesh['y'=4,'x'=4,'z'=8,'c'=2] {'z'}, dimensions={0} | all-to-all | bytes 393216 | tf_op jit(solution)/shard_map/all_to_all | solution.py:19
  183.5 8.1 %collective-permute-start.35 = (bf16[8,96,128]{2,1,0:T(8,128)(2,1)S(1)}, bf16[8,96,128]{2,1,0:T(8,128)(2,1)S(1)}, u32[]{:S(2)}, u32[]{:S(2)}) collective-permute-start(bf16[8,96,128]{2,1,0:T(8,128)(2,1)S(1)} %all_to_all.26.own), channel_id=1, source_target_pairs={{0,1},{1,0},{2,3},{3,2},{4,5},{5,4},{6,7},{7,6},{8,9},{9,8},{10,11... | collective-permute-start | bytes 589832 | tf_op jit(solution)/shard_map/ppermute | solution.py:23
  (83 shorter events, 31.8 us)
Async XLA Ops:
  7.4 57.0 %all-to-all-start = ((bf16[16,24,2176]{2,1,0:T(8,128)(2,1)}), bf16[16,24,2176]{2,1,0:T(8,128)(2,1)S(1)}, u32[]{:S(2)}, u32[]{:S(2)}) async-start(bf16[16,24,2176]{2,1,0:T(8,128)(2,1)} %bitcast.2), calls=%async_computation | async-start | bytes 3342336 | tf_op jit(solution)/shard_map/all_to_all | solution.py:19
  12.6 32.5 %collective-permute-start.4 = (bf16[1024,256]{1,0:T(8,128)(2,1)S(1)}, bf16[1024,256]{1,0:T(8,128)(2,1)}, u32[]{:S(2)}, u32[]{:S(2)}) collective-permute-start(bf16[1024,256]{1,0:T(8,128)(2,1)S(1)} %copy-done), channel_id=1, source_target_pairs={{0,64},{64,128},{128,192},{192,0},{1,65},{65,129},{129,193},{193,1... | collective-permute-start | bytes 1572872 | tf_op jit(solution)/shard_map/ppermute | solution.py:28
  14.1 32.1 %collective-permute-start.6 = (bf16[1024,256]{1,0:T(8,128)(2,1)S(1)}, bf16[1024,256]{1,0:T(8,128)(2,1)}, u32[]{:S(2)}, u32[]{:S(2)}) collective-permute-start(bf16[1024,256]{1,0:T(8,128)(2,1)S(1)} %copy-done), channel_id=1, source_target_pairs={{0,192},{64,0},{128,64},{192,128},{1,193},{65,1},{129,65},{193,129... | collective-permute-start | bytes 1572872 | tf_op jit(solution)/shard_map/ppermute | solution.py:28
  15.4 47.8 %collective-permute-start.8 = (bf16[1024,256]{1,0:T(8,128)(2,1)S(1)}, bf16[1024,256]{1,0:T(8,128)(2,1)S(1)}, u32[]{:S(2)}, u32[]{:S(2)}) collective-permute-start(bf16[1024,256]{1,0:T(8,128)(2,1)S(1)} %copy-done), channel_id=1, source_target_pairs={{0,1},{1,0},{2,3},{3,2},{4,5},{5,4},{6,7},{7,6},{8,9},{9,8},{10,11... | collective-permute-start | bytes 1572872 | tf_op jit(solution)/shard_map/ppermute | solution.py:23
  16.2 48.6 %collective-permute-start.14 = (bf16[256,1024]{1,0:T(8,128)(2,1)}, bf16[256,1024]{1,0:T(8,128)(2,1)}, u32[]{:S(2)}, u32[]{:S(2)}) collective-permute-start(bf16[256,1024]{1,0:T(8,128)(2,1)} %refs_0_.4), channel_id=1, source_target_pairs={{0,64},{64,128},{128,192},{192,0},{1,65},{65,129},{129,193},{193,1... | collective-permute-start | bytes 1572872 | tf_op jit(solution)/shard_map/ppermute | solution.py:28
  46.1 15.9 %collective-permute-start.5 = (bf16[512,256]{1,0:T(8,128)(2,1)S(1)}, bf16[512,256]{1,0:T(8,128)(2,1)}, u32[]{:S(2)}, u32[]{:S(2)}) collective-permute-start(bf16[512,256]{1,0:T(8,128)(2,1)S(1)} %slice.8), channel_id=1, source_target_pairs={{0,64},{64,128},{128,192},{192,0},{1,65},{65,129},{129,193},{193,1... | collective-permute-start | bytes 786440 | tf_op jit(solution)/shard_map/ppermute | solution.py:28
  47.2 16.0 %collective-permute-start.7 = (bf16[512,256]{1,0:T(8,128)(2,1)S(1)}, bf16[512,256]{1,0:T(8,128)(2,1)}, u32[]{:S(2)}, u32[]{:S(2)}) collective-permute-start(bf16[512,256]{1,0:T(8,128)(2,1)S(1)} %slice.9), channel_id=1, source_target_pairs={{0,192},{64,0},{128,64},{192,128},{1,193},{65,1},{129,65},{193,129... | collective-permute-start | bytes 786440 | tf_op jit(solution)/shard_map/ppermute | solution.py:28
  49.9 19.8 %collective-permute-start.12 = (bf16[1024,256]{1,0:T(8,128)(2,1)}, bf16[1024,256]{1,0:T(8,128)(2,1)S(1)}, u32[]{:S(2)}, u32[]{:S(2)}) collective-permute-start(bf16[1024,256]{1,0:T(8,128)(2,1)} %collective-permute-done.6.refs_4_), channel_id=1, source_target_pairs={{0,1},{1,0},{2,3},{3,2},{4,5},{5,4},{6,7},{7,6},{8,9},{9,8},{10,11... | collective-permute-start | bytes 1572872 | tf_op jit(solution)/shard_map/ppermute | solution.py:23
  64.0 10.4 %collective-permute-start.9 = (bf16[1024,256]{1,0:T(8,128)(2,1)}, bf16[1024,256]{1,0:T(8,128)(2,1)S(1)}, u32[]{:S(2)}, u32[]{:S(2)}) collective-permute-start(bf16[1024,256]{1,0:T(8,128)(2,1)} %collective-permute-done.4.refs_1_), channel_id=1, source_target_pairs={{0,1},{1,0},{2,3},{3,2},{4,5},{5,4},{6,7},{7,6},{8,9},{9,8},{10,11... | collective-permute-start | bytes 1572872 | tf_op jit(solution)/shard_map/ppermute | solution.py:23
  69.7 16.7 %collective-permute-start.15 = (bf16[256,1024]{1,0:T(8,128)(2,1)}, bf16[256,1024]{1,0:T(8,128)(2,1)}, u32[]{:S(2)}, u32[]{:S(2)}) collective-permute-start(bf16[256,1024]{1,0:T(8,128)(2,1)} %refs_0_.4), channel_id=1, source_target_pairs={{0,128},{64,192},{128,0},{192,64},{1,129},{65,193},{129,1},{193,65... | collective-permute-start | bytes 1572872 | tf_op jit(solution)/shard_map/ppermute | solution.py:28
  70.5 23.3 %collective-permute-start.16 = (bf16[256,1024]{1,0:T(8,128)(2,1)}, bf16[256,1024]{1,0:T(8,128)(2,1)}, u32[]{:S(2)}, u32[]{:S(2)}) collective-permute-start(bf16[256,1024]{1,0:T(8,128)(2,1)} %refs_0_.4), channel_id=1, source_target_pairs={{0,192},{64,0},{128,64},{192,128},{1,193},{65,1},{129,65},{193,129... | collective-permute-start | bytes 1572872 | tf_op jit(solution)/shard_map/ppermute | solution.py:28
  73.5 38.2 %collective-permute-start.17 = (bf16[256,1024]{1,0:T(8,128)(2,1)}, bf16[256,1024]{1,0:T(8,128)(2,1)}, u32[]{:S(2)}, u32[]{:S(2)}) collective-permute-start(bf16[256,1024]{1,0:T(8,128)(2,1)} %refs_0_.4), channel_id=1, source_target_pairs={{0,1},{1,0},{2,3},{3,2},{4,5},{5,4},{6,7},{7,6},{8,9},{9,8},{10,11... | collective-permute-start | bytes 1572872 | tf_op jit(solution)/shard_map/ppermute | solution.py:23
  74.4 40.2 %collective-permute-start.18 = (bf16[256,1024]{1,0:T(8,128)(2,1)}, bf16[256,1024]{1,0:T(8,128)(2,1)S(1)}, u32[]{:S(2)}, u32[]{:S(2)}) collective-permute-start(bf16[256,1024]{1,0:T(8,128)(2,1)} %collective-permute-done.14.refs_1_), channel_id=1, source_target_pairs={{0,1},{1,0},{2,3},{3,2},{4,5},{5,4},{6,7},{7,6},{8,9},{9,8},{10,11... | collective-permute-start | bytes 1572872 | tf_op jit(solution)/shard_map/ppermute | solution.py:23
  78.2 17.8 %all-to-all-start.1 = ((bf16[8,96,128]{2,1,0:T(8,128)(2,1)}), bf16[8,96,128]{2,1,0:T(8,128)(2,1)S(1)}, u32[]{:S(2)}, u32[]{:S(2)}) async-start(bf16[8,96,128]{2,1,0:T(8,128)(2,1)} %shard_map.76), calls=%async_computation.1 | async-start | bytes 393216 | tf_op jit(solution)/shard_map/all_to_all | solution.py:19
  86.4 28.2 %collective-permute-start.19 = (bf16[256,1024]{1,0:T(8,128)(2,1)}, bf16[256,1024]{1,0:T(8,128)(2,1)S(1)}, u32[]{:S(2)}, u32[]{:S(2)}) collective-permute-start(bf16[256,1024]{1,0:T(8,128)(2,1)} %collective-permute-done.15.refs_2_), channel_id=1, source_target_pairs={{0,1},{1,0},{2,3},{3,2},{4,5},{5,4},{6,7},{7,6},{8,9},{9,8},{10,11... | collective-permute-start | bytes 1572872 | tf_op jit(solution)/shard_map/ppermute | solution.py:23
  93.8 20.9 %collective-permute-start.20 = (bf16[256,1024]{1,0:T(8,128)(2,1)}, bf16[256,1024]{1,0:T(8,128)(2,1)S(1)}, u32[]{:S(2)}, u32[]{:S(2)}) collective-permute-start(bf16[256,1024]{1,0:T(8,128)(2,1)} %collective-permute-done.16.refs_3_), channel_id=1, source_target_pairs={{0,1},{1,0},{2,3},{3,2},{4,5},{5,4},{6,7},{7,6},{8,9},{9,8},{10,11... | collective-permute-start | bytes 1572872 | tf_op jit(solution)/shard_map/ppermute | solution.py:23
  96.7 23.5 %all-to-all-start.2 = ((bf16[8,104,128]{2,1,0:T(8,128)(2,1)}), bf16[8,104,128]{2,1,0:T(8,128)(2,1)S(1)}, u32[]{:S(2)}, u32[]{:S(2)}) async-start(bf16[8,104,128]{2,1,0:T(8,128)(2,1)} %get-tuple-element.17), calls=%async_computation.2 | async-start | bytes 425984 | tf_op jit(solution)/shard_map/all_to_all | solution.py:19
  111.0 28.2 %collective-permute-start.27 = (bf16[1024,256]{1,0:T(8,128)(2,1)}, bf16[1024,256]{1,0:T(8,128)(2,1)S(1)}, u32[]{:S(2)}, u32[]{:S(2)}) collective-permute-start(bf16[1024,256]{1,0:T(8,128)(2,1)} %refs_0_.5), channel_id=1, source_target_pairs={{0,64},{64,128},{128,192},{192,0},{1,65},{65,129},{129,193},{193,1... | collective-permute-start | bytes 1572872 | tf_op jit(solution)/shard_map/ppermute | solution.py:28
  111.7 27.6 %collective-permute-start.28 = (bf16[1024,256]{1,0:T(8,128)(2,1)}, bf16[1024,256]{1,0:T(8,128)(2,1)S(1)}, u32[]{:S(2)}, u32[]{:S(2)}) collective-permute-start(bf16[1024,256]{1,0:T(8,128)(2,1)} %refs_0_.5), channel_id=1, source_target_pairs={{0,128},{64,192},{128,0},{192,64},{1,129},{65,193},{129,1},{193,65... | collective-permute-start | bytes 1572872 | tf_op jit(solution)/shard_map/ppermute | solution.py:28
  114.6 25.1 %collective-permute-start.29 = (bf16[1024,256]{1,0:T(8,128)(2,1)}, bf16[1024,256]{1,0:T(8,128)(2,1)}, u32[]{:S(2)}, u32[]{:S(2)}) collective-permute-start(bf16[1024,256]{1,0:T(8,128)(2,1)} %refs_0_.5), channel_id=1, source_target_pairs={{0,192},{64,0},{128,64},{192,128},{1,193},{65,1},{129,65},{193,129... | collective-permute-start | bytes 1572872 | tf_op jit(solution)/shard_map/ppermute | solution.py:28
  133.1 16.4 %collective-permute-start.30 = (bf16[1024,256]{1,0:T(8,128)(2,1)S(1)}, bf16[1024,256]{1,0:T(8,128)(2,1)S(1)}, u32[]{:S(2)}, u32[]{:S(2)}) collective-permute-start(bf16[1024,256]{1,0:T(8,128)(2,1)S(1)} %copy-done.1), channel_id=1, source_target_pairs={{0,1},{1,0},{2,3},{3,2},{4,5},{5,4},{6,7},{7,6},{8,9},{9,8},{10,11... | collective-permute-start | bytes 1572872 | tf_op jit(solution)/shard_map/ppermute | solution.py:23
  139.2 10.4 %collective-permute-start.31 = (bf16[1024,256]{1,0:T(8,128)(2,1)S(1)}, bf16[1024,256]{1,0:T(8,128)(2,1)S(1)}, u32[]{:S(2)}, u32[]{:S(2)}) collective-permute-start(bf16[1024,256]{1,0:T(8,128)(2,1)S(1)} %collective-permute-done.27.refs_1_), channel_id=1, source_target_pairs={{0,1},{1,0},{2,3},{3,2},{4,5},{5,4},{6,7},{7,6},{8,9},{9,8},{10,11... | collective-permute-start | bytes 1572872 | tf_op jit(solution)/shard_map/ppermute | solution.py:23
  139.3 10.2 %collective-permute-start.32 = (bf16[1024,256]{1,0:T(8,128)(2,1)S(1)}, bf16[1024,256]{1,0:T(8,128)(2,1)S(1)}, u32[]{:S(2)}, u32[]{:S(2)}) collective-permute-start(bf16[1024,256]{1,0:T(8,128)(2,1)S(1)} %collective-permute-done.28.refs_2_), channel_id=1, source_target_pairs={{0,1},{1,0},{2,3},{3,2},{4,5},{5,4},{6,7},{7,6},{8,9},{9,8},{10,11... | collective-permute-start | bytes 1572872 | tf_op jit(solution)/shard_map/ppermute | solution.py:23
  139.7 9.9 %collective-permute-start.33 = (bf16[1024,256]{1,0:T(8,128)(2,1)}, bf16[1024,256]{1,0:T(8,128)(2,1)S(1)}, u32[]{:S(2)}, u32[]{:S(2)}) collective-permute-start(bf16[1024,256]{1,0:T(8,128)(2,1)} %collective-permute-done.29.refs_3_), channel_id=1, source_target_pairs={{0,1},{1,0},{2,3},{3,2},{4,5},{5,4},{6,7},{7,6},{8,9},{9,8},{10,11... | collective-permute-start | bytes 1572872 | tf_op jit(solution)/shard_map/ppermute | solution.py:23
  (21 other events, 126.4 us)

commit v9 on v8

--- a/solution.py
+++ b/solution.py
@@ -318,18 +318,18 @@
     hidden = activate(parts)
 
     hidden = from_x_ring(hidden, nx)
-    branch = call(down_kernel, down_out, held(down_first, 2), whole=1, loose=ny)(hidden, *downs)
+    branch = call(down_kernel, down_out, held(down_first, 2), whole=1, loose=2 * ny + 1)(hidden, *downs)
     ups = around(up_second, swapped[1])
     branch = exchange(branch, "z")
     downs = around(down_second, swapped[2])
     finish_first = call(finish_first_kernel, (sds((per_y, LANES)), sds((nz, per_y + 8, LANES))))
     middle, payload = finish_first(branch, kept)
     payload = exchange(payload, "z")
-    parts = call(up_second_kernel, (sds((few, wide)),) * nx, held(up_second), whole=1, loose=ny - 1)(payload, *ups)
+    parts = call(up_second_kernel, (sds((few, wide)),) * nx, held(up_second), whole=1, loose=2 * ny - 1)(payload, *ups)
     parts = [parts[0]] + [along_x(parts[j], nx - j) for j in far_first(nx)]
     hidden = activate(*parts)
     hidden = from_x_ring(hidden, nx)
-    branch = call(down_kernel, down_out, held(down_second), whole=1, loose=ny - 1)(hidden, *downs)
+    branch = call(down_kernel, down_out, held(down_second), whole=1, loose=2 * ny - 1)(hidden, *downs)
     finished = call(finish_second_kernel, sds((per_y, LANES)))(exchange(branch, "z"), middle)
     rows = exchange(spread(by_plane(finished, lambda z: -(z // 2)), nz), "z")
     placed = pltpu.VMEM((2 * ny * nx, few, channels), F32)

time: 194 us -> 194 us (level)
    ppermute x10, waiting for transfers between devices: 44.6 us -> 46.6 us  [along_y(): return lax.ppermute(a, 'y', [(i, (i + shift) % n) for i in range(n)])]
  transfers between devices with their start and end apart: 39 -> 39, of which waited for: 11 -> 11; matrix products, arithmetic and copies ran while one was open for 1% -> 0% of each run, Pallas kernels for 5% -> 5%
where the time goes in v9:
time: 194 us; the launch traced here: 193 us
  starting transfers between devices  76.4 us (39%)
  waiting for transfers between devices  68.5 us (35%)
  blocking collectives  29.6 us (15%)
  Pallas kernels  15.3 us (8%)
  local copies, waits for them, and re-layouts  2.71 us (1%)
    ppermute x10, waiting for transfers between devices, along_y(): return lax.ppermute(a, 'y', [(i, (i + shift) % n) for i in range(n)])  46.6 us
    all_to_all x2, blocking collectives, exchange(): return lax.all_to_all(parts, axis, 0, 0, tiled=True)  29.6 us
    all_to_all x3, starting transfers between devices, exchange(): return lax.all_to_all(parts, axis, 0, 0, tiled=True)  27.5 us
    ppermute x15, starting transfers between devices, from_other_core(): return lax.ppermute(w, 'c', [(0, 1), (1, 0)])  25.2 us
    ppermute x9, waiting for transfers between devices, along_x(): return lax.ppermute(a, 'x', [(i, (i + shift) % n) for i in range(n)])  15.9 us
    pallas_call x10, Pallas kernels, run(): pl.pallas_call(kernel, out_shape=out, in_specs=[vmem] * first + [lies] *...  15.3 us
    ppermute x9, starting transfers between devices, along_x(): return lax.ppermute(a, 'x', [(i, (i + shift) % n) for i in range(n)])  11.8 us
    ppermute x10, starting transfers between devices, along_y(): return lax.ppermute(a, 'y', [(i, (i + shift) % n) for i in range(n)])  10.6 us
  transfers between devices with their start and end apart: 39, of which 11 were waited for; matrix products, arithmetic and copies ran while one was open for 0% of the time, Pallas kernels for 5%

profile of v9, /device:TPU:1, one launch (start us, length us, event | category | flops | bytes accessed | tf_op | source)
XLA Modules:
  0.0 192.9 jit_solution(3883448472616317158)
XLA Ops:
  0.0 3.2 %collective-permute-start = (bf16[256,1024]{1,0:T(8,128)(2,1)}, bf16[256,1024]{1,0:T(8,128)(2,1)S(1)}, u32[]{:S(2)}, u32[]{:S(2)}) collective-permute-start(bf16[256,1024]{1,0:T(8,128)(2,1)} %own.1), channel_id=1, source_target_pairs={{0,1},{1,0},{2,3},{3,2},{4,5},{5,4},{6,7},{7,6},{8,9},{9,8},{10,11... | collective-permute-start | bytes 1572872 | tf_op jit(solution)/shard_map/ppermute | solution.py:23
  3.2 2.8 %shard_map.73 = (bf16[384,2176]{1,0:T(8,128)(2,1)}, bf16[384,256]{1,0:T(8,128)(2,1)S(1)}, f32[104,128]{1,0:T(8,128)S(1)}) custom-call(bf16[768,256]{1,0:T(8,128)(2,1)} %tokens.1, f32[1,256]{1,0:T(1,128)} %bitcast.3, f32[1,256]{1,0:T(1,128)} %bitcast.4, bf16[256,1024]{1,0:T(8,128)(2,1)} %own.1), custom_call_target="tpu_custom_call" | custom-call | tf_op jit(solution)/shard_map/pallas_call | solution.py:54
  7.4 5.1 %all-to-all-start = ((bf16[16,24,2176]{2,1,0:T(8,128)(2,1)}), bf16[16,24,2176]{2,1,0:T(8,128)(2,1)S(1)}, u32[]{:S(2)}, u32[]{:S(2)}) async-start(bf16[16,24,2176]{2,1,0:T(8,128)(2,1)} %bitcast.2), calls=%async_computation | async-start | bytes 3342336 | tf_op jit(solution)/shard_map/all_to_all | solution.py:19
  16.5 28.5 %collective-permute-done.4.refs_1_ = bf16[1024,256]{1,0:T(8,128)(2,1)S(1)} collective-permute-done((bf16[1024,256]{1,0:T(8,128)(2,1)}, bf16[1024,256]{1,0:T(8,128)(2,1)S(1)}, u32[]{:S(2)}, u32[]{:S(2)}) %collective-permute-start.4) | collective-permute-done | bytes 524320 | tf_op jit(solution)/shard_map/ppermute | solution.py:28
  45.1 2.7 %collective-permute-start.7 = (bf16[512,256]{1,0:T(8,128)(2,1)S(1)}, bf16[512,256]{1,0:T(8,128)(2,1)}, u32[]{:S(2)}, u32[]{:S(2)}) collective-permute-start(bf16[512,256]{1,0:T(8,128)(2,1)S(1)} %slice.9), channel_id=1, source_target_pairs={{0,192},{64,0},{128,64},{192,128},{1,193},{65,1},{129,65},{193,129... | collective-permute-start | bytes 786440 | tf_op jit(solution)/shard_map/ppermute | solution.py:28
  47.8 2.4 %collective-permute-start.12 = (bf16[1024,256]{1,0:T(8,128)(2,1)S(1)}, bf16[1024,256]{1,0:T(8,128)(2,1)}, u32[]{:S(2)}, u32[]{:S(2)}) collective-permute-start(bf16[1024,256]{1,0:T(8,128)(2,1)S(1)} %collective-permute-done.6.refs_4_), channel_id=1, source_target_pairs={{0,1},{1,0},{2,3},{3,2},{4,5},{5,4},{6,7},{7,6},{8,9},{9,8},{10,11... | collective-permute-start | bytes 1572872 | tf_op jit(solution)/shard_map/ppermute | solution.py:23
  50.3 11.5 %collective-permute-done.5.refs_2_ = bf16[512,256]{1,0:T(8,128)(2,1)S(1)} collective-permute-done((bf16[512,256]{1,0:T(8,128)(2,1)S(1)}, bf16[512,256]{1,0:T(8,128)(2,1)S(1)}, u32[]{:S(2)}, u32[]{:S(2)}) %collective-permute-start.5) | collective-permute-done | bytes 262176 | tf_op jit(solution)/shard_map/ppermute | solution.py:28
  70.8 2.4 %collective-permute-done.2 = bf16[24,2048]{1,0:T(8,128)(2,1)S(1)} collective-permute-done((bf16[24,2048]{1,0:T(8,128)(2,1)S(1)}, bf16[24,2048]{1,0:T(8,128)(2,1)S(1)}, u32[]{:S(2)}, u32[]{:S(2)}) %collective-permute-start.2) | collective-permute-done | bytes 98336 | tf_op jit(solution)/shard_map/ppermute | solution.py:33
  74.2 3.7 %shard_map.76 = bf16[8,96,128]{2,1,0:T(8,128)(2,1)} custom-call(bf16[96,2048]{1,0:T(8,128)(2,1)S(1)} %pad_maximum_fusion.hidden, bf16[1024,256]{1,0:T(8,128)(2,1)} %refs_0_.3, bf16[1024,256]{1,0:T(8,128)(2,1)S(1)} %collective-permute-done.4.refs_1_, bf16[512,256]{1,0:T(8,128)(2,1)S(1)} %collective-permute-done.5.refs_2_, ...), custom_call_target="tpu_custom_call" | custom-call | tf_op jit(solution)/shard_map/pallas_call | solution.py:54
  77.9 8.2 %all-to-all-start.1 = ((bf16[8,96,128]{2,1,0:T(8,128)(2,1)}), bf16[8,96,128]{2,1,0:T(8,128)(2,1)S(1)}, u32[]{:S(2)}, u32[]{:S(2)}) async-start(bf16[8,96,128]{2,1,0:T(8,128)(2,1)} %shard_map.76), calls=%async_computation.1 | async-start | bytes 393216 | tf_op jit(solution)/shard_map/all_to_all | solution.py:19
  87.0 6.6 %collective-permute-done.16.refs_3_ = bf16[256,1024]{1,0:T(8,128)(2,1)} collective-permute-done((bf16[256,1024]{1,0:T(8,128)(2,1)}, bf16[256,1024]{1,0:T(8,128)(2,1)}, u32[]{:S(2)}, u32[]{:S(2)}) %collective-permute-start.16) | collective-permute-done | bytes 524320 | tf_op jit(solution)/shard_map/ppermute | solution.py:28
  96.5 14.3 %all-to-all-start.2 = ((bf16[8,104,128]{2,1,0:T(8,128)(2,1)}), bf16[8,104,128]{2,1,0:T(8,128)(2,1)S(1)}, u32[]{:S(2)}, u32[]{:S(2)}) async-start(bf16[8,104,128]{2,1,0:T(8,128)(2,1)} %get-tuple-element.17), calls=%async_computation.2 | async-start | bytes 425984 | tf_op jit(solution)/shard_map/all_to_all | solution.py:19
  112.2 2.9 %collective-permute-start.28 = (bf16[1024,256]{1,0:T(8,128)(2,1)}, bf16[1024,256]{1,0:T(8,128)(2,1)S(1)}, u32[]{:S(2)}, u32[]{:S(2)}) collective-permute-start(bf16[1024,256]{1,0:T(8,128)(2,1)} %refs_0_.5), channel_id=1, source_target_pairs={{0,128},{64,192},{128,0},{192,64},{1,129},{65,193},{129,1},{193,65... | collective-permute-start | bytes 1572872 | tf_op jit(solution)/shard_map/ppermute | solution.py:28
  115.1 4.9 %all-to-all-done.2.x = bf16[8,104,128]{2,1,0:T(8,128)(2,1)S(1)} async-done(((bf16[8,104,128]{2,1,0:T(8,128)(2,1)}), bf16[8,104,128]{2,1,0:T(8,128)(2,1)S(1)}, u32[]{:S(2)}, u32[]{:S(2)}) %all-to-all-start.2) | async-done | bytes 213024 | tf_op jit(solution)/shard_map/all_to_all | solution.py:19
  123.7 2.5 %collective-permute-start.22 = (bf16[24,2176]{1,0:T(8,128)(2,1)S(1)}, bf16[24,2176]{1,0:T(8,128)(2,1)S(1)}, u32[]{:S(2)}, u32[]{:S(2)}) collective-permute-start(bf16[24,2176]{1,0:T(8,128)(2,1)S(1)} %get-tuple-element.20), channel_id=1, source_target_pairs={{0,48},{16,0},{32,16},{48,32},{1,49},{17,1},{33,17},{49,33},{2,50}... | collective-permute-start | bytes 313352 | tf_op jit(solution)/shard_map/ppermute | solution.py:33
  126.2 2.6 %collective-permute-done.21.refs_1_ = bf16[24,2176]{1,0:T(8,128)(2,1)S(1)} collective-permute-done((bf16[24,2176]{1,0:T(8,128)(2,1)S(1)}, bf16[24,2176]{1,0:T(8,128)(2,1)S(1)}, u32[]{:S(2)}, u32[]{:S(2)}) %collective-permute-start.21) | collective-permute-done | bytes 104480 | tf_op jit(solution)/shard_map/ppermute | solution.py:33
  129.1 4.6 %collective-permute-done.23.refs_3_ = bf16[24,2176]{1,0:T(8,128)(2,1)S(1)} collective-permute-done((bf16[24,2176]{1,0:T(8,128)(2,1)S(1)}, bf16[24,2176]{1,0:T(8,128)(2,1)S(1)}, u32[]{:S(2)}, u32[]{:S(2)}) %collective-permute-start.23) | collective-permute-done | bytes 104480 | tf_op jit(solution)/shard_map/ppermute | solution.py:33
  134.0 5.0 %collective-permute-start.30 = (bf16[1024,256]{1,0:T(8,128)(2,1)}, bf16[1024,256]{1,0:T(8,128)(2,1)S(1)}, u32[]{:S(2)}, u32[]{:S(2)}) collective-permute-start(bf16[1024,256]{1,0:T(8,128)(2,1)} %refs_0_.5), channel_id=1, source_target_pairs={{0,1},{1,0},{2,3},{3,2},{4,5},{5,4},{6,7},{7,6},{8,9},{9,8},{10,11... | collective-permute-start | bytes 1572872 | tf_op jit(solution)/shard_map/ppermute | solution.py:23
  140.5 4.4 %collective-permute-done.25 = bf16[24,2048]{1,0:T(8,128)(2,1)S(1)} collective-permute-done((bf16[24,2048]{1,0:T(8,128)(2,1)S(1)}, bf16[24,2048]{1,0:T(8,128)(2,1)S(1)}, u32[]{:S(2)}, u32[]{:S(2)}) %collective-permute-start.25) | collective-permute-done | bytes 98336 | tf_op jit(solution)/shard_map/ppermute | solution.py:33
  145.0 2.8 %collective-permute-start.26 = (bf16[24,2048]{1,0:T(8,128)(2,1)S(1)}, bf16[24,2048]{1,0:T(8,128)(2,1)S(1)}, u32[]{:S(2)}, u32[]{:S(2)}) collective-permute-start(bf16[24,2048]{1,0:T(8,128)(2,1)S(1)} %shard_map.79), channel_id=1, source_target_pairs={{0,48},{16,0},{32,16},{48,32},{1,49},{17,1},{33,17},{49,33},{2,50}... | collective-permute-start | bytes 294920 | tf_op jit(solution)/shard_map/ppermute | solution.py:33
  149.5 3.0 %shard_map.80 = bf16[8,96,128]{2,1,0:T(8,128)(2,1)S(1)} custom-call(bf16[96,2048]{1,0:T(8,128)(2,1)S(1)} %pad_maximum_fusion.1.hidden, bf16[1024,256]{1,0:T(8,128)(2,1)} %refs_0_.5, bf16[1024,256]{1,0:T(8,128)(2,1)S(1)} %collective-permute-done.27.refs_1_, bf16[1024,256]{1,0:T(8,128)(2,1)S(1)} %collective-permute-done.28.refs_2_, ...), custom_call_target="tpu_custom_call" | custom-call | tf_op jit(solution)/shard_map/pallas_call | solution.py:54
  152.5 14.2 %all_to_all.25.parts = bf16[8,96,128]{2,1,0:T(8,128)(2,1)S(1)} all-to-all(bf16[8,96,128]{2,1,0:T(8,128)(2,1)S(1)} %shard_map.80), channel_id=1, replica_groups=mesh['y'=4,'x'=4,'z'=8,'c'=2] {'z'}, dimensions={0} | all-to-all | bytes 393216 | tf_op jit(solution)/shard_map/all_to_all | solution.py:19
  167.4 15.4 %all_to_all.26.own = bf16[8,96,128]{2,1,0:T(8,128)(2,1)S(1)} all-to-all(bf16[8,96,128]{2,1,0:T(8,128)(2,1)S(1)} %broadcast_in_dim.14), channel_id=1, replica_groups=mesh['y'=4,'x'=4,'z'=8,'c'=2] {'z'}, dimensions={0} | all-to-all | bytes 393216 | tf_op jit(solution)/shard_map/all_to_all | solution.py:19
  182.8 8.2 %collective-permute-start.35 = (bf16[8,96,128]{2,1,0:T(8,128)(2,1)S(1)}, bf16[8,96,128]{2,1,0:T(8,128)(2,1)S(1)}, u32[]{:S(2)}, u32[]{:S(2)}) collective-permute-start(bf16[8,96,128]{2,1,0:T(8,128)(2,1)S(1)} %all_to_all.26.own), channel_id=1, source_target_pairs={{0,1},{1,0},{2,3},{3,2},{4,5},{5,4},{6,7},{7,6},{8,9},{9,8},{10,11... | collective-permute-start | bytes 589832 | tf_op jit(solution)/shard_map/ppermute | solution.py:23
  (83 shorter events, 30.8 us)
Async XLA Ops:
  7.4 56.8 %all-to-all-start = ((bf16[16,24,2176]{2,1,0:T(8,128)(2,1)}), bf16[16,24,2176]{2,1,0:T(8,128)(2,1)S(1)}, u32[]{:S(2)}, u32[]{:S(2)}) async-start(bf16[16,24,2176]{2,1,0:T(8,128)(2,1)} %bitcast.2), calls=%async_computation | async-start | bytes 3342336 | tf_op jit(solution)/shard_map/all_to_all | solution.py:19
  12.5 32.4 %collective-permute-start.4 = (bf16[1024,256]{1,0:T(8,128)(2,1)}, bf16[1024,256]{1,0:T(8,128)(2,1)S(1)}, u32[]{:S(2)}, u32[]{:S(2)}) collective-permute-start(bf16[1024,256]{1,0:T(8,128)(2,1)} %refs_0_.3), channel_id=1, source_target_pairs={{0,64},{64,128},{128,192},{192,0},{1,65},{65,129},{129,193},{193,1... | collective-permute-start | bytes 1572872 | tf_op jit(solution)/shard_map/ppermute | solution.py:28
  13.9 31.2 %collective-permute-start.6 = (bf16[1024,256]{1,0:T(8,128)(2,1)}, bf16[1024,256]{1,0:T(8,128)(2,1)S(1)}, u32[]{:S(2)}, u32[]{:S(2)}) collective-permute-start(bf16[1024,256]{1,0:T(8,128)(2,1)} %refs_0_.3), channel_id=1, source_target_pairs={{0,192},{64,0},{128,64},{192,128},{1,193},{65,1},{129,65},{193,129... | collective-permute-start | bytes 1572872 | tf_op jit(solution)/shard_map/ppermute | solution.py:28
  15.3 47.7 %collective-permute-start.8 = (bf16[1024,256]{1,0:T(8,128)(2,1)}, bf16[1024,256]{1,0:T(8,128)(2,1)S(1)}, u32[]{:S(2)}, u32[]{:S(2)}) collective-permute-start(bf16[1024,256]{1,0:T(8,128)(2,1)} %refs_0_.3), channel_id=1, source_target_pairs={{0,1},{1,0},{2,3},{3,2},{4,5},{5,4},{6,7},{7,6},{8,9},{9,8},{10,11... | collective-permute-start | bytes 1572872 | tf_op jit(solution)/shard_map/ppermute | solution.py:23
  16.1 48.5 %collective-permute-start.14 = (bf16[256,1024]{1,0:T(8,128)(2,1)}, bf16[256,1024]{1,0:T(8,128)(2,1)S(1)}, u32[]{:S(2)}, u32[]{:S(2)}) collective-permute-start(bf16[256,1024]{1,0:T(8,128)(2,1)} %refs_0_.4), channel_id=1, source_target_pairs={{0,64},{64,128},{128,192},{192,0},{1,65},{65,129},{129,193},{193,1... | collective-permute-start | bytes 1572872 | tf_op jit(solution)/shard_map/ppermute | solution.py:28
  45.0 16.8 %collective-permute-start.5 = (bf16[512,256]{1,0:T(8,128)(2,1)S(1)}, bf16[512,256]{1,0:T(8,128)(2,1)S(1)}, u32[]{:S(2)}, u32[]{:S(2)}) collective-permute-start(bf16[512,256]{1,0:T(8,128)(2,1)S(1)} %slice.8), channel_id=1, source_target_pairs={{0,64},{64,128},{128,192},{192,0},{1,65},{65,129},{129,193},{193,1... | collective-permute-start | bytes 786440 | tf_op jit(solution)/shard_map/ppermute | solution.py:28
  45.1 17.8 %collective-permute-start.7 = (bf16[512,256]{1,0:T(8,128)(2,1)S(1)}, bf16[512,256]{1,0:T(8,128)(2,1)}, u32[]{:S(2)}, u32[]{:S(2)}) collective-permute-start(bf16[512,256]{1,0:T(8,128)(2,1)S(1)} %slice.9), channel_id=1, source_target_pairs={{0,192},{64,0},{128,64},{192,128},{1,193},{65,1},{129,65},{193,129... | collective-permute-start | bytes 786440 | tf_op jit(solution)/shard_map/ppermute | solution.py:28
  47.8 21.7 %collective-permute-start.12 = (bf16[1024,256]{1,0:T(8,128)(2,1)S(1)}, bf16[1024,256]{1,0:T(8,128)(2,1)}, u32[]{:S(2)}, u32[]{:S(2)}) collective-permute-start(bf16[1024,256]{1,0:T(8,128)(2,1)S(1)} %collective-permute-done.6.refs_4_), channel_id=1, source_target_pairs={{0,1},{1,0},{2,3},{3,2},{4,5},{5,4},{6,7},{7,6},{8,9},{9,8},{10,11... | collective-permute-start | bytes 1572872 | tf_op jit(solution)/shard_map/ppermute | solution.py:23
  63.7 10.5 %collective-permute-start.9 = (bf16[1024,256]{1,0:T(8,128)(2,1)S(1)}, bf16[1024,256]{1,0:T(8,128)(2,1)}, u32[]{:S(2)}, u32[]{:S(2)}) collective-permute-start(bf16[1024,256]{1,0:T(8,128)(2,1)S(1)} %collective-permute-done.4.refs_1_), channel_id=1, source_target_pairs={{0,1},{1,0},{2,3},{3,2},{4,5},{5,4},{6,7},{7,6},{8,9},{9,8},{10,11... | collective-permute-start | bytes 1572872 | tf_op jit(solution)/shard_map/ppermute | solution.py:23
  69.5 16.6 %collective-permute-start.15 = (bf16[256,1024]{1,0:T(8,128)(2,1)}, bf16[256,1024]{1,0:T(8,128)(2,1)}, u32[]{:S(2)}, u32[]{:S(2)}) collective-permute-start(bf16[256,1024]{1,0:T(8,128)(2,1)} %refs_0_.4), channel_id=1, source_target_pairs={{0,128},{64,192},{128,0},{192,64},{1,129},{65,193},{129,1},{193,65... | collective-permute-start | bytes 1572872 | tf_op jit(solution)/shard_map/ppermute | solution.py:28
  70.3 23.3 %collective-permute-start.16 = (bf16[256,1024]{1,0:T(8,128)(2,1)}, bf16[256,1024]{1,0:T(8,128)(2,1)}, u32[]{:S(2)}, u32[]{:S(2)}) collective-permute-start(bf16[256,1024]{1,0:T(8,128)(2,1)} %refs_0_.4), channel_id=1, source_target_pairs={{0,192},{64,0},{128,64},{192,128},{1,193},{65,1},{129,65},{193,129... | collective-permute-start | bytes 1572872 | tf_op jit(solution)/shard_map/ppermute | solution.py:28
  73.3 38.1 %collective-permute-start.17 = (bf16[256,1024]{1,0:T(8,128)(2,1)}, bf16[256,1024]{1,0:T(8,128)(2,1)S(1)}, u32[]{:S(2)}, u32[]{:S(2)}) collective-permute-start(bf16[256,1024]{1,0:T(8,128)(2,1)} %refs_0_.4), channel_id=1, source_target_pairs={{0,1},{1,0},{2,3},{3,2},{4,5},{5,4},{6,7},{7,6},{8,9},{9,8},{10,11... | collective-permute-start | bytes 1572872 | tf_op jit(solution)/shard_map/ppermute | solution.py:23
  74.1 41.0 %collective-permute-start.18 = (bf16[256,1024]{1,0:T(8,128)(2,1)S(1)}, bf16[256,1024]{1,0:T(8,128)(2,1)}, u32[]{:S(2)}, u32[]{:S(2)}) collective-permute-start(bf16[256,1024]{1,0:T(8,128)(2,1)S(1)} %collective-permute-done.14.refs_1_), channel_id=1, source_target_pairs={{0,1},{1,0},{2,3},{3,2},{4,5},{5,4},{6,7},{7,6},{8,9},{9,8},{10,11... | collective-permute-start | bytes 1572872 | tf_op jit(solution)/shard_map/ppermute | solution.py:23
  77.9 17.9 %all-to-all-start.1 = ((bf16[8,96,128]{2,1,0:T(8,128)(2,1)}), bf16[8,96,128]{2,1,0:T(8,128)(2,1)S(1)}, u32[]{:S(2)}, u32[]{:S(2)}) async-start(bf16[8,96,128]{2,1,0:T(8,128)(2,1)} %shard_map.76), calls=%async_computation.1 | async-start | bytes 393216 | tf_op jit(solution)/shard_map/all_to_all | solution.py:19
  86.1 29.0 %collective-permute-start.19 = (bf16[256,1024]{1,0:T(8,128)(2,1)}, bf16[256,1024]{1,0:T(8,128)(2,1)S(1)}, u32[]{:S(2)}, u32[]{:S(2)}) collective-permute-start(bf16[256,1024]{1,0:T(8,128)(2,1)} %collective-permute-done.15.refs_2_), channel_id=1, source_target_pairs={{0,1},{1,0},{2,3},{3,2},{4,5},{5,4},{6,7},{7,6},{8,9},{9,8},{10,11... | collective-permute-start | bytes 1572872 | tf_op jit(solution)/shard_map/ppermute | solution.py:23
  93.5 21.6 %collective-permute-start.20 = (bf16[256,1024]{1,0:T(8,128)(2,1)}, bf16[256,1024]{1,0:T(8,128)(2,1)}, u32[]{:S(2)}, u32[]{:S(2)}) collective-permute-start(bf16[256,1024]{1,0:T(8,128)(2,1)} %collective-permute-done.16.refs_3_), channel_id=1, source_target_pairs={{0,1},{1,0},{2,3},{3,2},{4,5},{5,4},{6,7},{7,6},{8,9},{9,8},{10,11... | collective-permute-start | bytes 1572872 | tf_op jit(solution)/shard_map/ppermute | solution.py:23
  96.5 23.5 %all-to-all-start.2 = ((bf16[8,104,128]{2,1,0:T(8,128)(2,1)}), bf16[8,104,128]{2,1,0:T(8,128)(2,1)S(1)}, u32[]{:S(2)}, u32[]{:S(2)}) async-start(bf16[8,104,128]{2,1,0:T(8,128)(2,1)} %get-tuple-element.17), calls=%async_computation.2 | async-start | bytes 425984 | tf_op jit(solution)/shard_map/all_to_all | solution.py:19
  110.8 28.3 %collective-permute-start.27 = (bf16[1024,256]{1,0:T(8,128)(2,1)}, bf16[1024,256]{1,0:T(8,128)(2,1)S(1)}, u32[]{:S(2)}, u32[]{:S(2)}) collective-permute-start(bf16[1024,256]{1,0:T(8,128)(2,1)} %refs_0_.5), channel_id=1, source_target_pairs={{0,64},{64,128},{128,192},{192,0},{1,65},{65,129},{129,193},{193,1... | collective-permute-start | bytes 1572872 | tf_op jit(solution)/shard_map/ppermute | solution.py:28
  112.2 27.0 %collective-permute-start.28 = (bf16[1024,256]{1,0:T(8,128)(2,1)}, bf16[1024,256]{1,0:T(8,128)(2,1)S(1)}, u32[]{:S(2)}, u32[]{:S(2)}) collective-permute-start(bf16[1024,256]{1,0:T(8,128)(2,1)} %refs_0_.5), channel_id=1, source_target_pairs={{0,128},{64,192},{128,0},{192,64},{1,129},{65,193},{129,1},{193,65... | collective-permute-start | bytes 1572872 | tf_op jit(solution)/shard_map/ppermute | solution.py:28
  115.1 24.5 %collective-permute-start.29 = (bf16[1024,256]{1,0:T(8,128)(2,1)}, bf16[1024,256]{1,0:T(8,128)(2,1)S(1)}, u32[]{:S(2)}, u32[]{:S(2)}) collective-permute-start(bf16[1024,256]{1,0:T(8,128)(2,1)} %refs_0_.5), channel_id=1, source_target_pairs={{0,192},{64,0},{128,64},{192,128},{1,193},{65,1},{129,65},{193,129... | collective-permute-start | bytes 1572872 | tf_op jit(solution)/shard_map/ppermute | solution.py:28
  134.0 15.4 %collective-permute-start.30 = (bf16[1024,256]{1,0:T(8,128)(2,1)}, bf16[1024,256]{1,0:T(8,128)(2,1)S(1)}, u32[]{:S(2)}, u32[]{:S(2)}) collective-permute-start(bf16[1024,256]{1,0:T(8,128)(2,1)} %refs_0_.5), channel_id=1, source_target_pairs={{0,1},{1,0},{2,3},{3,2},{4,5},{5,4},{6,7},{7,6},{8,9},{9,8},{10,11... | collective-permute-start | bytes 1572872 | tf_op jit(solution)/shard_map/ppermute | solution.py:23
  139.1 10.3 %collective-permute-start.31 = (bf16[1024,256]{1,0:T(8,128)(2,1)S(1)}, bf16[1024,256]{1,0:T(8,128)(2,1)S(1)}, u32[]{:S(2)}, u32[]{:S(2)}) collective-permute-start(bf16[1024,256]{1,0:T(8,128)(2,1)S(1)} %collective-permute-done.27.refs_1_), channel_id=1, source_target_pairs={{0,1},{1,0},{2,3},{3,2},{4,5},{5,4},{6,7},{7,6},{8,9},{9,8},{10,11... | collective-permute-start | bytes 1572872 | tf_op jit(solution)/shard_map/ppermute | solution.py:23
  139.2 10.2 %collective-permute-start.32 = (bf16[1024,256]{1,0:T(8,128)(2,1)S(1)}, bf16[1024,256]{1,0:T(8,128)(2,1)S(1)}, u32[]{:S(2)}, u32[]{:S(2)}) collective-permute-start(bf16[1024,256]{1,0:T(8,128)(2,1)S(1)} %collective-permute-done.28.refs_2_), channel_id=1, source_target_pairs={{0,1},{1,0},{2,3},{3,2},{4,5},{5,4},{6,7},{7,6},{8,9},{9,8},{10,11... | collective-permute-start | bytes 1572872 | tf_op jit(solution)/shard_map/ppermute | solution.py:23
  139.6 9.8 %collective-permute-start.33 = (bf16[1024,256]{1,0:T(8,128)(2,1)S(1)}, bf16[1024,256]{1,0:T(8,128)(2,1)S(1)}, u32[]{:S(2)}, u32[]{:S(2)}) collective-permute-start(bf16[1024,256]{1,0:T(8,128)(2,1)S(1)} %collective-permute-done.29.refs_3_), channel_id=1, source_target_pairs={{0,1},{1,0},{2,3},{3,2},{4,5},{5,4},{6,7},{7,6},{8,9},{9,8},{10,11... | collective-permute-start | bytes 1572872 | tf_op jit(solution)/shard_map/ppermute | solution.py:23
  (21 other events, 111.2 us)
